TPU v7x, 256 devices: a whole 4x4x8 slice. The times are simulated.
256 devices in a mesh: sp: 64 (over z, x, core), tp: 4 (over y).
Axes of the slice: x: 4, y: 4, z: 8, core: 2. Of those that a mesh axis runs over, the one named last changes fastest.
Arguments:
- stream: bfloat16 [32768, 2048], P(('sp', 'tp')), may hold values from -6 to 6
- queries: bfloat16 [32768, 512], P('sp', 'tp'), may hold values from -6 to 6
- key_rows: bfloat16 [32768, 512], P('sp', 'tp'), may hold values from -6 to 6
- values: bfloat16 [32768, 1024], P('sp', 'tp'), may hold values from -6 to 6
- out_gate: bfloat16 [32768, 1024], P('sp', 'tp'), may hold values from -6 to 6
- fwd_decay: float32 [32768, 512], P('sp', 'tp'), may hold values from -14 to 14
- bwd_decay: float32 [32768, 512], P('sp', 'tp'), may hold values from -14 to 14
- head_gain: float32 [1024], P('tp'), may hold values from 0.1 to 1.9
- out_proj: bfloat16 [1024, 2048], replicated, may hold values from -0.1875 to 0.1875
- mix_gain: float32 [2048], replicated, may hold values from 0.1 to 1.9
- ffn_gain: float32 [2048], replicated, may hold values from 0.1 to 1.9
- moe_gain: float32 [2048], replicated, may hold values from 0.1 to 1.9
- routes: int32 [32768, 2], P(('sp', 'tp')), may hold values from 0 to 63, all different within a row; in each aligned block of 128 rows (0 to 127, 128 to 255, ...) at most 6 rows name the same one
- route_weight: float32 [32768, 2], P(('sp', 'tp')), may hold values from 0.25 to 2.5
- expert_gate: bfloat16 [64, 2048, 1024], P('sp', None, 'tp'), may hold values from -0.125 to 0.125
- expert_up: bfloat16 [64, 2048, 1024], P('sp', None, 'tp'), may hold values from -0.125 to 0.125
- expert_down: bfloat16 [64, 1024, 2048], P('sp', 'tp'), may hold values from -0.1875 to 0.1875
- shared_gate: bfloat16 [2048, 512], P(None, 'tp'), may hold values from -0.125 to 0.125
- shared_up: bfloat16 [2048, 512], P(None, 'tp'), may hold values from -0.125 to 0.125
- shared_down: bfloat16 [512, 2048], P('tp'), may hold values from -0.25 to 0.25
Outputs:
- updated: bfloat16 [32768, 2048], P(('sp', 'tp'))
Inputs may be any that keep to these rules, and one draw needn't show every extreme that they name: `routes`: each row names 2 different experts. Among the rows of one device no expert is named more than 6 times, and in every draw some device names some expert exactly 6 times.
All inputs are finite; a program needn't handle non-finite values.
Results may differ from a plain program's by a relative error of at most 0.023.
Values may be sent and summed in bfloat16 or wider, within the bound.
No kernel may reach another device: no remote copies, remote signals or barrier semaphores. Data moves between devices by JAX's collectives and lax.ppermute only.
A program may use at most 128 MiB of HBM per device.

v0:
```python
import jax
import jax.numpy as jnp
from jax import lax
from jax.sharding import Mesh
from jax.sharding import PartitionSpec as P

KEY_CHANNELS = 64
DV = 128
BLK = 64
TOPK = 2
SP = ("sp_0", "sp_1", "sp_2")
SP_TP = ("sp_0", "sp_1", "sp_2", "tp")


EPS = 1e-06
GATE_NORM = 16.0
ROPE_BASE = 10000.0


def gathered_once(array, axis):
    leaves = jax.tree.leaves(array)
    sequence = sorted(range(len(leaves)), key=lambda k: -leaves[k].size)
    width = (1, *leaves[sequence[0]].shape)[-1]
    lines = [
        jnp.pad(leaves[k].reshape(-1), (0, -leaves[k].size % width)).reshape(-1, width)
        for k in sequence
    ]
    both, at, found = (lax.all_gather(jnp.concatenate(lines), axis), 0, {})
    for k, line in zip(sequence, lines):
        share = both[:, at : at + len(line)].reshape(len(both), -1)
        found[k] = share[:, : leaves[k].size].reshape(-1, *leaves[k].shape)
        at += len(line)
    numbers = iter(range(len(leaves)))
    return jax.tree.map(lambda _: found[next(numbers)], array)


def prefix(array, axis, combine, identity):
    length, position = (lax.axis_size(axis), lax.axis_index(axis))
    everything = gathered_once(
        jax.tree.map(
            lambda part, kind: part.astype(kind),
            array,
            jax.tree.map(lambda a: jnp.bfloat16 if a.dtype == jnp.float32 else a.dtype, array),
        ),
        axis,
    )
    start = jax.tree.map(
        lambda part, zero: jnp.broadcast_to(jnp.asarray(zero, part.dtype), part.shape),
        array,
        identity,
    )

    def step(k, before):
        reached = k < position
        new = combine(
            before, jax.tree.map(lambda part, own: part[k].astype(own.dtype), everything, array)
        )
        return jax.tree.map(lambda a, b: jnp.where(reached, a, b), new, before)

    return lax.fori_loop(0, length, step, start)


def neutral_like(array, identity):
    return jax.tree.map(
        lambda a, e: jnp.broadcast_to(jnp.asarray(e, a.dtype), a.shape), array, identity
    )


def entering(array, axes, combine, identity):
    before = start = neutral_like(array, identity)
    so_far = array
    for axis in reversed(axes):
        length, position = (lax.axis_size(axis), lax.axis_index(axis))
        pieces = gathered_once(
            jax.tree.map(
                lambda part, kind: part.astype(kind),
                so_far,
                jax.tree.map(lambda a: jnp.bfloat16 if a.dtype == jnp.float32 else a.dtype, array),
            ),
            axis,
        )
        inside, so_far = (start, start)
        for k in reversed(range(length)):
            passed = k > position
            so_far = combine(
                so_far, jax.tree.map(lambda part, own: part[k].astype(own.dtype), pieces, array)
            )
            inside = jax.tree.map(lambda new, old: jnp.where(passed, new, old), so_far, inside)
        before = combine(inside, before)
    return before


def normalize(tensor):
    return tensor * lax.rsqrt(jnp.mean(tensor * tensor, axis=-1, keepdims=True) + EPS)


def rotate(tensor, positions):
    half_width = tensor.shape[-1] // 2
    frequency = ROPE_BASE ** (-jnp.arange(half_width, dtype=jnp.float32) / half_width)
    angles = positions[:, None] * frequency[None, :]
    cosine = jnp.cos(angles)[:, None, :]
    sine_part = jnp.sin(angles)[:, None, :]
    front_half = tensor[..., :half_width]
    back_half = tensor[..., half_width:]
    return jnp.concatenate(
        [front_half * cosine - back_half * sine_part, front_half * sine_part + back_half * cosine],
        axis=-1,
    )


def blockwise(query_rows, key_data, value_matrix, log_decay, start_state):
    length, head_count, key_width = query_rows.shape
    value_width = value_matrix.shape[-1]
    block_count = length // BLK
    query_blocks = query_rows.reshape(block_count, BLK, head_count, key_width)
    key_blocks = key_data.reshape(block_count, BLK, head_count, key_width)
    value_blocks = value_matrix.reshape(block_count, BLK, head_count, value_width)
    cumul = jnp.cumsum(log_decay.reshape(block_count, BLK, head_count, key_width), axis=1)
    middle = cumul[:, BLK // 2 - 1 : BLK // 2]
    query_scaled = query_blocks * jnp.exp(cumul - middle)
    key_scaled = key_blocks * jnp.exp(middle - cumul)
    scores = jnp.einsum("nthk,nshk->nhts", query_scaled, key_scaled)
    lower_mask = jnp.arange(BLK)[:, None] >= jnp.arange(BLK)[None, :]
    scores = jnp.where(lower_mask, scores, 0.0)
    within = jnp.einsum("nhts,nshv->nthv", scores, value_blocks)
    last_cumul = cumul[:, -1:]
    query_in = query_blocks * jnp.exp(cumul)
    key_out = key_blocks * jnp.exp(last_cumul - cumul)
    block_decay = jnp.exp(last_cumul[:, 0])

    def advance(carried_state, pieces):
        query_segment, key_segment, value_segment, decay_segment = pieces
        across_blocks = jnp.einsum("asu,sun->asn", query_segment, carried_state)
        carried_state = carried_state * decay_segment[:, :, None] + jnp.einsum(
            "jco,jcm->com", key_segment, value_segment
        )
        return (carried_state, across_blocks)

    final_state, across_blocks = lax.scan(
        advance, start_state, (query_in, key_out, value_blocks, block_decay)
    )
    return ((within + across_blocks).reshape(length, head_count, value_width), final_state)


def readout(query_rows, log_decay, carried_state):
    cumul = jnp.cumsum(log_decay, axis=0)
    return jnp.einsum("asu,sun->asn", query_rows * jnp.exp(cumul), carried_state)


def compose(earlier, later):
    return (earlier[0] * later[0], earlier[1] * later[0][:, :, None] + later[1])


def feed_forward(row_data, gate_mat, up_mat, down_mat):
    hidden = (
        jax.nn.silu(jnp.dot(row_data, gate_mat, preferred_element_type=jnp.float32))
        * jnp.dot(row_data, up_mat, preferred_element_type=jnp.float32)
    ).astype(jnp.bfloat16)
    return jnp.dot(hidden, down_mat, preferred_element_type=jnp.float32)


def place_slots(route_block, experts):
    flat_ids = route_block.reshape(-1)
    onehot = (flat_ids[:, None] == jnp.arange(experts, dtype=jnp.int32)[None, :]).astype(jnp.int32)
    before = jnp.cumsum(onehot, axis=0) - onehot
    return (flat_ids, jnp.sum(before * onehot, axis=1))


def fill_slots(row_data, route_block, experts, capacity):
    flat_ids, slot_ids = place_slots(route_block, experts)
    token_ids = jnp.arange(flat_ids.shape[0], dtype=jnp.int32) // route_block.shape[1]
    buffer = jnp.zeros((experts, capacity, row_data.shape[1]), row_data.dtype)
    return buffer.at[flat_ids, slot_ids].set(row_data[token_ids])


def body(
    stream,
    queries,
    key_rows,
    values,
    out_gate,
    fwd_decay,
    bwd_decay,
    head_gain,
    out_proj,
    mix_gain,
    ffn_gain,
    moe_gain,
    routes,
    route_weight,
    expert_gate,
    expert_up,
    expert_down,
    shared_gate,
    shared_up,
    shared_down,
):
    tokens_here = stream.shape[0]
    span_rows = queries.shape[0]
    heads_here = queries.shape[1] // KEY_CHANNELS
    offset = lax.axis_index(SP) * span_rows
    positions = (offset + jnp.arange(span_rows, dtype=jnp.int32)).astype(jnp.float32)
    query_rows = rotate(
        queries.astype(jnp.float32).reshape(span_rows, heads_here, KEY_CHANNELS)
        * KEY_CHANNELS ** (-0.5),
        positions,
    )
    key_data = rotate(
        key_rows.astype(jnp.float32).reshape(span_rows, heads_here, KEY_CHANNELS), positions
    )
    value_matrix = values.astype(jnp.float32).reshape(span_rows, heads_here, DV)
    fwd_log = jax.nn.log_sigmoid(fwd_decay).reshape(span_rows, heads_here, KEY_CHANNELS) / GATE_NORM
    bwd_log = (
        jax.nn.log_sigmoid(bwd_decay[::-1]).reshape(span_rows, heads_here, KEY_CHANNELS) / GATE_NORM
    )
    query_back = query_rows[::-1]
    key_back = key_data[::-1]
    value_back = value_matrix[::-1]
    zero_state = jnp.zeros((heads_here, KEY_CHANNELS, DV), jnp.float32)
    identity = (jnp.ones((heads_here, KEY_CHANNELS), jnp.float32), zero_state)
    fwd_out, fwd_final = blockwise(query_rows, key_data, value_matrix, fwd_log, zero_state)
    bwd_out, bwd_final = blockwise(query_back, key_back, value_back, bwd_log, zero_state)
    fwd_summary = (jnp.exp(jnp.sum(fwd_log, axis=0)), fwd_final)
    bwd_summary = (jnp.exp(jnp.sum(bwd_log, axis=0)), bwd_final)
    fwd_carry = prefix(fwd_summary, SP, compose, identity)[1]
    bwd_carry = entering(bwd_summary, SP, compose, identity)[1]
    fwd_out = fwd_out + readout(query_rows, fwd_log, fwd_carry)
    bwd_out = bwd_out + readout(query_back, bwd_log, bwd_carry)
    combined = normalize(fwd_out + bwd_out[::-1]) * head_gain.reshape(heads_here, DV)
    head_mixed = (
        combined.reshape(span_rows, -1) * jax.nn.silu(out_gate.astype(jnp.float32))
    ).astype(jnp.bfloat16)
    mixed_out = lax.all_to_all(head_mixed, "tp", split_axis=0, concat_axis=1, tiled=True)
    projected = jnp.dot(mixed_out, out_proj, preferred_element_type=jnp.float32)
    residual = (stream.astype(jnp.float32) + normalize(projected) * mix_gain).astype(jnp.bfloat16)
    normed = (normalize(residual.astype(jnp.float32)) * ffn_gain).astype(jnp.bfloat16)
    experts = lax.axis_size(SP)
    groups = lax.axis_size("tp")
    capacity = max(2, 3 * tokens_here * TOPK // (2 * experts))
    model_width = normed.shape[1]
    arrived = lax.all_to_all(
        fill_slots(normed, routes, experts, capacity), SP, split_axis=0, concat_axis=0, tiled=True
    )
    fanned, shared_flat = (
        lax.all_gather(arrived.reshape(experts * capacity, model_width), "tp", axis=0, tiled=True),
        lax.all_gather(normed, "tp", axis=0, tiled=True),
    )
    routed_rows = fanned.reshape(groups, experts * capacity, model_width)
    shared_rows = shared_flat.reshape(groups, tokens_here, model_width)
    width_rows = experts * capacity + tokens_here
    number = width_rows * lax.axis_size("tp") // width_rows
    routed_part = routed_rows.reshape(number * experts * capacity, model_width)
    shared_part = shared_rows.reshape(number * tokens_here, model_width)
    routed_out = feed_forward(routed_part, expert_gate[0], expert_up[0], expert_down[0]).reshape(
        number, experts * capacity, model_width
    )
    shared_out = feed_forward(shared_part, shared_gate, shared_up, shared_down).reshape(
        number, tokens_here, model_width
    )
    summed = lax.psum_scatter(
        jnp.concatenate([routed_out, shared_out], axis=1)
        .reshape(width_rows * lax.axis_size("tp"), model_width)
        .astype(jnp.bfloat16),
        "tp",
        scatter_dimension=0,
        tiled=True,
    ).astype(jnp.float32)
    routed_done = (
        summed[: experts * capacity].astype(jnp.bfloat16).reshape(experts, capacity, model_width)
    )
    routed_back = lax.all_to_all(routed_done, SP, split_axis=0, concat_axis=0, tiled=True)
    shared_sum = summed[experts * capacity :]
    flat_ids, slot_ids = place_slots(routes, experts)
    picked = routed_back.reshape(experts * capacity, model_width)[flat_ids * capacity + slot_ids]
    picked = picked.astype(jnp.float32).reshape(tokens_here, TOPK, model_width)
    mixture = shared_sum + jnp.sum(picked * route_weight[:, :, None], axis=1)
    return (residual.astype(jnp.float32) + normalize(mixture) * moe_gain).astype(jnp.bfloat16)


def solution(mesh):
    finer = Mesh(mesh.devices.reshape(8, 4, 2, mesh.shape["tp"]), ("sp_0", "sp_1", "sp_2", "tp"))
    placed = (
        P(SP_TP, None),
        P(SP, "tp"),
        P(SP, "tp"),
        P(SP, "tp"),
        P(SP, "tp"),
        P(SP, "tp"),
        P(SP, "tp"),
        P("tp"),
        P(),
        P(),
        P(),
        P(),
        P(SP_TP, None),
        P(SP_TP, None),
        P(SP, None, "tp"),
        P(SP, None, "tp"),
        P(SP, "tp", None),
        P(None, "tp"),
        P(None, "tp"),
        P("tp", None),
    )
    return jax.shard_map(
        body, mesh=finer, in_specs=placed, out_specs=P(SP_TP, None), check_vma=False
    )
```

profile of v0, /device:TPU:2, one launch (start us, length us, event | category | flops | bytes accessed | tf_op | source)
XLA Modules:
  0.0 553.1 jit_solution(17728160664577737282)
XLA Ops:
  10.0 13.0 %fusion.178 = f32[8,64,2,64]{3,0,1,2:T(8,128)S(1)} fusion(f32[8,64,2,64]{3,0,1,2:T(8,128)S(1)} %copy.134), kind=kOutput, calls=%fused_computation.308 | output fusion | flops 4128768 | bytes 524288 | tf_op jit(solution)/shard_map/jit(cumsum)/reduce_window_sum | solution.py:118
  36.9 24.3 %while.40 = (s32[]{:T(128)}, f32[2,64,128]{2,1,0:T(8,128)S(1)}, f32[8,64,2,128]{3,1,2,0:T(8,128)}, f32[8,2,64]{2,0,1:T(8,128)S(1)}, f32[8,64,2,64]{3,0,1,2:T(8,1...) while((s32[]{:T(128)}, f32[2,64,128]{2,1,0:T(8,128)S(1)}, ...), condition=%wide.region_2.3_spmd.clone, body=%wide.region_1.2_spmd.clone.sunk | while | flops 4259843 | bytes 494192 | solution.py:139
  63.6 3.1 rev.15
  66.7 3.1 rev.17
  83.2 24.4 %while.42 = (s32[]{:T(128)}, f32[2,64,128]{2,1,0:T(8,128)S(1)}, f32[8,64,2,128]{3,1,2,0:T(8,128)}, f32[8,2,64]{2,0,1:T(8,128)S(1)}, f32[8,64,2,64]{3,0,1,2:T(8,1...) while((s32[]{:T(128)}, f32[2,64,128]{2,1,0:T(8,128)S(1)}, ...), condition=%wide.region_10.11_spmd.clone, body=%wide.region_9.10_spmd.clone.sunk | while | flops 4259843 | bytes 494192 | solution.py:139
  116.6 12.1 %all-gather.6 = bf16[4,129,128]{2,1,0:T(8,128)(2,1)S(1)} all-gather(bf16[1,129,128]{2,1,0:T(8,128)(2,1)S(1)} %maximum_bitcast_fusion.2), channel_id=4, replica_groups=mesh['sp_0'=8,'sp_1'=4,'sp_2'=2,'tp'=4] {'sp_1'}, dimensions={0}, use_global_device_ids=true | all-gather | bytes 165120 | tf_op jit(solution)/shard_map/all_gather | solution.py:28
  129.3 28.6 %all-gather.7 = bf16[8,129,128]{2,1,0:T(8,128)(2,1)S(1)} all-gather(bf16[1,129,128]{2,1,0:T(8,128)(2,1)S(1)} %maximum_bitcast_fusion.3), channel_id=5, replica_groups=mesh['sp_0'=8,'sp_1'=4,'sp_2'=2,'tp'=4] {'sp_0'}, dimensions={0}, use_global_device_ids=true | all-gather | bytes 297216 | tf_op jit(solution)/shard_map/all_gather | solution.py:28
  167.0 3.0 rev.19
  176.4 8.8 %while.41 = (s32[]{:T(128)}, f32[2,64,128]{2,1,0:T(8,128)S(1)}, s32[]{:T(128)}, bf16[64,2,64]{2,1,0:T(2,128)(2,1)S(1)}, bf16[64,2,64,128]{3,2,1,0:T(8,128)(2,1)S(1)}, /*index=5*/s32[]{:T(128)}, s32[]{:T(128)}) while((s32[]{:T(128)}, f32[2,64,128]{2,1,0:T(8,128)S(1)}, s32[]{:T(128)}, bf16[64,2,64]{2,1,0:T(2,128)(2,1)S(1)}, ...), condition=%wide.region_5.6_spmd.clone, body=%wide.region_4.5_spmd.clone.sunk | while | flops 82052 | bytes 165225 | solution.py:60
  188.2 4.4 all-to-all-start
  192.6 6.7 %all-to-all-done = bf16[4,128,256]{2,1,0:T(8,128)(2,1)S(1)} async-done(((bf16[4,128,256]{2,1,0:T(8,128)(2,1)}), bf16[4,128,256]{2,1,0:T(8,128)(2,1)S(1)}, u32[]{:S(2)}, u32[]{:S(2)}) %all-to-all-start) | async-done | bytes 262176 | tf_op jit(solution)/shard_map/all_to_all | solution.py:233
  199.5 3.1 multiply_reduce_fusion.2
  208.3 33.6 %scatter_fusion = bf16[64,6,2048]{2,0,1:T(8,128)(2,1)S(1)} fusion(bf16[64,6,2048]{2,0,1:T(8,128)(2,1)S(1)} %broadcast_in_dim.40, s32[256]{0:T(256)S(1)} %bitcast.315, bf16[256,2048]{1,0:T(8,128)(2,1)} %gather_fusion), kind=kCustom, calls=%fused_computation.2 | custom fusion | bytes 3147776 | tf_op jit(solution)/shard_map/scatter | solution.py:173
  242.8 59.3 %all_to_all.29 = bf16[64,6,2048]{2,1,0:T(8,128)(2,1)S(1)} all-to-all(bf16[64,6,2048]{2,1,0:T(8,128)(2,1)S(1)} %copy.181), channel_id=1, replica_groups=mesh['sp_0'=8,'sp_1'=4,'sp_2'=2,'tp'=4] {'sp_0','sp_1','sp_2'}, dimensions={0} | all-to-all | bytes 3145728 | tf_op jit(solution)/shard_map/all_to_all | solution.py:241
  306.3 4.9 convolution_convert_fusion.1
  311.1 55.2 %all-gather.12.cloned.1.call-done = bf16[1536,2048]{1,0:T(8,128)(2,1)} async-done(((bf16[384,2048]{1,0:T(8,128)(2,1)}), bf16[1536,2048]{1,0:T(8,128)(2,1)}) %all-gather.12.cloned.1.call-update) | async-done | bytes 6291472 | tf_op jit(solution)/shard_map/all_gather | solution.py:245
  366.3 5.1 fusion.32
  373.5 4.5 convolution_convert_fusion
  378.1 7.6 %pad_maximum_fusion = bf16[4,512,2048]{2,1,0:T(8,128)(2,1)} fusion(bf16[4,128,2048]{2,1,0:T(8,128)(2,1)S(1)} %bitcast.316, bf16[4,384,2048]{2,1,0:T(8,128)(2,1)} %convolution_convert_fusion), kind=kLoop, calls=%fused_computation.32 | loop fusion | flops 16777216 | bytes 16777216 | tf_op jit(solution)/shard_map/concatenate | solution.py:261
  385.7 83.9 %reduce-scatter.2.cloned.1.call-done = bf16[512,2048]{1,0:T(8,128)(2,1)} async-done(((bf16[2048,2048]{1,0:T(8,128)(2,1)}), bf16[512,2048]{1,0:T(8,128)(2,1)}) %reduce-scatter.2.cloned.1.call-update) | async-done | bytes 2097168 | tf_op jit(solution)/shard_map/reduce_scatter | solution.py:260
  472.6 10.9 %all-to-all-start.2 = ((bf16[64,6,2048]{2,1,0:T(8,128)(2,1)}), bf16[64,6,2048]{2,1,0:T(8,128)(2,1)}, u32[]{:S(2)}, u32[]{:S(2)}) async-start(bf16[64,6,2048]{2,1,0:T(8,128)(2,1)} %reshape.770), calls=%async_computation.3 | async-start | bytes 4194304 | tf_op jit(solution)/shard_map/all_to_all | solution.py:271
  483.6 51.0 %all-to-all-done.2 = bf16[64,6,2048]{2,1,0:T(8,128)(2,1)} async-done(((bf16[64,6,2048]{2,1,0:T(8,128)(2,1)}), bf16[64,6,2048]{2,1,0:T(8,128)(2,1)}, u32[]{:S(2)}, u32[]{:S(2)}) %all-to-all-start.2) | async-done | bytes 1572896 | tf_op jit(solution)/shard_map/all_to_all | solution.py:271
  534.6 2.6 reshape.771
  542.0 3.2 multiply_reduce_fusion
  (409 shorter events, 137.4 us)
Async XLA Ops:
  6.5 367.0 %copy-start = (bf16[1,256,2048]{2,1,0:T(8,128)(2,1)S(1)}, bf16[1,256,2048]{2,1,0:T(8,128)(2,1)}, u32[]{:S(2)}) copy-start(bf16[1,256,2048]{2,1,0:T(8,128)(2,1)} %param.42) | copy-start | bytes 3145732
  6.5 167.2 %all-gather.16.cloned.1.call-start = ((), (), s32[]{:S(2)}) async-start(), calls=%async_computation.7 | async-start | bytes 2263040 | tf_op jit(solution)/shard_map/all_gather | solution.py:28
  9.2 13.9 %copy-start.21 = (bf16[512,128]{1,0:T(8,128)(2,1)S(1)}, bf16[512,128]{1,0:T(8,128)(2,1)}, u32[]{:S(2)}) copy-start(bf16[512,128]{1,0:T(8,128)(2,1)} %param.27) | copy-start | bytes 393220
  9.2 14.1 %copy-start.22 = (bf16[512,128]{1,0:T(8,128)(2,1)S(1)}, bf16[512,128]{1,0:T(8,128)(2,1)}, u32[]{:S(2)}) copy-start(bf16[512,128]{1,0:T(8,128)(2,1)} %param.28) | copy-start | bytes 393220
  9.6 13.5 %copy-start.7 = (f32[512,128]{0,1:T(8,128)}, f32[512,128]{0,1:T(8,128)S(1)}, u32[]{:S(2)}) copy-start(f32[512,128]{0,1:T(8,128)S(1)} %get-tuple-element.357) | copy-start | bytes 786436
  9.6 60.2 %copy-start.9 = (f32[512,128]{0,1:T(8,128)}, f32[512,128]{0,1:T(8,128)S(1)}, u32[]{:S(2)}) copy-start(f32[512,128]{0,1:T(8,128)S(1)} %get-tuple-element.416) | copy-start | bytes 786436
  23.9 5.2 copy-start.15
  23.9 5.2 copy-start.16
  74.9 4.5 copy-start.12
  82.4 25.3 %copy-start.18 = (bf16[8,64,2,128]{3,2,1,0:T(2,128)(2,1)S(1)}, bf16[8,64,2,128]{3,2,1,0:T(2,128)(2,1)}, u32[]{:S(2)}) copy-start(bf16[8,64,2,128]{3,2,1,0:T(2,128)(2,1)} %reshape_reshape.8) | copy-start | bytes 786436
  83.2 26.8 %copy-start.26 = (s32[128,2]{0,1:T(2,128)S(1)}, s32[128,2]{0,1:T(2,128)}, u32[]{:S(2)}) copy-start(s32[128,2]{0,1:T(2,128)} %param.38) | copy-start | bytes 3076
  162.0 4.0 copy-start.11
  165.0 5.0 copy-start.8
  174.8 12.2 %copy-start.27 = (f32[256]{0:T(256)S(1)}, f32[256]{0:T(256)}, u32[]{:S(2)}) copy-start(f32[256]{0:T(256)} %param.33) | copy-start | bytes 3076
  188.2 11.1 %all-to-all-start = ((bf16[4,128,256]{2,1,0:T(8,128)(2,1)}), bf16[4,128,256]{2,1,0:T(8,128)(2,1)S(1)}, u32[]{:S(2)}, u32[]{:S(2)}) async-start(bf16[4,128,256]{2,1,0:T(8,128)(2,1)} %bitcast.62), calls=%async_computation | async-start | bytes 524288 | tf_op jit(solution)/shard_map/all_to_all | solution.py:233
  192.6 111.1 %all-gather.14.cloned.1.call-start = ((), (), s32[]{:S(2)}) async-start(), calls=%async_computation.5 | async-start | bytes 2621440 | tf_op jit(solution)/shard_map/all_gather | solution.py:246
  204.8 161.6 %all-gather.12.cloned.1.call-start = ((), (), s32[]{:S(2)}) async-start(), calls=%async_computation.4 | async-start | bytes 7864320 | tf_op jit(solution)/shard_map/all_gather | solution.py:245
  303.7 166.0 %reduce-scatter.2.cloned.1.call-start = ((), (), s32[]{:S(2)}) async-start(), calls=%async_computation.6 | async-start | bytes 10485760 | tf_op jit(solution)/shard_map/reduce_scatter | solution.py:260
  311.1 60.3 %copy-start.30 = (bf16[1,2048,256]{2,1,0:T(8,128)(2,1)S(1)}, bf16[1,2048,256]{2,1,0:T(8,128)(2,1)}, u32[]{:S(2)}) copy-start(bf16[1,2048,256]{2,1,0:T(8,128)(2,1)} %param.41) | copy-start | bytes 3145732
  366.3 5.1 copy-start.29
  373.5 4.5 copy-start.3
  472.6 10.9 %copy-start.28 = (f32[128,2]{0,1:T(2,128)S(1)}, f32[128,2]{0,1:T(2,128)}, u32[]{:S(2)}) copy-start(f32[128,2]{0,1:T(2,128)} %param.39) | copy-start | bytes 3076
  472.6 62.0 %all-to-all-start.2 = ((bf16[64,6,2048]{2,1,0:T(8,128)(2,1)}), bf16[64,6,2048]{2,1,0:T(8,128)(2,1)}, u32[]{:S(2)}, u32[]{:S(2)}) async-start(bf16[64,6,2048]{2,1,0:T(8,128)(2,1)} %reshape.770), calls=%async_computation.3 | async-start | bytes 4194304 | tf_op jit(solution)/shard_map/all_to_all | solution.py:271
  542.0 3.5 copy-start.6
  (15 other events, 29.9 us)
Sparse Core Ops, SparseCore 0:
  62.0 79.3 all-gather.15
  204.9 30.5 all-gather.13
  303.8 62.5 all-gather.11
  385.8 83.7 reduce-scatter.1
where the time goes:
time: 557 us; the launch traced here: 553 us
  waiting for transfers between devices  197 us (35%)
  local copies, waits for them, and re-layouts  119 us (21%)
  blocking collectives  102 us (18%)
  matrix products  56.2 us (10%)
  other arithmetic  46.9 us (8%)
  starting transfers between devices  15.3 us (3%)
  between operations  14 us (3%)
    reduce_scatter x1, waiting for transfers between devices, body(): lax.psum_scatter(jnp.concatenate([routed_out, shared_out], axis=1).reshap...  83.9 us
    all_to_all x1, blocking collectives, body(): lax.all_to_all(fill_slots(normed, routes, experts, capacity), SP, split_a...  59.3 us
    all_gather x1, waiting for transfers between devices, body(): lax.all_gather(arrived.reshape(experts * capacity, model_width), 'tp', ax...  55.2 us
    all_to_all x1, waiting for transfers between devices, body(): lax.all_to_all(routed_done, SP, split_axis=0, concat_axis=0, tiled=True)  51 us
    all_gather x3, blocking collectives, gathered_once(): both, at, found = (lax.all_gather(jnp.concatenate(lines), axis), 0, {})  42.6 us
    scatter x2, local copies, waits for them, and re-layouts, fill_slots(): return buffer.at[flat_ids, slot_ids].set(row_data[token_ids])  34.5 us
    dynamic_slice x32, local copies, waits for them, and re-layouts, blockwise(): lax.scan(advance, start_state, (query_in, key_out, value_blocks, block_de...  20.9 us
    dot_general x16, matrix products, advance(): jnp.einsum('jco,jcm->com', key_segment, value_segment)  15.2 us
  transfers between devices with their start and end apart: 6, of which 4 were waited for; matrix products, arithmetic and copies ran while one was open for 21% of the time, Pallas kernels for 0%

commit v1 on v0

v1 whole, which is shorter than its diff:
```python
import functools

import jax
import jax.numpy as jnp
import numpy as np
from jax import lax
from jax.experimental import pallas as pl
from jax.experimental.pallas import tpu as pltpu
from jax.sharding import Mesh
from jax.sharding import PartitionSpec as P

KEY_CHANNELS = 64
DV = 128
BLK = 128
TOPK = 2
CAP = 6
Z, XC, TP = 8, 8, 4
SP = ("sp_0", "sp_1", "sp_2")
PLANE = ("sp_1", "sp_2")
SP_TP = ("sp_0", "sp_1", "sp_2", "tp")
SPAN = 512
TOK = 128
D = 2048
EXPERTS = 64
SLOTS = EXPERTS * CAP
LANES = 128
COLS = D // LANES
MSG = 272

EPS = 1e-06
GATE_NORM = 16.0
ROPE_BASE = 10000.0
F32 = jnp.float32
BF16 = jnp.bfloat16
HIGH = lax.Precision.HIGHEST
NT = (((1,), (1,)), ((), ()))
TN = (((0,), (0,)), ((), ()))
VMEM_LIMIT = 60 * 1024 * 1024


def rope_tables():
    half = KEY_CHANNELS // 2
    frequency = ROPE_BASE ** (-np.arange(half, dtype=np.float64) / half)
    lanes = np.tile(frequency, LANES // half)
    sign = np.tile(np.concatenate([-np.ones(half), np.ones(half)]), LANES // KEY_CHANNELS)
    inner = np.arange(BLK)[:, None] * lanes[None, :]
    local = np.stack([np.cos(inner), np.sin(inner) * sign, np.sin(inner), np.cos(inner) * sign])
    blocks = (np.arange(Z * XC * SPAN // BLK) * BLK)[:, None] * lanes[None, :]
    count = SPAN // BLK
    base = np.concatenate(
        [np.cos(blocks).reshape(-1, count, LANES), np.sin(blocks).reshape(-1, count, LANES)], axis=1
    )
    return local.astype(np.float32), base.astype(np.float32)


def dot(a, b, dims=(((1,), (0,)), ((), ())), precision=None):
    return lax.dot_general(a, b, dims, precision=precision, preferred_element_type=F32)


def iota(shape, axis):
    return lax.broadcasted_iota(jnp.int32, shape, axis)


def log_sigmoid(x):
    return jnp.minimum(x, 0.0) - jnp.log1p(jnp.exp(-jnp.abs(x)))


def spread(state, low):
    return jnp.concatenate([jnp.where(low, state, 0.0), jnp.where(low, 0.0, state)], axis=0)


def split_rows(rows):
    pieces = []
    for row in rows:
        high = row.astype(BF16)
        pieces += [high.astype(F32), row - high.astype(F32)]
    row_id = iota((16, LANES), 0)
    out = jnp.zeros((16, LANES), F32)
    for i, piece in enumerate(pieces):
        out = jnp.where(row_id == i, piece, out)
    return out


def attention_kernel(
    q_ref, k_ref, v_ref, fd_ref, bd_ref, local_ref, base_ref, routes_ref,
    part_ref, qdev_ref, msg_ref, slots_ref, within_ref, qin_ref,
):
    count = SPAN // BLK
    lane = iota((BLK, LANES), 1)
    low = lane < KEY_CHANNELS
    front = lane % KEY_CHANNELS < KEY_CHANNELS // 2
    row, col = iota((BLK, BLK), 0), iota((BLK, BLK), 1)
    tri_f = (row >= col).astype(F32)
    tri_b = (row <= col).astype(F32)
    row2, col2 = iota((BLK, 2 * BLK), 0), iota((BLK, 2 * BLK), 1) % BLK
    wide_low = iota((BLK, 2 * DV), 1) < DV

    def rotate(u, cosine, signed_sine):
        swapped = jnp.where(
            front,
            pltpu.roll(u, LANES - KEY_CHANNELS // 2, 1),
            pltpu.roll(u, KEY_CHANNELS // 2, 1),
        )
        return u * cosine + swapped * signed_sine

    updates_f, updates_b, last_f, last_b = [], [], [], []
    for n in range(count):
        rows = pl.ds(n * BLK, BLK)
        base_cos = base_ref[n : n + 1, :]
        base_sin = base_ref[count + n : count + n + 1, :]
        cosine = base_cos * local_ref[0] - base_sin * local_ref[2]
        signed_sine = base_sin * local_ref[3] + base_cos * local_ref[1]
        q = rotate(q_ref[rows, :].astype(F32) * KEY_CHANNELS ** (-0.5), cosine, signed_sine)
        k = rotate(k_ref[rows, :].astype(F32), cosine, signed_sine)
        v = v_ref[rows, :].astype(F32)
        v_bd = jnp.concatenate(
            [jnp.where(wide_low, v, 0.0), jnp.where(wide_low, 0.0, v)], axis=0
        ).astype(BF16)
        scores = jnp.zeros((BLK, 2 * BLK), F32)
        for forward in (True, False):
            log = log_sigmoid((fd_ref if forward else bd_ref)[rows, :]) * (1.0 / GATE_NORM)
            cumul = dot(tri_f if forward else tri_b, log, precision=HIGH)
            middle = cumul[BLK // 2 - 1 : BLK // 2, :] if forward else cumul[BLK // 2 : BLK // 2 + 1, :]
            total = cumul[BLK - 1 : BLK, :] if forward else cumul[0:1, :]
            offset = cumul - middle
            q_scaled = q * jnp.exp(offset)
            k_scaled = k * jnp.exp(-offset)
            q_in = q_scaled * jnp.exp(middle)
            k_out = k_scaled * jnp.exp(total - middle)
            both = dot(q_scaled.astype(BF16), spread(k_scaled, low).astype(BF16), NT)
            reach = row2 >= col2 if forward else row2 <= col2
            scores = scores + jnp.where(reach, both, 0.0)
            product = dot(v.astype(BF16), k_out.astype(BF16), TN)
            update = jnp.where(low, product[:DV], product[DV:])
            (updates_f if forward else updates_b).append(update)
            (last_f if forward else last_b).append(total)
            qin_ref[rows, pl.ds(0 if forward else LANES, LANES)] = q_in
        within_ref[rows, :] = dot(scores.astype(BF16), v_bd)

    zero_row = jnp.zeros((1, LANES), F32)
    states_f, states_b = [jnp.zeros((DV, LANES), F32)], [jnp.zeros((DV, LANES), F32)]
    sums_f, sums_b = [zero_row], [zero_row]
    for n in range(count):
        states_f.append(states_f[-1] * jnp.exp(last_f[n]) + updates_f[n])
        sums_f.append(sums_f[-1] + last_f[n])
        m = count - 1 - n
        states_b.append(states_b[-1] * jnp.exp(last_b[m]) + updates_b[m])
        sums_b.append(sums_b[-1] + last_b[m])
    for n in range(count):
        m = count - 1 - n
        rows = pl.ds(n * BLK, BLK)
        q_in = qin_ref[rows, :]
        carried = jnp.concatenate([spread(states_f[n], low), spread(states_b[m], low)], axis=1)
        part_ref[rows, :] = within_ref[rows, :] + dot(q_in.astype(BF16), carried.astype(BF16), NT)
        reach = jnp.exp(jnp.concatenate([sums_f[n], sums_b[m]], axis=1))
        qdev_ref[rows, :] = (q_in * reach).astype(BF16)
    final_f, final_b = states_f[count].astype(BF16), states_b[count].astype(BF16)
    sums = split_rows([sums_f[count], sums_b[count]]).astype(BF16)
    for j in range(XC):
        msg_ref[j, pl.ds(0, DV), :] = final_f
        msg_ref[j, pl.ds(DV, DV), :] = final_b
        msg_ref[j, pl.ds(2 * DV, 16), :] = sums

    expert = iota((TOK, EXPERTS), 1)
    picks = [routes_ref[:, k : k + 1] == expert for k in range(TOPK)]
    chosen = jnp.zeros((TOK, EXPERTS), F32)
    for pick in picks:
        chosen = chosen + pick.astype(F32)
    strict = (row > col).astype(BF16)
    before = dot(strict, chosen.astype(BF16))
    place = before + (CAP * expert).astype(F32)
    column = iota((TOK, TOPK), 1)
    slots = jnp.zeros((TOK, TOPK), F32)
    for k, pick in enumerate(picks):
        found = jnp.sum(jnp.where(pick, place, 0.0), axis=1, keepdims=True)
        slots = jnp.where(column == k, found, slots)
    slots_ref[...] = slots.astype(jnp.int32)


def compose_gathered(own, gathered_ref, length):
    results = []
    for forward in (True, False):
        start, at = (0, 2 * DV) if forward else (DV, 2 * DV + 2)
        state, logs = jnp.zeros((DV, LANES), F32), jnp.zeros((1, LANES), F32)
        inner, inner_logs = state, logs
        for step in range(length):
            k = step if forward else length - 1 - step
            here = own == k
            inner = jnp.where(here, state, inner)
            inner_logs = jnp.where(here, logs, inner_logs)
            tail = gathered_ref[k, pl.ds(2 * DV, 16), :].astype(F32)
            first = at - 2 * DV
            log = tail[first : first + 1, :] + tail[first + 1 : first + 2, :]
            state = state * jnp.exp(log) + gathered_ref[k, pl.ds(start, DV), :].astype(F32)
            logs = logs + log
        results.append((state, logs, inner, inner_logs))
    return results


def plane_kernel(own_ref, gathered_ref, inner_ref, logs_ref, msg_ref):
    forward, backward = compose_gathered(own_ref[0], gathered_ref, XC)
    inner_ref[0] = forward[2]
    inner_ref[1] = backward[2]
    row_id = iota((8, LANES), 0)
    logs_ref[...] = jnp.where(row_id == 0, forward[3], jnp.where(row_id == 1, backward[3], 0.0))
    total_f, total_b = forward[0].astype(BF16), backward[0].astype(BF16)
    sums = split_rows([forward[1], backward[1]]).astype(BF16)
    for j in range(Z):
        msg_ref[j, pl.ds(0, DV), :] = total_f
        msg_ref[j, pl.ds(DV, DV), :] = total_b
        msg_ref[j, pl.ds(2 * DV, 16), :] = sums


def readout_kernel(
    own_ref, gathered_ref, inner_ref, logs_ref, part_ref, qdev_ref, gate_ref, gain_ref, out_ref
):
    forward, backward = compose_gathered(own_ref[0], gathered_ref, Z)
    low = iota((DV, LANES), 1) < KEY_CHANNELS
    carry_f = inner_ref[0] + forward[2] * jnp.exp(logs_ref[0:1, :])
    carry_b = inner_ref[1] + backward[2] * jnp.exp(logs_ref[1:2, :])
    carried = jnp.concatenate([spread(carry_f, low), spread(carry_b, low)], axis=1).astype(BF16)
    for n in range(TP):
        rows = pl.ds(n * TOK, TOK)
        attended = part_ref[rows, :] + dot(qdev_ref[rows, :], carried, NT)
        heads = []
        for h in range(2):
            head = attended[:, h * DV : (h + 1) * DV]
            heads.append(head * lax.rsqrt(jnp.mean(head * head, axis=-1, keepdims=True) + EPS))
        gate = gate_ref[rows, :].astype(F32)
        mixed = jnp.concatenate(heads, axis=1) * gain_ref[...] * (gate * jax.nn.sigmoid(gate))
        out_ref[n] = mixed.astype(BF16)


def normalize(x):
    return x * lax.rsqrt(jnp.mean(x * x, axis=-1, keepdims=True) + EPS)


def project_kernel(
    slots_ref, mixed_ref, weight_ref, stream_ref, mix_ref, ffn_ref,
    residual_ref, normed_ref, sent_ref, acc_ref, rows_ref,
):
    step = pl.program_id(0)
    product = dot(mixed_ref[0], weight_ref[...])

    @pl.when(step == 0)
    def _():
        acc_ref[...] = product
        sent_ref[...] = jnp.zeros_like(sent_ref)

    @pl.when(step > 0)
    def _():
        acc_ref[...] += product

    @pl.when(step == TP - 1)
    def _():
        projected = normalize(acc_ref[...]) * mix_ref[...]
        residual = (stream_ref[...].astype(F32) + projected).astype(BF16)
        residual_ref[...] = residual
        normed = (normalize(residual.astype(F32)) * ffn_ref[...]).astype(BF16)
        normed_ref[...] = normed
        wide = normed.astype(F32)
        for j in range(COLS):
            rows_ref[pl.ds(j, TOK, stride=COLS), :] = wide[:, j * LANES : (j + 1) * LANES]

        def place(t, carry):
            line = rows_ref[pl.ds(pl.multiple_of(t * COLS, COLS), COLS), :].astype(BF16)
            for k in range(TOPK):
                sent_ref[slots_ref[t * TOPK + k]] = line
            return carry

        lax.fori_loop(0, TOK, place, 0, unroll=8)


def hidden_of(rows, gate, up):
    a = dot(rows, gate)
    return (a * jax.nn.sigmoid(a) * dot(rows, up)).astype(BF16)


def expert_kernel(sent_ref, gate_ref, up_ref, down_ref, out_ref, lines_ref, rows_ref, acc_ref):
    step = pl.program_id(0)

    @pl.when(step == 0)
    def _():
        lines_ref[...] = sent_ref[...].astype(F32)
        for j in range(COLS):
            rows_ref[:, j * LANES : (j + 1) * LANES] = lines_ref[
                pl.ds(j, SLOTS, stride=COLS), :
            ].astype(BF16)

    product = dot(hidden_of(rows_ref[...], gate_ref[0], up_ref[0]), down_ref[0])

    @pl.when(step == 0)
    def _():
        acc_ref[...] = product

    @pl.when(step > 0)
    def _():
        acc_ref[...] += product

    @pl.when(step == TP - 1)
    def _():
        for j in range(COLS):
            lines_ref[pl.ds(j, SLOTS, stride=COLS), :] = acc_ref[:, j * LANES : (j + 1) * LANES]
        out_ref[...] = lines_ref[...].astype(BF16)


def shared_kernel(rows_ref, gate_ref, up_ref, down_ref, out_ref):
    step = pl.program_id(0)
    product = dot(hidden_of(rows_ref[...], gate_ref[0], up_ref[0]), down_ref[0])

    @pl.when(step == 0)
    def _():
        out_ref[...] = product

    @pl.when(step > 0)
    def _():
        out_ref[...] += product


def combine_kernel(
    slots_ref, weights_ref, back_ref, shared_ref, residual_ref, gain_ref, out_ref, lines_ref, mix_ref
):
    def gather(t, carry):
        line = jnp.zeros((COLS, LANES), F32)
        for k in range(TOPK):
            at = t * TOPK + k
            line = line + back_ref[slots_ref[at]].astype(F32) * weights_ref[at]
        lines_ref[pl.ds(pl.multiple_of(t * COLS, COLS), COLS), :] = line
        return carry

    lax.fori_loop(0, TOK, gather, 0, unroll=8)
    for j in range(COLS):
        columns = slice(j * LANES, (j + 1) * LANES)
        mix_ref[:, columns] = shared_ref[:, columns] + lines_ref[pl.ds(j, TOK, stride=COLS), :]
    out_ref[...] = (
        residual_ref[...].astype(F32) + normalize(mix_ref[...]) * gain_ref[...]
    ).astype(BF16)


def vmem():
    return pl.BlockSpec(memory_space=pltpu.VMEM)


def smem():
    return pl.BlockSpec(memory_space=pltpu.SMEM)


def params(**extra):
    return pltpu.CompilerParams(vmem_limit_bytes=VMEM_LIMIT, **extra)


def shape(dims, kind):
    return jax.ShapeDtypeStruct(dims, kind)


def cost(flops, moved):
    return pl.CostEstimate(flops=flops, bytes_accessed=moved, transcendentals=0)


def whole(dims):
    return pl.BlockSpec(dims, lambda i, *_: (0,) * len(dims))


def body(
    stream,
    queries,
    key_rows,
    values,
    out_gate,
    fwd_decay,
    bwd_decay,
    head_gain,
    out_proj,
    mix_gain,
    ffn_gain,
    moe_gain,
    routes,
    route_weight,
    expert_gate,
    expert_up,
    expert_down,
    shared_gate,
    shared_up,
    shared_down,
):
    gates = lax.all_gather(expert_gate[0], "tp", axis=0)
    ups = lax.all_gather(expert_up[0], "tp", axis=0)
    downs = lax.all_gather(expert_down[0], "tp", axis=0)
    shared_gates = lax.all_gather(shared_gate, "tp", axis=0)
    shared_ups = lax.all_gather(shared_up, "tp", axis=0)
    shared_downs = lax.all_gather(shared_down, "tp", axis=0)

    local, base = rope_tables()
    base_here = lax.dynamic_index_in_dim(jnp.asarray(base), lax.axis_index(SP), 0, keepdims=False)
    part, qdev, msg, slots = pl.pallas_call(
        attention_kernel,
        out_shape=(
            shape((SPAN, 2 * DV), F32),
            shape((SPAN, 2 * LANES), BF16),
            shape((XC, MSG, LANES), BF16),
            shape((TOK, TOPK), jnp.int32),
        ),
        in_specs=[vmem()] * 8,
        out_specs=(vmem(),) * 4,
        scratch_shapes=[pltpu.VMEM((SPAN, 2 * DV), F32), pltpu.VMEM((SPAN, 2 * LANES), F32)],
        compiler_params=params(),
        cost_estimate=cost(600_000_000, 4_000_000),
        name="attention",
    )(queries, key_rows, values, fwd_decay, bwd_decay, jnp.asarray(local), base_here, routes)
    flat_slots = slots.reshape(-1)

    in_plane = lax.all_to_all(msg, PLANE, split_axis=0, concat_axis=0, tiled=True)
    inner, logs, msg = pl.pallas_call(
        plane_kernel,
        out_shape=(
            shape((2, DV, LANES), F32),
            shape((8, LANES), F32),
            shape((Z, MSG, LANES), BF16),
        ),
        in_specs=[smem(), vmem()],
        out_specs=(vmem(),) * 3,
        compiler_params=params(),
        cost_estimate=cost(10_000_000, 1_000_000),
        name="plane",
    )(lax.axis_index(PLANE).astype(jnp.int32).reshape(1), in_plane)
    planes = lax.all_to_all(msg, "sp_0", split_axis=0, concat_axis=0, tiled=True)
    mixed = pl.pallas_call(
        readout_kernel,
        out_shape=shape((TP, TOK, 2 * DV), BF16),
        in_specs=[smem()] + [vmem()] * 7,
        out_specs=vmem(),
        compiler_params=params(),
        cost_estimate=cost(100_000_000, 3_000_000),
        name="readout",
    )(
        lax.axis_index("sp_0").astype(jnp.int32).reshape(1),
        planes, inner, logs, part, qdev, out_gate, head_gain.reshape(1, -1),
    )
    mixed = lax.all_to_all(mixed, "tp", split_axis=0, concat_axis=0, tiled=True)

    residual, normed, sent = pl.pallas_call(
        project_kernel,
        grid=(TP,),
        out_shape=(
            shape((TOK, D), BF16),
            shape((TOK, D), BF16),
            shape((SLOTS, COLS, LANES), BF16),
        ),
        in_specs=[
            smem(),
            pl.BlockSpec((1, TOK, 2 * DV), lambda i: (i, 0, 0)),
            pl.BlockSpec((2 * DV, D), lambda i: (i, 0)),
            whole((TOK, D)),
            whole((1, D)),
            whole((1, D)),
        ],
        out_specs=(whole((TOK, D)), whole((TOK, D)), whole((SLOTS, COLS, LANES))),
        scratch_shapes=[pltpu.VMEM((TOK, D), F32), pltpu.VMEM((TOK * COLS, LANES), F32)],
        compiler_params=params(dimension_semantics=("arbitrary",)),
        cost_estimate=cost(600_000_000, 8_000_000),
        name="project",
    )(flat_slots, mixed, out_proj, stream, mix_gain.reshape(1, -1), ffn_gain.reshape(1, -1))

    arrived = lax.all_to_all(
        sent.reshape(EXPERTS, CAP * COLS, LANES), SP, split_axis=0, concat_axis=0, tiled=True
    )
    width = gates.shape[-1]
    done = pl.pallas_call(
        expert_kernel,
        grid=(TP,),
        out_shape=shape((SLOTS * COLS, LANES), BF16),
        in_specs=[
            whole((SLOTS * COLS, LANES)),
            pl.BlockSpec((1, D, width), lambda i: (i, 0, 0)),
            pl.BlockSpec((1, D, width), lambda i: (i, 0, 0)),
            pl.BlockSpec((1, width, D), lambda i: (i, 0, 0)),
        ],
        out_specs=whole((SLOTS * COLS, LANES)),
        scratch_shapes=[
            pltpu.VMEM((SLOTS * COLS, LANES), F32),
            pltpu.VMEM((SLOTS, D), BF16),
            pltpu.VMEM((SLOTS, D), F32),
        ],
        compiler_params=params(dimension_semantics=("arbitrary",)),
        cost_estimate=cost(4_900_000_000, 16_000_000),
        name="experts",
    )(arrived.reshape(SLOTS * COLS, LANES), gates, ups, downs)
    back = lax.all_to_all(
        done.reshape(EXPERTS, CAP * COLS, LANES), SP, split_axis=0, concat_axis=0, tiled=True
    )
    shared_width = shared_gates.shape[-1]
    shared = pl.pallas_call(
        shared_kernel,
        grid=(TP,),
        out_shape=shape((TOK, D), F32),
        in_specs=[
            whole((TOK, D)),
            pl.BlockSpec((1, D, shared_width), lambda i: (i, 0, 0)),
            pl.BlockSpec((1, D, shared_width), lambda i: (i, 0, 0)),
            pl.BlockSpec((1, shared_width, D), lambda i: (i, 0, 0)),
        ],
        out_specs=whole((TOK, D)),
        compiler_params=params(dimension_semantics=("arbitrary",)),
        cost_estimate=cost(800_000_000, 8_000_000),
        name="shared",
    )(normed, shared_gates, shared_ups, shared_downs)
    return pl.pallas_call(
        combine_kernel,
        out_shape=shape((TOK, D), BF16),
        in_specs=[smem(), smem()] + [vmem()] * 4,
        out_specs=vmem(),
        scratch_shapes=[pltpu.VMEM((TOK * COLS, LANES), F32), pltpu.VMEM((TOK, D), F32)],
        compiler_params=params(),
        cost_estimate=cost(5_000_000, 4_000_000),
        name="combine",
    )(
        flat_slots, route_weight.reshape(-1), back.reshape(SLOTS, COLS, LANES),
        shared, residual, moe_gain.reshape(1, -1),
    )


def solution(mesh):
    finer = Mesh(mesh.devices.reshape(8, 4, 2, mesh.shape["tp"]), ("sp_0", "sp_1", "sp_2", "tp"))
    placed = (
        P(SP_TP, None),
        P(SP, "tp"),
        P(SP, "tp"),
        P(SP, "tp"),
        P(SP, "tp"),
        P(SP, "tp"),
        P(SP, "tp"),
        P("tp"),
        P(),
        P(),
        P(),
        P(),
        P(SP_TP, None),
        P(SP_TP, None),
        P(SP, None, "tp"),
        P(SP, None, "tp"),
        P(SP, "tp", None),
        P(None, "tp"),
        P(None, "tp"),
        P("tp", None),
    )
    return jax.shard_map(
        body, mesh=finer, in_specs=placed, out_specs=P(SP_TP, None), check_vma=False
    )
```

time: 557 us -> 294 us (0.53)
  local copies, waits for them, and re-layouts: 119 us -> 5.38 us
  blocking collectives: 102 us -> 41.3 us
  matrix products: 56.2 us -> 0 us
  other arithmetic: 46.9 us -> 0 us
  Pallas kernels: 0 us -> 40.9 us
  waiting for transfers between devices: 197 us -> 171 us
    reduce_scatter x1 -> x0, waiting for transfers between devices: 83.9 us -> none  [body(): lax.psum_scatter(jnp.concatenate([routed_out, shared_out], axis=1).reshap...]
    all_gather x3 -> x6, waiting for transfers between devices: 55.2 us -> 122 us  [the longest x1 42.3 us: body(): downs = lax.all_gather(expert_down[0], 'tp', axis=0)]
    dot_general x42 -> x0, matrix products: 56.2 us -> none  [the longest x16 15.2 us: advance(): jnp.einsum('jco,jcm->com', key_segment, value_segment)]
    all_gather x3 -> x0, blocking collectives: 42.6 us -> none  [gathered_once(): both, at, found = (lax.all_gather(jnp.concatenate(lines), axis), 0, {})]
    pallas_call x0 -> x7, Pallas kernels: none -> 40.9 us  [the longest x1 14.3 us: body(): pl.pallas_call(expert_kernel, grid=(TP,), out_shape=shape((SLOTS * COLS,...]
    scatter x2 -> x0, local copies, waits for them, and re-layouts: 34.5 us -> none  [fill_slots(): return buffer.at[flat_ids, slot_ids].set(row_data[token_ids])]
    dynamic_slice x32 -> x0, local copies, waits for them, and re-layouts: 20.9 us -> none  [blockwise(): lax.scan(advance, start_state, (query_in, key_out, value_blocks, block_de...]
    another operation x9 -> x0, other arithmetic: 19.7 us -> none  [the longest x2 14.1 us: blockwise(): jnp.cumsum(log_decay.reshape(block_count, BLK, head_count, key_width), ax...]
  transfers between devices with their start and end apart: 6 -> 9, of which waited for: 4 -> 6; matrix products, arithmetic and copies ran while one was open for 21% -> 1% of each run, Pallas kernels for 0% -> 13%
where the time goes in v1:
time: 294 us; the launch traced here: 293 us
  waiting for transfers between devices  171 us (58%)
  blocking collectives  41.3 us (14%)
  Pallas kernels  40.9 us (14%)
  starting transfers between devices  20.8 us (7%)
  between operations  13.5 us (5%)
  local copies, waits for them, and re-layouts  5.38 us (2%)
    all_gather x1, waiting for transfers between devices, body(): downs = lax.all_gather(expert_down[0], 'tp', axis=0)  42.3 us
    all_to_all x1, waiting for transfers between devices, body(): lax.all_to_all(sent.reshape(EXPERTS, CAP * COLS, LANES), SP, split_axis=0...  39.5 us
    all_gather x1, waiting for transfers between devices, body(): shared_downs = lax.all_gather(shared_down, 'tp', axis=0)  35.1 us
    all_gather x1, waiting for transfers between devices, body(): shared_ups = lax.all_gather(shared_up, 'tp', axis=0)  35.1 us
    all_to_all x1, blocking collectives, body(): lax.all_to_all(msg, 'sp_0', split_axis=0, concat_axis=0, tiled=True)  25.7 us
    all_to_all x1, blocking collectives, body(): lax.all_to_all(msg, PLANE, split_axis=0, concat_axis=0, tiled=True)  15.7 us
    pallas_call x1, Pallas kernels, body(): pl.pallas_call(expert_kernel, grid=(TP,), out_shape=shape((SLOTS * COLS,...  14.3 us
    all_to_all x1, starting transfers between devices, body(): lax.all_to_all(done.reshape(EXPERTS, CAP * COLS, LANES), SP, split_axis=0...  10.7 us
  transfers between devices with their start and end apart: 9, of which 6 were waited for; matrix products, arithmetic and copies ran while one was open for 1% of the time, Pallas kernels for 13%

profile of v1, /device:TPU:2, one launch (start us, length us, event | category | flops | bytes accessed | tf_op | source)
XLA Modules:
  0.0 292.5 jit_solution(9433183582984118191)
XLA Ops:
  6.5 0.7 all-gather.10.cloned.1.call-update
  7.3 0.7 all-gather.12.cloned.1.call-update
  9.3 0.7 copy.26.routes_ref
  10.1 1.3 dynamic-slice_bitcast_fusion.base_ref
  11.4 4.7 %attention.1 = (f32[512,256]{1,0:T(8,128)}, bf16[512,256]{1,0:T(8,128)(2,1)}, bf16[8,272,128]{2,1,0:T(8,128)(2,1)}, s32[128,2]{1,0:T(8,128)}) custom-call(bf16[512,128]{1,0:T(8,128)(2,1)} %q_ref.1, bf16[512,128]{1,0:T(8,128)(2,1)} %k_ref.1, bf16[512,256]{1,0:T(8,128)(2,1)} %v_ref.1, f32[512,128]{1,0:T(8,128)} %fd_ref.1, f32[512,128]{1,0:T(8,128)} %bd_ref.1, ...), custom_call_target="tpu_custom_call" | custom-call | flops 600000000 | bytes 4000000 | tf_op jit(solution)/shard_map/attention/pallas_call | solution.py:395
  16.1 15.7 %all_to_all.25.gathered_ref = bf16[8,272,128]{2,1,0:T(8,128)(2,1)} all-to-all(bf16[8,272,128]{2,1,0:T(8,128)(2,1)} %get-tuple-element.16), channel_id=1, replica_groups=mesh['sp_0'=8,'sp_1'=4,'sp_2'=2,'tp'=4] {'sp_1','sp_2'}, dimensions={0} | all-to-all | bytes 1114112 | tf_op jit(solution)/shard_map/all_to_all | solution.py:412
  31.7 2.1 plane.1
  33.8 25.7 %all_to_all.26.gathered_ref = bf16[8,272,128]{2,1,0:T(8,128)(2,1)} all-to-all(bf16[8,272,128]{2,1,0:T(8,128)(2,1)} %get-tuple-element.17), channel_id=1, replica_groups=mesh['sp_0'=8,'sp_1'=4,'sp_2'=2,'tp'=4] {'sp_0'}, dimensions={0} | all-to-all | bytes 1114112 | tf_op jit(solution)/shard_map/all_to_all | solution.py:426
  59.5 2.7 readout.1
  62.2 4.3 %all-to-all-start.2 = ((bf16[4,128,256]{2,1,0:T(8,128)(2,1)}), bf16[4,128,256]{2,1,0:T(8,128)(2,1)S(1)}, u32[]{:S(2)}, u32[]{:S(2)}) async-start(bf16[4,128,256]{2,1,0:T(8,128)(2,1)} %readout.1), calls=%async_computation.2 | async-start | bytes 524288 | tf_op jit(solution)/shard_map/all_to_all | solution.py:439
  67.7 5.4 %all-to-all-done.2.mixed_ref = bf16[4,128,256]{2,1,0:T(8,128)(2,1)S(1)} async-done(((bf16[4,128,256]{2,1,0:T(8,128)(2,1)}), bf16[4,128,256]{2,1,0:T(8,128)(2,1)S(1)}, u32[]{:S(2)}, u32[]{:S(2)}) %all-to-all-start.2) | async-done | bytes 262176 | tf_op jit(solution)/shard_map/all_to_all | solution.py:439
  73.9 6.9 %project.1 = (bf16[128,2048]{1,0:T(8,128)(2,1)}, bf16[128,2048]{1,0:T(8,128)(2,1)}, bf16[384,16,128]{2,1,0:T(8,128)(2,1)}) custom-call(s32[256]{0:T(256)} %reshape.36.slots_ref, bf16[4,128,256]{2,1,0:T(8,128)(2,1)} %copy-done.2, bf16[1024,2048]{1,0:T(8,128)(2,1)} %weight_ref.1, bf16[128,2048]{1,0:T(8,128)(2,1)} %stream_ref.1, f32[1,2048]{1,0:T(1,128)} %bitcast.22, ...), custom_call_target="tpu_custom_call" | custom-call | flops 600000000 | bytes 8000000 | tf_op jit(solution)/shard_map/project/pallas_call | solution.py:441
  80.8 5.6 %all-to-all-start.3 = ((bf16[64,96,128]{2,1,0:T(8,128)(2,1)}), bf16[64,96,128]{2,1,0:T(8,128)(2,1)S(1)}, u32[]{:S(2)}, u32[]{:S(2)}) async-start(bf16[64,96,128]{2,1,0:T(8,128)(2,1)} %bitcast.21), calls=%async_computation.3 | async-start | bytes 3145728 | tf_op jit(solution)/shard_map/all_to_all | solution.py:464
  87.0 39.5 %all-to-all-done.3 = bf16[64,96,128]{2,1,0:T(8,128)(2,1)S(1)} async-done(((bf16[64,96,128]{2,1,0:T(8,128)(2,1)}), bf16[64,96,128]{2,1,0:T(8,128)(2,1)S(1)}, u32[]{:S(2)}, u32[]{:S(2)}) %all-to-all-start.3) | async-done | bytes 1572896 | tf_op jit(solution)/shard_map/all_to_all | solution.py:464
  126.5 42.3 %all-gather.14.cloned.1.call-done.down_ref = bf16[4,256,2048]{2,1,0:T(8,128)(2,1)} async-done(((bf16[1,256,2048]{2,1,0:T(8,128)(2,1)}), bf16[4,256,2048]{2,1,0:T(8,128)(2,1)}) %all-gather.14.cloned.1.call-update) | async-done | bytes 4194320 | tf_op jit(solution)/shard_map/all_gather | solution.py:388
  168.8 14.3 %experts.1 = bf16[6144,128]{1,0:T(8,128)(2,1)} custom-call(bf16[6144,128]{1,0:T(8,128)(2,1)} %bitcast.19, bf16[4,2048,256]{2,1,0:T(8,128)(2,1)} %all-gather.10.cloned.1.call-done.gate_ref, bf16[4,2048,256]{2,1,0:T(8,128)(2,1)} %all-gather.12.cloned.1.call-done.up_ref, bf16[4,256,2048]{2,1,0:T(8,128)(2,1)} %all-gather.14.cloned.1.call-done.down_ref), custom_call_target="tpu_custom_call" | custom-call | flops 4899999744 | bytes 16000000 | tf_op jit(solution)/shard_map/experts/pallas_call | solution.py:468
  183.2 10.7 %all-to-all-start.4 = ((bf16[64,96,128]{2,1,0:T(8,128)(2,1)}), bf16[64,96,128]{2,1,0:T(8,128)(2,1)S(1)}, u32[]{:S(2)}, u32[]{:S(2)}) async-start(bf16[64,96,128]{2,1,0:T(8,128)(2,1)} %bitcast.20), calls=%async_computation.4 | async-start | bytes 3145728 | tf_op jit(solution)/shard_map/all_to_all | solution.py:488
  194.0 0.7 reshape.37.weights_ref
  194.7 9.5 %all-gather.16.cloned.1.call-done = bf16[8192,128]{1,0:T(8,128)(2,1)} async-done(((bf16[2048,128]{1,0:T(8,128)(2,1)}), bf16[8192,128]{1,0:T(8,128)(2,1)}) %all-gather.16.cloned.1.call-update) | async-done | bytes 2097168 | tf_op jit(solution)/shard_map/all_gather | solution.py:389
  204.2 35.1 %all-gather.18.cloned.1.call-done = bf16[8192,128]{1,0:T(8,128)(2,1)} async-done(((bf16[2048,128]{1,0:T(8,128)(2,1)}), bf16[8192,128]{1,0:T(8,128)(2,1)}) %all-gather.18.cloned.1.call-update) | async-done | bytes 2097168 | tf_op jit(solution)/shard_map/all_gather | solution.py:390
  239.3 35.1 %all-gather.20.cloned.1.call-done = bf16[512,2048]{1,0:T(8,128)(2,1)} async-done(((bf16[128,2048]{1,0:T(8,128)(2,1)}), bf16[512,2048]{1,0:T(8,128)(2,1)}) %all-gather.20.cloned.1.call-update) | async-done | bytes 2097168 | tf_op jit(solution)/shard_map/all_gather | solution.py:391
  274.4 6.4 %shared.1.shared_ref = f32[128,2048]{1,0:T(8,128)} custom-call(bf16[128,2048]{1,0:T(8,128)(2,1)} %get-tuple-element.23.rows_ref, bf16[4,2048,128]{2,1,0:T(8,128)(2,1)} %bitcast.16, bf16[4,2048,128]{2,1,0:T(8,128)(2,1)} %bitcast.17, bf16[4,128,2048]{2,1,0:T(8,128)(2,1)} %bitcast.18), custom_call_target="tpu_custom_call" | custom-call | flops 800000000 | bytes 8000000 | tf_op jit(solution)/shard_map/shared/pallas_call | solution.py:492
  280.8 1.2 copy-done
  282.0 3.7 %combine.1 = bf16[128,2048]{1,0:T(8,128)(2,1)} custom-call(s32[256]{0:T(256)} %reshape.36.slots_ref, f32[256]{0:T(256)} %reshape.37.weights_ref, bf16[384,16,128]{2,1,0:T(8,128)(2,1)} %bitcast.15, f32[128,2048]{1,0:T(8,128)} %shared.1.shared_ref, bf16[128,2048]{1,0:T(8,128)(2,1)} %get-tuple-element.24.residual_ref, f32[1,2048]{1,0:T(1,128)} %bitcast.24), custom_call_target="tpu_custom_call" | custom-call | flops 5000000 | bytes 4000000 | tf_op jit(solution)/shard_map/combine/pallas_call | solution.py:507
  (26 shorter events, 3.9 us)
Async XLA Ops:
  6.5 2.8 copy-start.4
  6.5 120.0 %all-gather.10.cloned.1.call-start = ((), (), s32[]{:S(2)}) async-start(), calls=%async_computation.5 | async-start | bytes 5242880 | tf_op jit(solution)/shard_map/all_gather | solution.py:386
  7.3 119.2 %all-gather.12.cloned.1.call-start = ((), (), s32[]{:S(2)}) async-start(), calls=%async_computation.6 | async-start | bytes 5242880 | tf_op jit(solution)/shard_map/all_gather | solution.py:387
  8.0 160.8 %all-gather.14.cloned.1.call-start = ((), (), s32[]{:S(2)}) async-start(), calls=%async_computation.7 | async-start | bytes 5242880 | tf_op jit(solution)/shard_map/all_gather | solution.py:388
  8.7 195.5 %all-gather.16.cloned.1.call-start = ((), (), s32[]{:S(2)}) async-start(), calls=%async_computation.8 | async-start | bytes 2621440 | tf_op jit(solution)/shard_map/all_gather | solution.py:389
  33.8 33.3 %copy-start.3 = (s32[128,2]{1,0:T(8,128)S(1)}, s32[128,2]{1,0:T(8,128)}, u32[]{:S(2)}) copy-start(s32[128,2]{1,0:T(8,128)} %get-tuple-element.15) | copy-start | bytes 3076
  62.2 11.0 %all-to-all-start.2 = ((bf16[4,128,256]{2,1,0:T(8,128)(2,1)}), bf16[4,128,256]{2,1,0:T(8,128)(2,1)S(1)}, u32[]{:S(2)}, u32[]{:S(2)}) async-start(bf16[4,128,256]{2,1,0:T(8,128)(2,1)} %readout.1), calls=%async_computation.2 | async-start | bytes 524288 | tf_op jit(solution)/shard_map/all_to_all | solution.py:439
  66.5 172.8 %all-gather.18.cloned.1.call-start = ((), (), s32[]{:S(2)}) async-start(), calls=%async_computation.9 | async-start | bytes 2621440 | tf_op jit(solution)/shard_map/all_gather | solution.py:390
  73.2 0.7 copy-start.2
  80.8 45.7 %all-to-all-start.3 = ((bf16[64,96,128]{2,1,0:T(8,128)(2,1)}), bf16[64,96,128]{2,1,0:T(8,128)(2,1)S(1)}, u32[]{:S(2)}, u32[]{:S(2)}) async-start(bf16[64,96,128]{2,1,0:T(8,128)(2,1)} %bitcast.21), calls=%async_computation.3 | async-start | bytes 3145728 | tf_op jit(solution)/shard_map/all_to_all | solution.py:464
  86.4 188.0 %all-gather.20.cloned.1.call-start = ((), (), s32[]{:S(2)}) async-start(), calls=%async_computation.10 | async-start | bytes 2621440 | tf_op jit(solution)/shard_map/all_gather | solution.py:391
  126.5 42.3 %copy-start.1 = (bf16[64,96,128]{2,1,0:T(8,128)(2,1)}, bf16[64,96,128]{2,1,0:T(8,128)(2,1)S(1)}, u32[]{:S(2)}) copy-start(bf16[64,96,128]{2,1,0:T(8,128)(2,1)S(1)} %all-to-all-done.3) | copy-start | bytes 4718596
  183.2 10.7 %copy-start.5 = (f32[128,2]{0,1:T(2,128)S(1)}, f32[128,2]{0,1:T(2,128)}, u32[]{:S(2)}) copy-start(f32[128,2]{0,1:T(2,128)} %param.35) | copy-start | bytes 3076
  183.2 97.6 %all-to-all-start.4 = ((bf16[64,96,128]{2,1,0:T(8,128)(2,1)}), bf16[64,96,128]{2,1,0:T(8,128)(2,1)S(1)}, u32[]{:S(2)}, u32[]{:S(2)}) async-start(bf16[64,96,128]{2,1,0:T(8,128)(2,1)} %bitcast.20), calls=%async_computation.4 | async-start | bytes 3145728 | tf_op jit(solution)/shard_map/all_to_all | solution.py:488
  280.8 1.2 copy-start
Sparse Core Ops, SparseCore 0:
  9.1 53.7 all-gather.9
  64.7 51.1 all-gather.11
  117.7 51.1 all-gather.13
  170.5 33.6 all-gather.15
  205.9 33.3 all-gather.17
  241.0 33.3 all-gather.19

commit v2 on v1

--- a/solution.py
+++ b/solution.py
@@ -1,5 +1,3 @@
-import functools
-
 import jax
 import jax.numpy as jnp
 import numpy as np
@@ -8,6 +6,7 @@
 from jax.experimental.pallas import tpu as pltpu
 from jax.sharding import Mesh
 from jax.sharding import PartitionSpec as P
+
 
 KEY_CHANNELS = 64
 DV = 128
@@ -25,7 +24,10 @@
 SLOTS = EXPERTS * CAP
 LANES = 128
 COLS = D // LANES
+CHUNK = 256
+CHUNKS = D // CHUNK
 MSG = 272
+HALF_MSG = 144
 
 EPS = 1e-06
 GATE_NORM = 16.0
@@ -156,10 +158,9 @@
         qdev_ref[rows, :] = (q_in * reach).astype(BF16)
     final_f, final_b = states_f[count].astype(BF16), states_b[count].astype(BF16)
     sums = split_rows([sums_f[count], sums_b[count]]).astype(BF16)
-    for j in range(XC):
-        msg_ref[j, pl.ds(0, DV), :] = final_f
-        msg_ref[j, pl.ds(DV, DV), :] = final_b
-        msg_ref[j, pl.ds(2 * DV, 16), :] = sums
+    msg_ref[pl.ds(0, DV), :] = final_f
+    msg_ref[pl.ds(DV, DV), :] = final_b
+    msg_ref[pl.ds(2 * DV, 16), :] = sums
 
     expert = iota((TOK, EXPERTS), 1)
     picks = [routes_ref[:, k : k + 1] == expert for k in range(TOPK)]
@@ -177,10 +178,12 @@
     slots_ref[...] = slots.astype(jnp.int32)
 
 
-def compose_gathered(own, gathered_ref, length):
+def compose_gathered(own, gathered_ref, length, shared_place=False):
     results = []
     for forward in (True, False):
-        start, at = (0, 2 * DV) if forward else (DV, 2 * DV + 2)
+        start, tail_at, first = (0, 2 * DV, 0) if forward else (DV, 2 * DV, 2)
+        if shared_place:
+            start, tail_at, first = 0, DV, 0
         state, logs = jnp.zeros((DV, LANES), F32), jnp.zeros((1, LANES), F32)
         inner, inner_logs = state, logs
         for step in range(length):
@@ -188,8 +191,7 @@
             here = own == k
             inner = jnp.where(here, state, inner)
             inner_logs = jnp.where(here, logs, inner_logs)
-            tail = gathered_ref[k, pl.ds(2 * DV, 16), :].astype(F32)
-            first = at - 2 * DV
+            tail = gathered_ref[k, pl.ds(tail_at, 16), :].astype(F32)
             log = tail[first : first + 1, :] + tail[first + 1 : first + 2, :]
             state = state * jnp.exp(log) + gathered_ref[k, pl.ds(start, DV), :].astype(F32)
             logs = logs + log
@@ -203,24 +205,23 @@
     inner_ref[1] = backward[2]
     row_id = iota((8, LANES), 0)
     logs_ref[...] = jnp.where(row_id == 0, forward[3], jnp.where(row_id == 1, backward[3], 0.0))
-    total_f, total_b = forward[0].astype(BF16), backward[0].astype(BF16)
-    sums = split_rows([forward[1], backward[1]]).astype(BF16)
     for j in range(Z):
-        msg_ref[j, pl.ds(0, DV), :] = total_f
-        msg_ref[j, pl.ds(DV, DV), :] = total_b
-        msg_ref[j, pl.ds(2 * DV, 16), :] = sums
+        later = own_ref[1] < j
+        msg_ref[j, pl.ds(0, DV), :] = jnp.where(later, forward[0], backward[0]).astype(BF16)
+        logs = jnp.where(later, forward[1], backward[1])
+        msg_ref[j, pl.ds(DV, 16), :] = split_rows([logs]).astype(BF16)
 
 
 def readout_kernel(
-    own_ref, gathered_ref, inner_ref, logs_ref, part_ref, qdev_ref, gate_ref, gain_ref, out_ref
+    own_ref, gathered_ref, inner_ref, logs_ref, part_ref, qdev_ref, gate_ref, gain_ref, *out_refs
 ):
-    forward, backward = compose_gathered(own_ref[0], gathered_ref, Z)
+    forward, backward = compose_gathered(own_ref[1], gathered_ref, Z, shared_place=True)
     low = iota((DV, LANES), 1) < KEY_CHANNELS
     carry_f = inner_ref[0] + forward[2] * jnp.exp(logs_ref[0:1, :])
     carry_b = inner_ref[1] + backward[2] * jnp.exp(logs_ref[1:2, :])
     carried = jnp.concatenate([spread(carry_f, low), spread(carry_b, low)], axis=1).astype(BF16)
     for n in range(TP):
-        rows = pl.ds(n * TOK, TOK)
+        rows = pl.ds(pl.multiple_of((own_ref[2] + n) % TP * TOK, TOK), TOK)
         attended = part_ref[rows, :] + dot(qdev_ref[rows, :], carried, NT)
         heads = []
         for h in range(2):
@@ -228,7 +229,7 @@
             heads.append(head * lax.rsqrt(jnp.mean(head * head, axis=-1, keepdims=True) + EPS))
         gate = gate_ref[rows, :].astype(F32)
         mixed = jnp.concatenate(heads, axis=1) * gain_ref[...] * (gate * jax.nn.sigmoid(gate))
-        out_ref[n] = mixed.astype(BF16)
+        out_refs[n][...] = mixed.astype(BF16)
 
 
 def normalize(x):
@@ -236,20 +237,21 @@
 
 
 def project_kernel(
-    slots_ref, mixed_ref, weight_ref, stream_ref, mix_ref, ffn_ref,
-    residual_ref, normed_ref, sent_ref, acc_ref, rows_ref,
+    own_ref, slots_ref, mixed_0, mixed_1, mixed_2, mixed_3, weight_ref, stream_ref, mix_ref,
+    ffn_ref, residual_ref, normed_ref, sent_ref, acc_ref, rows_ref,
 ):
     step = pl.program_id(0)
-    product = dot(mixed_ref[0], weight_ref[...])
 
     @pl.when(step == 0)
     def _():
-        acc_ref[...] = product
+        acc_ref[...] = dot(mixed_0[...], weight_ref[...])
         sent_ref[...] = jnp.zeros_like(sent_ref)
 
-    @pl.when(step > 0)
-    def _():
-        acc_ref[...] += product
+    for n, mixed_ref in enumerate((mixed_1, mixed_2, mixed_3)):
+
+        @pl.when(step == n + 1)
+        def _(mixed_ref=mixed_ref):
+            acc_ref[...] += dot(mixed_ref[...], weight_ref[...])
 
     @pl.when(step == TP - 1)
     def _():
@@ -271,50 +273,97 @@
         lax.fori_loop(0, TOK, place, 0, unroll=8)
 
 
-def hidden_of(rows, gate, up):
-    a = dot(rows, gate)
-    return (a * jax.nn.sigmoid(a) * dot(rows, up)).astype(BF16)
-
-
-def expert_kernel(sent_ref, gate_ref, up_ref, down_ref, out_ref, lines_ref, rows_ref, acc_ref):
-    step = pl.program_id(0)
-
-    @pl.when(step == 0)
-    def _():
-        lines_ref[...] = sent_ref[...].astype(F32)
-        for j in range(COLS):
-            rows_ref[:, j * LANES : (j + 1) * LANES] = lines_ref[
-                pl.ds(j, SLOTS, stride=COLS), :
-            ].astype(BF16)
-
-    product = dot(hidden_of(rows_ref[...], gate_ref[0], up_ref[0]), down_ref[0])
-
-    @pl.when(step == 0)
-    def _():
-        acc_ref[...] = product
-
-    @pl.when(step > 0)
-    def _():
-        acc_ref[...] += product
-
-    @pl.when(step == TP - 1)
-    def _():
-        for j in range(COLS):
-            lines_ref[pl.ds(j, SLOTS, stride=COLS), :] = acc_ref[:, j * LANES : (j + 1) * LANES]
-        out_ref[...] = lines_ref[...].astype(BF16)
-
-
-def shared_kernel(rows_ref, gate_ref, up_ref, down_ref, out_ref):
-    step = pl.program_id(0)
-    product = dot(hidden_of(rows_ref[...], gate_ref[0], up_ref[0]), down_ref[0])
-
-    @pl.when(step == 0)
-    def _():
-        out_ref[...] = product
-
-    @pl.when(step > 0)
-    def _():
-        out_ref[...] += product
+def pack_shared_kernel(gate_ref, up_ref, down_ref, after_ref, out_ref):
+    for i in range(CHUNKS):
+        rows = pl.ds(i * CHUNK, CHUNK)
+        out_ref[i, pl.ds(0, CHUNK), pl.ds(0, LANES)] = gate_ref[rows, :]
+        out_ref[i, pl.ds(0, CHUNK), pl.ds(LANES, LANES)] = up_ref[rows, :]
+        out_ref[i, pl.ds(CHUNK, LANES), :] = down_ref[:, rows]
+
+
+def pack_shared(gate, up, down, after):
+    return pl.pallas_call(
+        pack_shared_kernel,
+        out_shape=shape((CHUNKS, CHUNK + LANES, CHUNK), BF16),
+        in_specs=[vmem()] * 3 + [anywhere()],
+        out_specs=vmem(),
+        compiler_params=params(),
+        cost_estimate=cost(1_000_000, 3_200_000),
+        name="pack_shared",
+    )(gate, up, down, after)
+
+
+def silu(x):
+    return x * jax.nn.sigmoid(x)
+
+
+def expert_kernel(*refs):
+    sent_ref, gates, ups = refs[0], refs[1:5], refs[5:9]
+    downs = refs[9:13]
+    out_ref, lines_ref, rows_ref, acc_ref, gate_ref, up_ref, down_ref, sems = refs[13:]
+
+    def pieces(n):
+        return [
+            pltpu.make_async_copy(gates[n], gate_ref.at[n], sems.at[0, n]),
+            pltpu.make_async_copy(ups[n], up_ref.at[n], sems.at[1, n]),
+            pltpu.make_async_copy(downs[n], down_ref.at[n], sems.at[2, n]),
+        ]
+
+    for n in range(TP):
+        for piece in pieces(n):
+            piece.start()
+    lines_ref[...] = sent_ref[...].astype(F32)
+    for j in range(COLS):
+        rows_ref[:, j * LANES : (j + 1) * LANES] = lines_ref[
+            pl.ds(j, SLOTS, stride=COLS), :
+        ].astype(BF16)
+    acc_ref[...] = jnp.zeros_like(acc_ref)
+
+    def shard(n, carry):
+        pltpu.make_async_copy(gates[0], gate_ref.at[n], sems.at[0, n]).wait()
+        pltpu.make_async_copy(ups[0], up_ref.at[n], sems.at[1, n]).wait()
+        rows = rows_ref[...]
+        hidden = (silu(dot(rows, gate_ref[n])) * dot(rows, up_ref[n])).astype(BF16)
+        pltpu.make_async_copy(downs[0], down_ref.at[n], sems.at[2, n]).wait()
+        for j in range(CHUNKS):
+            columns = pl.ds(j * CHUNK, CHUNK)
+            acc_ref[:, columns] += dot(hidden, down_ref[n, :, columns])
+        return carry
+
+    lax.fori_loop(0, TP, shard, 0)
+    for j in range(COLS):
+        lines_ref[pl.ds(j, SLOTS, stride=COLS), :] = acc_ref[:, j * LANES : (j + 1) * LANES]
+    out_ref[...] = lines_ref[...].astype(BF16)
+
+
+def shared_kernel(*refs):
+    rows_ref, shards, out_ref, weight_ref, sems = refs[0], refs[1:6], refs[6], refs[7], refs[8]
+    half = CHUNKS // 2
+    copies = [pltpu.make_async_copy(shards[n], weight_ref.at[n], sems.at[n]) for n in range(TP - 1)]
+    copies += [
+        pltpu.make_async_copy(
+            shards[TP - 1 + n], weight_ref.at[TP - 1, pl.ds(n * half, half)], sems.at[TP - 1 + n]
+        )
+        for n in range(2)
+    ]
+    for copy in copies:
+        copy.start()
+    for n in range(TP):
+        copies[n].wait()
+        if n == TP - 1:
+            copies[TP].wait()
+        joint = jnp.zeros((TOK, 2 * LANES), F32)
+        for i in range(CHUNKS):
+            columns = pl.ds(i * CHUNK, CHUNK)
+            joint = joint + dot(rows_ref[:, columns], weight_ref[n, i, 0:CHUNK, :])
+        hidden = (silu(joint[:, :LANES]) * joint[:, LANES:]).astype(BF16)
+        for i in range(CHUNKS):
+            columns = pl.ds(i * CHUNK, CHUNK)
+            product = dot(hidden, weight_ref[n, i, CHUNK:, :])
+            if n == 0:
+                out_ref[:, columns] = product
+            else:
+                out_ref[:, columns] += product
 
 
 def combine_kernel(
@@ -339,6 +388,14 @@
 
 def vmem():
     return pl.BlockSpec(memory_space=pltpu.VMEM)
+
+
+def anywhere():
+    return pl.BlockSpec(memory_space=pl.ANY)
+
+
+def shift(array, hops):
+    return lax.ppermute(array, "tp", [(i, (i + hops) % TP) for i in range(TP)])
 
 
 def smem():
@@ -383,12 +440,13 @@
     shared_up,
     shared_down,
 ):
-    gates = lax.all_gather(expert_gate[0], "tp", axis=0)
-    ups = lax.all_gather(expert_up[0], "tp", axis=0)
-    downs = lax.all_gather(expert_down[0], "tp", axis=0)
-    shared_gates = lax.all_gather(shared_gate, "tp", axis=0)
-    shared_ups = lax.all_gather(shared_up, "tp", axis=0)
-    shared_downs = lax.all_gather(shared_down, "tp", axis=0)
+    own = jnp.stack([lax.axis_index(axes) for axes in (PLANE, "sp_0", "tp", "sp_2")])
+    own = own.astype(jnp.int32)
+    gate, up, down = expert_gate[0], expert_up[0], expert_down[0]
+    gate_left = shift(gate, 1)
+    gate_right = shift(gate, -1)
+    up_left = shift(up, 1)
+    up_right = shift(up, -1)
 
     local, base = rope_tables()
     base_here = lax.dynamic_index_in_dim(jnp.asarray(base), lax.axis_index(SP), 0, keepdims=False)
@@ -397,7 +455,7 @@
         out_shape=(
             shape((SPAN, 2 * DV), F32),
             shape((SPAN, 2 * LANES), BF16),
-            shape((XC, MSG, LANES), BF16),
+            shape((MSG, LANES), BF16),
             shape((TOK, TOPK), jnp.int32),
         ),
         in_specs=[vmem()] * 8,
@@ -409,101 +467,116 @@
     )(queries, key_rows, values, fwd_decay, bwd_decay, jnp.asarray(local), base_here, routes)
     flat_slots = slots.reshape(-1)
 
-    in_plane = lax.all_to_all(msg, PLANE, split_axis=0, concat_axis=0, tiled=True)
+    in_plane = lax.all_gather(msg, PLANE, axis=0)
     inner, logs, msg = pl.pallas_call(
         plane_kernel,
         out_shape=(
             shape((2, DV, LANES), F32),
             shape((8, LANES), F32),
-            shape((Z, MSG, LANES), BF16),
+            shape((Z, HALF_MSG, LANES), BF16),
         ),
         in_specs=[smem(), vmem()],
         out_specs=(vmem(),) * 3,
         compiler_params=params(),
         cost_estimate=cost(10_000_000, 1_000_000),
         name="plane",
-    )(lax.axis_index(PLANE).astype(jnp.int32).reshape(1), in_plane)
+    )(own, in_plane)
     planes = lax.all_to_all(msg, "sp_0", split_axis=0, concat_axis=0, tiled=True)
     mixed = pl.pallas_call(
         readout_kernel,
-        out_shape=shape((TP, TOK, 2 * DV), BF16),
+        out_shape=(shape((TOK, 2 * DV), BF16),) * TP,
         in_specs=[smem()] + [vmem()] * 7,
-        out_specs=vmem(),
+        out_specs=(vmem(),) * TP,
         compiler_params=params(),
         cost_estimate=cost(100_000_000, 3_000_000),
         name="readout",
     )(
-        lax.axis_index("sp_0").astype(jnp.int32).reshape(1),
-        planes, inner, logs, part, qdev, out_gate, head_gain.reshape(1, -1),
-    )
-    mixed = lax.all_to_all(mixed, "tp", split_axis=0, concat_axis=0, tiled=True)
+        own, planes, inner, logs, part, qdev, out_gate, head_gain.reshape(1, -1),
+    )
+    mixed = [shift(piece, n) if n else piece for n, piece in enumerate(mixed)]
+
+    down_left = shift(down, 1)
+    down_right = shift(down, -1)
+    gate_far = shift(gate_left, 1)
+    up_far = shift(up_right, -1)
+    down_far_1 = shift(down_left[: down.shape[0] // 2], 1)
+    down_far_2 = shift(down_right[down.shape[0] // 2 :], -1)
 
     residual, normed, sent = pl.pallas_call(
         project_kernel,
-        grid=(TP,),
         out_shape=(
             shape((TOK, D), BF16),
             shape((TOK, D), BF16),
             shape((SLOTS, COLS, LANES), BF16),
         ),
-        in_specs=[
-            smem(),
-            pl.BlockSpec((1, TOK, 2 * DV), lambda i: (i, 0, 0)),
-            pl.BlockSpec((2 * DV, D), lambda i: (i, 0)),
-            whole((TOK, D)),
-            whole((1, D)),
-            whole((1, D)),
-        ],
-        out_specs=(whole((TOK, D)), whole((TOK, D)), whole((SLOTS, COLS, LANES))),
-        scratch_shapes=[pltpu.VMEM((TOK, D), F32), pltpu.VMEM((TOK * COLS, LANES), F32)],
+        grid_spec=pltpu.PrefetchScalarGridSpec(
+            num_scalar_prefetch=2,
+            grid=(TP,),
+            in_specs=[whole((TOK, 2 * DV))] * TP
+            + [
+                pl.BlockSpec((2 * DV, D), lambda i, own, _: ((own[2] + TP - i) % TP, 0)),
+                whole((TOK, D)),
+                whole((1, D)),
+                whole((1, D)),
+            ],
+            out_specs=(whole((TOK, D)), whole((TOK, D)), whole((SLOTS, COLS, LANES))),
+            scratch_shapes=[pltpu.VMEM((TOK, D), F32), pltpu.VMEM((TOK * COLS, LANES), F32)],
+        ),
         compiler_params=params(dimension_semantics=("arbitrary",)),
         cost_estimate=cost(600_000_000, 8_000_000),
         name="project",
-    )(flat_slots, mixed, out_proj, stream, mix_gain.reshape(1, -1), ffn_gain.reshape(1, -1))
+    )(own, flat_slots, *mixed, out_proj, stream, mix_gain.reshape(1, -1), ffn_gain.reshape(1, -1))
 
     arrived = lax.all_to_all(
         sent.reshape(EXPERTS, CAP * COLS, LANES), SP, split_axis=0, concat_axis=0, tiled=True
     )
-    width = gates.shape[-1]
+    width = gate.shape[1]
+    down_far = jnp.concatenate([down_far_1, down_far_2], axis=0)
     done = pl.pallas_call(
         expert_kernel,
-        grid=(TP,),
         out_shape=shape((SLOTS * COLS, LANES), BF16),
-        in_specs=[
-            whole((SLOTS * COLS, LANES)),
-            pl.BlockSpec((1, D, width), lambda i: (i, 0, 0)),
-            pl.BlockSpec((1, D, width), lambda i: (i, 0, 0)),
-            pl.BlockSpec((1, width, D), lambda i: (i, 0, 0)),
-        ],
-        out_specs=whole((SLOTS * COLS, LANES)),
+        in_specs=[vmem()] + [anywhere()] * 12,
+        out_specs=vmem(),
         scratch_shapes=[
             pltpu.VMEM((SLOTS * COLS, LANES), F32),
             pltpu.VMEM((SLOTS, D), BF16),
             pltpu.VMEM((SLOTS, D), F32),
+            pltpu.VMEM((TP, D, width), BF16),
+            pltpu.VMEM((TP, D, width), BF16),
+            pltpu.VMEM((TP, width, D), BF16),
+            pltpu.SemaphoreType.DMA((3, TP)),
         ],
-        compiler_params=params(dimension_semantics=("arbitrary",)),
+        compiler_params=params(),
         cost_estimate=cost(4_900_000_000, 16_000_000),
         name="experts",
-    )(arrived.reshape(SLOTS * COLS, LANES), gates, ups, downs)
+    )(
+        arrived.reshape(SLOTS * COLS, LANES),
+        gate, gate_left, gate_right, gate_far,
+        up, up_left, up_right, up_far,
+        down, down_left, down_right, down_far,
+    )
     back = lax.all_to_all(
         done.reshape(EXPERTS, CAP * COLS, LANES), SP, split_axis=0, concat_axis=0, tiled=True
     )
-    shared_width = shared_gates.shape[-1]
+    packed = pack_shared(shared_gate, shared_up, shared_down, residual)
+    half = CHUNKS // 2
+    shared_left = shift(packed, 1)
+    shared_right = shift(packed, -1)
+    shared_far_1 = shift(shared_left[:half], 1)
+    shared_far_2 = shift(shared_right[half:], -1)
     shared = pl.pallas_call(
         shared_kernel,
-        grid=(TP,),
         out_shape=shape((TOK, D), F32),
-        in_specs=[
-            whole((TOK, D)),
-            pl.BlockSpec((1, D, shared_width), lambda i: (i, 0, 0)),
-            pl.BlockSpec((1, D, shared_width), lambda i: (i, 0, 0)),
-            pl.BlockSpec((1, shared_width, D), lambda i: (i, 0, 0)),
+        in_specs=[vmem()] + [anywhere()] * 5,
+        out_specs=vmem(),
+        scratch_shapes=[
+            pltpu.VMEM((TP, *packed.shape), BF16),
+            pltpu.SemaphoreType.DMA((TP + 1,)),
         ],
-        out_specs=whole((TOK, D)),
-        compiler_params=params(dimension_semantics=("arbitrary",)),
+        compiler_params=params(),
         cost_estimate=cost(800_000_000, 8_000_000),
         name="shared",
-    )(normed, shared_gates, shared_ups, shared_downs)
+    )(normed, packed, shared_left, shared_right, shared_far_1, shared_far_2)
     return pl.pallas_call(
         combine_kernel,
         out_shape=shape((TOK, D), BF16),
@@ -543,6 +616,7 @@
         P(None, "tp"),
         P("tp", None),
     )
+
     return jax.shard_map(
         body, mesh=finer, in_specs=placed, out_specs=P(SP_TP, None), check_vma=False
     )

time: 294 us -> 280 us (0.952)
  waiting for transfers between devices: 171 us -> 147 us
  starting transfers between devices: 20.8 us -> 40.3 us
  between operations: 13.5 us -> 0.18 us
  local copies, waits for them, and re-layouts: 5.38 us -> 10.9 us
  blocking collectives: 41.3 us -> 36.3 us
    ppermute x0 -> x17, waiting for transfers between devices: none -> 147 us  [shift(): return lax.ppermute(array, 'tp', [(i, (i + hops) % TP) for i in range(TP)])]
    all_gather x6 -> x0, waiting for transfers between devices: 122 us -> none  [the longest x1 42.3 us: body(): downs = lax.all_gather(expert_down[0], 'tp', axis=0)]
    all_to_all x1, waiting for transfers between devices: 39.5 us -> 0.01 us  [body(): lax.all_to_all(sent.reshape(EXPERTS, CAP * COLS, LANES), SP, split_axis=0...]
    ppermute x0 -> x17, starting transfers between devices: none -> 24.8 us  [shift(): return lax.ppermute(array, 'tp', [(i, (i + hops) % TP) for i in range(TP)])]
    all_to_all x1 -> x0, blocking collectives: 15.7 us -> none  [body(): lax.all_to_all(msg, PLANE, split_axis=0, concat_axis=0, tiled=True)]
    all_gather x0 -> x1, blocking collectives: none -> 14.6 us  [body(): in_plane = lax.all_gather(msg, PLANE, axis=0)]
    all_to_all x1 -> x0, waiting for transfers between devices: 5.44 us -> none  [body(): mixed = lax.all_to_all(mixed, 'tp', split_axis=0, concat_axis=0, tiled=True)]
    unnamed x14 -> x36, local copies, waits for them, and re-layouts: 2.75 us -> 8.04 us
  transfers between devices with their start and end apart: 9 -> 19, of which waited for: 6 -> 10; matrix products, arithmetic and copies ran while one was open for 1% -> 1% of each run, Pallas kernels for 13% -> 3%
where the time goes in v2:
time: 280 us; the launch traced here: 279 us
  waiting for transfers between devices  147 us (52%)
  Pallas kernels  42.1 us (15%)
  starting transfers between devices  40.3 us (14%)
  blocking collectives  36.3 us (13%)
  local copies, waits for them, and re-layouts  10.9 us (4%)
    ppermute x17, waiting for transfers between devices, shift(): return lax.ppermute(array, 'tp', [(i, (i + hops) % TP) for i in range(TP)])  147 us
    ppermute x17, starting transfers between devices, shift(): return lax.ppermute(array, 'tp', [(i, (i + hops) % TP) for i in range(TP)])  24.8 us
    all_to_all x1, blocking collectives, body(): lax.all_to_all(msg, 'sp_0', split_axis=0, concat_axis=0, tiled=True)  21.7 us
    all_gather x1, blocking collectives, body(): in_plane = lax.all_gather(msg, PLANE, axis=0)  14.6 us
    pallas_call x1, Pallas kernels, body(): pl.pallas_call(expert_kernel, out_shape=shape((SLOTS * COLS, LANES), BF16...  12.7 us
    all_to_all x1, starting transfers between devices, body(): lax.all_to_all(done.reshape(EXPERTS, CAP * COLS, LANES), SP, split_axis=0...  10.3 us
    unnamed x36, local copies, waits for them, and re-layouts  8.04 us
    pallas_call x1, Pallas kernels, body(): pl.pallas_call(project_kernel, out_shape=(shape((TOK, D), BF16), shape((T...  7.24 us
  transfers between devices with their start and end apart: 19, of which 10 were waited for; matrix products, arithmetic and copies ran while one was open for 1% of the time, Pallas kernels for 3%

profile of v2, /device:TPU:2, one launch (start us, length us, event | category | flops | bytes accessed | tf_op | source)
XLA Modules:
  0.0 278.7 jit_solution(5120043935719045466)
XLA Ops:
  2.7 4.7 %attention.1 = (f32[512,256]{1,0:T(8,128)}, bf16[512,256]{1,0:T(8,128)(2,1)}, bf16[272,128]{1,0:T(8,128)(2,1)}, s32[128,2]{1,0:T(8,128)}) custom-call(bf16[512,128]{1,0:T(8,128)(2,1)} %q_ref.1, bf16[512,128]{1,0:T(8,128)(2,1)} %k_ref.1, bf16[512,256]{1,0:T(8,128)(2,1)} %v_ref.1, f32[512,128]{1,0:T(8,128)} %fd_ref.1, f32[512,128]{1,0:T(8,128)} %bd_ref.1, ...), custom_call_target="tpu_custom_call" | custom-call | flops 600000000 | bytes 4000000 | tf_op jit(solution)/shard_map/attention/pallas_call | solution.py:453
  7.4 14.6 %all-gather = bf16[2176,128]{1,0:T(8,128)(2,1)} all-gather(bf16[272,128]{1,0:T(8,128)(2,1)} %get-tuple-element.20), channel_id=2, replica_groups=mesh['sp_0'=8,'sp_1'=4,'sp_2'=2,'tp'=4] {'sp_1','sp_2'}, dimensions={0}, use_global_device_ids=true | all-gather | bytes 626688 | tf_op jit(solution)/shard_map/all_gather | solution.py:470
  24.6 21.7 %all_to_all.15.gathered_ref = bf16[8,144,128]{2,1,0:T(8,128)(2,1)} all-to-all(bf16[8,144,128]{2,1,0:T(8,128)(2,1)} %get-tuple-element.21), channel_id=1, replica_groups=mesh['sp_0'=8,'sp_1'=4,'sp_2'=2,'tp'=4] {'sp_0'}, dimensions={0} | all-to-all | bytes 589824 | tf_op jit(solution)/shard_map/all_to_all | solution.py:484
  46.3 2.6 readout.1
  50.4 2.9 %collective-permute-start.1 = (bf16[128,256]{1,0:T(8,128)(2,1)}, bf16[128,256]{1,0:T(8,128)(2,1)S(1)}, u32[]{:S(2)}, u32[]{:S(2)}) collective-permute-start(bf16[128,256]{1,0:T(8,128)(2,1)} %get-tuple-element.28), channel_id=1, source_target_pairs={{0,2},{1,3},{2,0},{3,1},{4,6},{5,7},{6,4},{7,5},{8,10},{9,11},{10,... | collective-permute-start | bytes 196616 | tf_op jit(solution)/shard_map/ppermute | solution.py:398
  58.4 7.2 %project.1 = (bf16[128,2048]{1,0:T(8,128)(2,1)}, bf16[128,2048]{1,0:T(8,128)(2,1)}, bf16[384,16,128]{2,1,0:T(8,128)(2,1)}) custom-call(s32[4]{0:T(128)} %pad_add_fusion.own_ref, s32[256]{0:T(256)} %reshape.30.slots_ref, bf16[128,256]{1,0:T(8,128)(2,1)} %get-tuple-element.26.mixed_0, bf16[128,256]{1,0:T(8,128)(2,1)} %copy-done.6, bf16[128,256]{1,0:T(8,128)(2,1)} %copy-done.7, ...), custom_call_target="tpu_custom_call" | custom-call | flops 600000000 | bytes 8000000 | tf_op jit(solution)/shard_map/project/pallas_call | solution.py:505
  65.7 5.2 %all-to-all-start.1 = ((bf16[64,96,128]{2,1,0:T(8,128)(2,1)}), bf16[64,96,128]{2,1,0:T(8,128)(2,1)S(1)}, u32[]{:S(2)}, u32[]{:S(2)}) async-start(bf16[64,96,128]{2,1,0:T(8,128)(2,1)} %bitcast.20), calls=%async_computation.1 | async-start | bytes 3145728 | tf_op jit(solution)/shard_map/all_to_all | solution.py:530
  70.9 2.6 collective-permute-start.10
  73.5 3.2 %collective-permute-start.7 = (bf16[2048,256]{1,0:T(8,128)(2,1)}, bf16[2048,256]{1,0:T(8,128)(2,1)S(1)}, u32[]{:S(2)}, u32[]{:S(2)}) collective-permute-start(bf16[2048,256]{1,0:T(8,128)(2,1)} %bitcast.30), channel_id=1, source_target_pairs={{0,3},{1,0},{2,1},{3,2},{4,7},{5,4},{6,5},{7,6},{8,11},{9,8},{10,9... | collective-permute-start | bytes 3145736 | tf_op jit(solution)/shard_map/ppermute | solution.py:398
  76.7 20.6 %collective-permute-done.10.refs_11_ = bf16[256,2048]{1,0:T(8,128)(2,1)S(1)} collective-permute-done((bf16[256,2048]{1,0:T(8,128)(2,1)}, bf16[256,2048]{1,0:T(8,128)(2,1)S(1)}, u32[]{:S(2)}, u32[]{:S(2)}) %collective-permute-start.10) | collective-permute-done | bytes 1048608 | tf_op jit(solution)/shard_map/ppermute | solution.py:398
  97.4 3.7 %collective-permute-start.12 = (bf16[128,2048]{1,0:T(8,128)(2,1)S(1)}, bf16[128,2048]{1,0:T(8,128)(2,1)S(1)}, u32[]{:S(2)}, u32[]{:S(2)}) collective-permute-start(bf16[128,2048]{1,0:T(8,128)(2,1)S(1)} %slice.17), channel_id=1, source_target_pairs={{0,3},{1,0},{2,1},{3,2},{4,7},{5,4},{6,5},{7,6},{8,11},{9,8},{10,9... | collective-permute-start | bytes 1572872 | tf_op jit(solution)/shard_map/ppermute | solution.py:398
  103.1 16.7 %collective-permute-done.7.refs_7_ = bf16[2048,256]{1,0:T(8,128)(2,1)S(1)} collective-permute-done((bf16[2048,256]{1,0:T(8,128)(2,1)}, bf16[2048,256]{1,0:T(8,128)(2,1)S(1)}, u32[]{:S(2)}, u32[]{:S(2)}) %collective-permute-start.7) | collective-permute-done | bytes 1048608 | tf_op jit(solution)/shard_map/ppermute | solution.py:398
  120.0 3.2 %collective-permute-done.9.refs_10_ = bf16[256,2048]{1,0:T(8,128)(2,1)S(1)} collective-permute-done((bf16[256,2048]{1,0:T(8,128)(2,1)}, bf16[256,2048]{1,0:T(8,128)(2,1)S(1)}, u32[]{:S(2)}, u32[]{:S(2)}) %collective-permute-start.9) | collective-permute-done | bytes 1048608 | tf_op jit(solution)/shard_map/ppermute | solution.py:398
  123.6 7.4 %collective-permute-done.12 = bf16[128,2048]{1,0:T(8,128)(2,1)S(1)} collective-permute-done((bf16[128,2048]{1,0:T(8,128)(2,1)S(1)}, bf16[128,2048]{1,0:T(8,128)(2,1)S(1)}, u32[]{:S(2)}, u32[]{:S(2)}) %collective-permute-start.12) | collective-permute-done | bytes 524320 | tf_op jit(solution)/shard_map/ppermute | solution.py:398
  131.2 47.0 %collective-permute-done.11 = bf16[128,2048]{1,0:T(8,128)(2,1)S(1)} collective-permute-done((bf16[128,2048]{1,0:T(8,128)(2,1)S(1)}, bf16[128,2048]{1,0:T(8,128)(2,1)S(1)}, u32[]{:S(2)}, u32[]{:S(2)}) %collective-permute-start.11) | collective-permute-done | bytes 524320 | tf_op jit(solution)/shard_map/ppermute | solution.py:398
  182.9 12.7 %experts.1 = bf16[6144,128]{1,0:T(8,128)(2,1)} custom-call(bf16[6144,128]{1,0:T(8,128)(2,1)} %bitcast.21, bf16[2048,256]{1,0:T(8,128)(2,1)} %bitcast.27, bf16[2048,256]{1,0:T(8,128)(2,1)} %copy-done.12, bf16[2048,256]{1,0:T(8,128)(2,1)} %copy-done.14, bf16[2048,256]{1,0:T(8,128)(2,1)} %copy-done.16, bf16[2048,256]{1,0:T(8,128)(2,1)} %bitcast.32, ...), custom_call_target="tpu_custom_call" | custom-call | flops 4899999744 | bytes 16000000 | tf_op jit(solution)/shard_map/experts/pallas_call | solution.py:535
  195.6 10.3 %all-to-all-start.2 = ((bf16[64,96,128]{2,1,0:T(8,128)(2,1)}), bf16[64,96,128]{2,1,0:T(8,128)(2,1)S(1)}, u32[]{:S(2)}, u32[]{:S(2)}) async-start(bf16[64,96,128]{2,1,0:T(8,128)(2,1)} %bitcast.22), calls=%async_computation.2 | async-start | bytes 3145728 | tf_op jit(solution)/shard_map/all_to_all | solution.py:558
  205.9 2.7 pack_shared.1.refs_1_
  208.6 3.2 %collective-permute-start.14 = (bf16[8,384,256]{2,1,0:T(8,128)(2,1)}, bf16[8,384,256]{2,1,0:T(8,128)(2,1)S(1)}, u32[]{:S(2)}, u32[]{:S(2)}) collective-permute-start(bf16[8,384,256]{2,1,0:T(8,128)(2,1)} %pack_shared.1.refs_1_), channel_id=1, source_target_pairs={{0,3},{1,0},{2,1},{3,2},{4,7},{5,4},{6,5},{7,6},{8,11},{9,8},{10,9... | collective-permute-start | bytes 4718600 | tf_op jit(solution)/shard_map/ppermute | solution.py:398
  211.9 34.6 %collective-permute-done.13.refs_2_ = bf16[8,384,256]{2,1,0:T(8,128)(2,1)S(1)} collective-permute-done((bf16[8,384,256]{2,1,0:T(8,128)(2,1)}, bf16[8,384,256]{2,1,0:T(8,128)(2,1)S(1)}, u32[]{:S(2)}, u32[]{:S(2)}) %collective-permute-start.13) | collective-permute-done | bytes 1572896 | tf_op jit(solution)/shard_map/ppermute | solution.py:398
  248.2 3.2 %collective-permute-start.16 = (bf16[4,384,256]{2,1,0:T(8,128)(2,1)S(1)}, bf16[4,384,256]{2,1,0:T(8,128)(2,1)}, u32[]{:S(2)}, u32[]{:S(2)}) collective-permute-start(bf16[4,384,256]{2,1,0:T(8,128)(2,1)S(1)} %slice.19), channel_id=1, source_target_pairs={{0,3},{1,0},{2,1},{3,2},{4,7},{5,4},{6,5},{7,6},{8,11},{9,8},{10,9... | collective-permute-start | bytes 2359304 | tf_op jit(solution)/shard_map/ppermute | solution.py:398
  252.2 14.6 %collective-permute-done.15.refs_4_ = bf16[4,384,256]{2,1,0:T(8,128)(2,1)} collective-permute-done((bf16[4,384,256]{2,1,0:T(8,128)(2,1)S(1)}, bf16[4,384,256]{2,1,0:T(8,128)(2,1)}, u32[]{:S(2)}, u32[]{:S(2)}) %collective-permute-start.15) | collective-permute-done | bytes 786464 | tf_op jit(solution)/shard_map/ppermute | solution.py:398
  267.3 6.4 %shared.1.shared_ref = f32[128,2048]{1,0:T(8,128)} custom-call(bf16[128,2048]{1,0:T(8,128)(2,1)} %get-tuple-element.31.refs_0_, bf16[8,384,256]{2,1,0:T(8,128)(2,1)} %pack_shared.1.refs_1_, bf16[8,384,256]{2,1,0:T(8,128)(2,1)} %copy-done.1, bf16[8,384,256]{2,1,0:T(8,128)(2,1)} %copy-done.2, bf16[4,384,256]{2,1,0:T(8,128)(2,1)} %collective-permute-done.15.refs_4_, ...), custom_call_target="tpu_custom_call" | custom-call | flops 800000000 | bytes 8000000 | tf_op jit(solution)/shard_map/shared/pallas_call | solution.py:567
  275.0 3.7 %combine.1 = bf16[128,2048]{1,0:T(8,128)(2,1)} custom-call(s32[256]{0:T(256)} %reshape.30.slots_ref, f32[256]{0:T(256)} %reshape.31.weights_ref, bf16[384,16,128]{2,1,0:T(8,128)(2,1)} %bitcast.18, f32[128,2048]{1,0:T(8,128)} %shared.1.shared_ref, bf16[128,2048]{1,0:T(8,128)(2,1)} %get-tuple-element.32.after_ref.residual_ref, f32[1,2048]{1,0:T(1,128)} %bitcast.25), custom_call_target="tpu_custom_call" | custom-call | flops 5000000 | bytes 4000000 | tf_op jit(solution)/shard_map/combine/pallas_call | solution.py:580
  (69 shorter events, 23.5 us)
Async XLA Ops:
  7.4 47.3 %copy-start.9 = (s32[128,2]{1,0:T(8,128)S(1)}, s32[128,2]{1,0:T(8,128)}, u32[]{:S(2)}) copy-start(s32[128,2]{1,0:T(8,128)} %get-tuple-element.19) | copy-start | bytes 3076
  48.8 6.6 %collective-permute-start = (bf16[128,256]{1,0:T(8,128)(2,1)}, bf16[128,256]{1,0:T(8,128)(2,1)S(1)}, u32[]{:S(2)}, u32[]{:S(2)}) collective-permute-start(bf16[128,256]{1,0:T(8,128)(2,1)} %get-tuple-element.27), channel_id=1, source_target_pairs={{0,1},{1,2},{2,3},{3,0},{4,5},{5,6},{6,7},{7,4},{8,9},{9,10},{10,1... | collective-permute-start | bytes 196616 | tf_op jit(solution)/shard_map/ppermute | solution.py:398
  50.4 6.3 %collective-permute-start.1 = (bf16[128,256]{1,0:T(8,128)(2,1)}, bf16[128,256]{1,0:T(8,128)(2,1)S(1)}, u32[]{:S(2)}, u32[]{:S(2)}) collective-permute-start(bf16[128,256]{1,0:T(8,128)(2,1)} %get-tuple-element.28), channel_id=1, source_target_pairs={{0,2},{1,3},{2,0},{3,1},{4,6},{5,7},{6,4},{7,5},{8,10},{9,11},{10,... | collective-permute-start | bytes 196616 | tf_op jit(solution)/shard_map/ppermute | solution.py:398
  53.3 4.5 %collective-permute-start.2 = (bf16[128,256]{1,0:T(8,128)(2,1)}, bf16[128,256]{1,0:T(8,128)(2,1)S(1)}, u32[]{:S(2)}, u32[]{:S(2)}) collective-permute-start(bf16[128,256]{1,0:T(8,128)(2,1)} %get-tuple-element.29), channel_id=1, source_target_pairs={{0,3},{1,0},{2,1},{3,2},{4,7},{5,4},{6,5},{7,6},{8,11},{9,8},{10,9... | collective-permute-start | bytes 196616 | tf_op jit(solution)/shard_map/ppermute | solution.py:398
  65.7 116.0 %all-to-all-start.1 = ((bf16[64,96,128]{2,1,0:T(8,128)(2,1)}), bf16[64,96,128]{2,1,0:T(8,128)(2,1)S(1)}, u32[]{:S(2)}, u32[]{:S(2)}) async-start(bf16[64,96,128]{2,1,0:T(8,128)(2,1)} %bitcast.20), calls=%async_computation.1 | async-start | bytes 3145728 | tf_op jit(solution)/shard_map/all_to_all | solution.py:530
  70.9 26.5 %collective-permute-start.10 = (bf16[256,2048]{1,0:T(8,128)(2,1)}, bf16[256,2048]{1,0:T(8,128)(2,1)S(1)}, u32[]{:S(2)}, u32[]{:S(2)}) collective-permute-start(bf16[256,2048]{1,0:T(8,128)(2,1)} %bitcast.33), channel_id=1, source_target_pairs={{0,3},{1,0},{2,1},{3,2},{4,7},{5,4},{6,5},{7,6},{8,11},{9,8},{10,9... | collective-permute-start | bytes 3145736 | tf_op jit(solution)/shard_map/ppermute | solution.py:398
  73.5 27.7 %collective-permute-start.3 = (bf16[2048,256]{1,0:T(8,128)(2,1)S(1)}, bf16[2048,256]{1,0:T(8,128)(2,1)S(1)}, u32[]{:S(2)}, u32[]{:S(2)}) collective-permute-start(bf16[2048,256]{1,0:T(8,128)(2,1)S(1)} %bitcast.28), channel_id=1, source_target_pairs={{0,1},{1,2},{2,3},{3,0},{4,5},{5,6},{6,7},{7,4},{8,9},{9,10},{10,1... | collective-permute-start | bytes 3145736 | tf_op jit(solution)/shard_map/ppermute | solution.py:398
  73.5 46.3 %collective-permute-start.7 = (bf16[2048,256]{1,0:T(8,128)(2,1)}, bf16[2048,256]{1,0:T(8,128)(2,1)S(1)}, u32[]{:S(2)}, u32[]{:S(2)}) collective-permute-start(bf16[2048,256]{1,0:T(8,128)(2,1)} %bitcast.30), channel_id=1, source_target_pairs={{0,3},{1,0},{2,1},{3,2},{4,7},{5,4},{6,5},{7,6},{8,11},{9,8},{10,9... | collective-permute-start | bytes 3145736 | tf_op jit(solution)/shard_map/ppermute | solution.py:398
  76.7 46.5 %collective-permute-start.9 = (bf16[256,2048]{1,0:T(8,128)(2,1)}, bf16[256,2048]{1,0:T(8,128)(2,1)S(1)}, u32[]{:S(2)}, u32[]{:S(2)}) collective-permute-start(bf16[256,2048]{1,0:T(8,128)(2,1)} %bitcast.34), channel_id=1, source_target_pairs={{0,1},{1,2},{2,3},{3,0},{4,5},{5,6},{6,7},{7,4},{8,9},{9,10},{10,1... | collective-permute-start | bytes 3145736 | tf_op jit(solution)/shard_map/ppermute | solution.py:398
  97.4 82.0 %copy-start.4 = (bf16[256,2048]{1,0:T(8,128)(2,1)}, bf16[256,2048]{1,0:T(8,128)(2,1)S(1)}, u32[]{:S(2)}) copy-start(bf16[256,2048]{1,0:T(8,128)(2,1)S(1)} %collective-permute-done.10.refs_11_) | copy-start | bytes 3145732
  97.4 33.6 %collective-permute-start.12 = (bf16[128,2048]{1,0:T(8,128)(2,1)S(1)}, bf16[128,2048]{1,0:T(8,128)(2,1)S(1)}, u32[]{:S(2)}, u32[]{:S(2)}) collective-permute-start(bf16[128,2048]{1,0:T(8,128)(2,1)S(1)} %slice.17), channel_id=1, source_target_pairs={{0,3},{1,0},{2,1},{3,2},{4,7},{5,4},{6,5},{7,6},{8,11},{9,8},{10,9... | collective-permute-start | bytes 1572872 | tf_op jit(solution)/shard_map/ppermute | solution.py:398
  101.1 78.3 %collective-permute-start.4 = (bf16[2048,256]{1,0:T(8,128)(2,1)S(1)}, bf16[2048,256]{1,0:T(8,128)(2,1)S(1)}, u32[]{:S(2)}, u32[]{:S(2)}) collective-permute-start(bf16[2048,256]{1,0:T(8,128)(2,1)S(1)} %bitcast.29), channel_id=1, source_target_pairs={{0,3},{1,0},{2,1},{3,2},{4,7},{5,4},{6,5},{7,6},{8,11},{9,8},{10,9... | collective-permute-start | bytes 3145736 | tf_op jit(solution)/shard_map/ppermute | solution.py:398
  101.2 78.3 %copy-start.12 = (bf16[2048,256]{1,0:T(8,128)(2,1)}, bf16[2048,256]{1,0:T(8,128)(2,1)S(1)}, u32[]{:S(2)}) copy-start(bf16[2048,256]{1,0:T(8,128)(2,1)S(1)} %collective-permute-done.3.refs_2_) | copy-start | bytes 3145732
  101.2 78.2 %collective-permute-start.6 = (bf16[2048,256]{1,0:T(8,128)(2,1)}, bf16[2048,256]{1,0:T(8,128)(2,1)S(1)}, u32[]{:S(2)}, u32[]{:S(2)}) collective-permute-start(bf16[2048,256]{1,0:T(8,128)(2,1)} %bitcast.31), channel_id=1, source_target_pairs={{0,1},{1,2},{2,3},{3,0},{4,5},{5,6},{6,7},{7,4},{8,9},{9,10},{10,1... | collective-permute-start | bytes 3145736 | tf_op jit(solution)/shard_map/ppermute | solution.py:398
  119.8 59.6 %copy-start.13 = (bf16[2048,256]{1,0:T(8,128)(2,1)}, bf16[2048,256]{1,0:T(8,128)(2,1)S(1)}, u32[]{:S(2)}) copy-start(bf16[2048,256]{1,0:T(8,128)(2,1)S(1)} %collective-permute-done.7.refs_7_) | copy-start | bytes 3145732
  119.8 59.6 %collective-permute-start.5 = (bf16[2048,256]{1,0:T(8,128)(2,1)S(1)}, bf16[2048,256]{1,0:T(8,128)(2,1)S(1)}, u32[]{:S(2)}, u32[]{:S(2)}) collective-permute-start(bf16[2048,256]{1,0:T(8,128)(2,1)S(1)} %collective-permute-done.3.refs_2_), channel_id=1, source_target_pairs={{0,1},{1,2},{2,3},{3,0},{4,5},{5,6},{6,7},{7,4},{8,9},{9,10},{10,1... | collective-permute-start | bytes 3145736 | tf_op jit(solution)/shard_map/ppermute | solution.py:398
  123.2 58.5 %collective-permute-start.8 = (bf16[2048,256]{1,0:T(8,128)(2,1)S(1)}, bf16[2048,256]{1,0:T(8,128)(2,1)}, u32[]{:S(2)}, u32[]{:S(2)}) collective-permute-start(bf16[2048,256]{1,0:T(8,128)(2,1)S(1)} %collective-permute-done.7.refs_7_), channel_id=1, source_target_pairs={{0,3},{1,0},{2,1},{3,2},{4,7},{5,4},{6,5},{7,6},{8,11},{9,8},{10,9... | collective-permute-start | bytes 3145736 | tf_op jit(solution)/shard_map/ppermute | solution.py:398
  131.0 47.3 %collective-permute-start.11 = (bf16[128,2048]{1,0:T(8,128)(2,1)S(1)}, bf16[128,2048]{1,0:T(8,128)(2,1)S(1)}, u32[]{:S(2)}, u32[]{:S(2)}) collective-permute-start(bf16[128,2048]{1,0:T(8,128)(2,1)S(1)} %slice.16), channel_id=1, source_target_pairs={{0,1},{1,2},{2,3},{3,0},{4,5},{5,6},{6,7},{7,4},{8,9},{9,10},{10,1... | collective-permute-start | bytes 1572872 | tf_op jit(solution)/shard_map/ppermute | solution.py:398
  195.6 78.2 %all-to-all-start.2 = ((bf16[64,96,128]{2,1,0:T(8,128)(2,1)}), bf16[64,96,128]{2,1,0:T(8,128)(2,1)S(1)}, u32[]{:S(2)}, u32[]{:S(2)}) async-start(bf16[64,96,128]{2,1,0:T(8,128)(2,1)} %bitcast.22), calls=%async_computation.2 | async-start | bytes 3145728 | tf_op jit(solution)/shard_map/all_to_all | solution.py:558
  208.6 42.8 %copy-start.10 = (f32[128,2]{0,1:T(2,128)S(1)}, f32[128,2]{0,1:T(2,128)}, u32[]{:S(2)}) copy-start(f32[128,2]{0,1:T(2,128)} %param.35) | copy-start | bytes 3076
  208.6 37.8 %collective-permute-start.13 = (bf16[8,384,256]{2,1,0:T(8,128)(2,1)}, bf16[8,384,256]{2,1,0:T(8,128)(2,1)S(1)}, u32[]{:S(2)}, u32[]{:S(2)}) collective-permute-start(bf16[8,384,256]{2,1,0:T(8,128)(2,1)} %pack_shared.1.refs_1_), channel_id=1, source_target_pairs={{0,1},{1,2},{2,3},{3,0},{4,5},{5,6},{6,7},{7,4},{8,9},{9,10},{10,1... | collective-permute-start | bytes 4718600 | tf_op jit(solution)/shard_map/ppermute | solution.py:398
  208.6 38.2 %collective-permute-start.14 = (bf16[8,384,256]{2,1,0:T(8,128)(2,1)}, bf16[8,384,256]{2,1,0:T(8,128)(2,1)S(1)}, u32[]{:S(2)}, u32[]{:S(2)}) collective-permute-start(bf16[8,384,256]{2,1,0:T(8,128)(2,1)} %pack_shared.1.refs_1_), channel_id=1, source_target_pairs={{0,3},{1,0},{2,1},{3,2},{4,7},{5,4},{6,5},{7,6},{8,11},{9,8},{10,9... | collective-permute-start | bytes 4718600 | tf_op jit(solution)/shard_map/ppermute | solution.py:398
  246.5 20.3 %collective-permute-start.15 = (bf16[4,384,256]{2,1,0:T(8,128)(2,1)S(1)}, bf16[4,384,256]{2,1,0:T(8,128)(2,1)}, u32[]{:S(2)}, u32[]{:S(2)}) collective-permute-start(bf16[4,384,256]{2,1,0:T(8,128)(2,1)S(1)} %slice.18), channel_id=1, source_target_pairs={{0,1},{1,2},{2,3},{3,0},{4,5},{5,6},{6,7},{7,4},{8,9},{9,10},{10,1... | collective-permute-start | bytes 2359304 | tf_op jit(solution)/shard_map/ppermute | solution.py:398
  248.2 19.1 %collective-permute-start.16 = (bf16[4,384,256]{2,1,0:T(8,128)(2,1)S(1)}, bf16[4,384,256]{2,1,0:T(8,128)(2,1)}, u32[]{:S(2)}, u32[]{:S(2)}) collective-permute-start(bf16[4,384,256]{2,1,0:T(8,128)(2,1)S(1)} %slice.19), channel_id=1, source_target_pairs={{0,3},{1,0},{2,1},{3,2},{4,7},{5,4},{6,5},{7,6},{8,11},{9,8},{10,9... | collective-permute-start | bytes 2359304 | tf_op jit(solution)/shard_map/ppermute | solution.py:398
  (12 other events, 28.7 us)

commit v3 on v2

v3 whole, which is shorter than its diff:
```python
import jax
import jax.numpy as jnp
import numpy as np
from jax import lax
from jax.experimental import pallas as pl
from jax.experimental.pallas import tpu as pltpu
from jax.sharding import Mesh
from jax.sharding import PartitionSpec as P


KEY_CHANNELS = 64
DV = 128
BLK = 128
TOPK = 2
CAP = 6
Z, XC, TP = 8, 8, 4
SP = ("sp_0", "sp_1", "sp_2")
PLANE = ("sp_1", "sp_2")
SP_TP = ("sp_0", "sp_1", "sp_2", "tp")
SPAN = 512
TOK = 128
D = 2048
EXPERTS = 64
SLOTS = EXPERTS * CAP
LANES = 128
COLS = D // LANES
CHUNK = 256
PIECES = 4
CHUNKS = D // CHUNK
MSG = 272
HALF_MSG = 144

EPS = 1e-06
GATE_NORM = 16.0
ROPE_BASE = 10000.0
F32 = jnp.float32
BF16 = jnp.bfloat16
NT = (((1,), (1,)), ((), ()))
TN = (((0,), (0,)), ((), ()))


def rope_tables():
    half = KEY_CHANNELS // 2
    frequency = ROPE_BASE ** (-np.arange(half, dtype=np.float64) / half)
    lanes = np.tile(frequency, LANES // half)
    tables = []
    for count, step in ((BLK, 1), (SPAN // BLK, BLK), (Z * XC, SPAN)):
        angles = (np.arange(count) * step)[:, None] * lanes[None, :]
        tables.append(np.stack([np.cos(angles), np.sin(angles)], axis=0).astype(np.float32))
    return tables[0], tables[1].reshape(-1, LANES), tables[2].swapaxes(0, 1)


def dot(a, b, dims=(((1,), (0,)), ((), ()))):
    return lax.dot_general(a, b, dims, preferred_element_type=F32)


def iota(shape, axis):
    return lax.broadcasted_iota(jnp.int32, shape, axis)


def log_sigmoid(x):
    return jnp.minimum(x, 0.0) - jnp.log1p(jnp.exp(-jnp.abs(x)))


def spread(state, low):
    return jnp.concatenate([jnp.where(low, state, 0.0), jnp.where(low, 0.0, state)], axis=0)


def split_rows(rows):
    pieces = []
    for row in rows:
        high = row.astype(BF16)
        pieces += [high.astype(F32), row - high.astype(F32)]
    row_id = iota((16, LANES), 0)
    out = jnp.zeros((16, LANES), F32)
    for i, piece in enumerate(pieces):
        out = jnp.where(row_id == i, piece, out)
    return out


class Block:
    def __init__(self, own_ref, local_ref, block_ref, base_ref):
        self.count = SPAN // BLK
        lane = iota((BLK, LANES), 1)
        self.low = lane < KEY_CHANNELS
        self.front = lane % KEY_CHANNELS < KEY_CHANNELS // 2
        self.row, self.col = iota((BLK, BLK), 0), iota((BLK, BLK), 1)
        self.local, self.blocks = local_ref, block_ref
        self.base = base_ref[own_ref[1] * XC + own_ref[0]]

    def tables(self, n):
        def add(a, b):
            return a[0] * b[0] - a[1] * b[1], a[1] * b[0] + a[0] * b[1]

        span = self.base[0:1, :], self.base[1:2, :]
        m = self.count + n
        start = add(span, (self.blocks[n : n + 1, :], self.blocks[m : m + 1, :]))
        cosine, sine = add(start, (self.local[0], self.local[1]))
        return cosine, jnp.where(self.front, -sine, sine)

    def rotate(self, u, tables):
        swapped = jnp.where(
            self.front,
            pltpu.roll(u, LANES - KEY_CHANNELS // 2, 1),
            pltpu.roll(u, KEY_CHANNELS // 2, 1),
        )
        return u * tables[0] + swapped * tables[1]

    def decays(self, log_ref, forward):
        tri = (self.row >= self.col if forward else self.row <= self.col).astype(BF16)
        parts = []
        for n in range(self.count):
            log = log_sigmoid(log_ref[pl.ds(n * BLK, BLK), :]) * (1.0 / GATE_NORM)
            for _ in range(3):
                part = log.astype(BF16)
                parts.append(part)
                log = log - part.astype(F32)
        sums = dot(tri, jnp.concatenate(parts, axis=1))
        pieces = [sums[:, i * LANES : (i + 1) * LANES] for i in range(3 * self.count)]
        return [sum(pieces[3 * n + 1 : 3 * n + 3], pieces[3 * n]) for n in range(self.count)]


def states_kernel(
    own_ref, k_ref, v_ref, fd_ref, bd_ref, local_ref, block_ref, base_ref,
    msg_ref, key_ref, cumul_ref, states_ref,
):
    block = Block(own_ref, local_ref, block_ref, base_ref)
    count, low = block.count, block.low
    updates, lasts = ([], []), ([], [])
    decays = [block.decays(fd_ref, True), block.decays(bd_ref, False)]
    for n in range(count):
        rows = pl.ds(n * BLK, BLK)
        k = block.rotate(k_ref[rows, :].astype(F32), block.tables(n))
        key_ref[rows, :] = k
        v = v_ref[rows, :]
        for d in range(2):
            cumul = decays[d][n]
            end = BLK - 1 if d == 0 else 0
            total = cumul[end : end + 1, :]
            cumul_ref[d, rows, :] = cumul
            k_out = k * jnp.exp(total - cumul)
            product = dot(v, k_out.astype(BF16), TN)
            updates[d].append(jnp.where(low, product[:DV], product[DV:]))
            lasts[d].append(total)
    finals, sums = [], []
    for d in range(2):
        state, logs = jnp.zeros((DV, LANES), F32), jnp.zeros((1, LANES), F32)
        for n in range(count) if d == 0 else reversed(range(count)):
            states_ref[d, n] = state
            state = state * jnp.exp(lasts[d][n]) + updates[d][n]
            logs = logs + lasts[d][n]
        finals.append(state.astype(BF16))
        sums.append(logs)
    tail = split_rows(sums).astype(BF16)
    for j in range(XC):
        msg_ref[j, pl.ds(0, DV), :] = finals[0]
        msg_ref[j, pl.ds(DV, DV), :] = finals[1]
        msg_ref[j, pl.ds(2 * DV, 16), :] = tail


def attention_kernel(
    own_ref, q_ref, v_ref, key_ref, cumul_ref, states_ref, local_ref, block_ref, base_ref,
    routes_ref,
    part_ref, qdev_ref, slots_ref,
):
    block = Block(own_ref, local_ref, block_ref, base_ref)
    count, low, row, col = block.count, block.low, block.row, block.col
    row2, col2 = iota((BLK, 2 * BLK), 0), iota((BLK, 2 * BLK), 1) % BLK
    wide_low = iota((BLK, 2 * DV), 1) < DV
    zero_row = jnp.zeros((1, LANES), F32)
    lasts = [
        [cumul_ref[0, pl.ds(n * BLK + BLK - 1, 1), :] for n in range(count)],
        [cumul_ref[1, pl.ds(n * BLK, 1), :] for n in range(count)],
    ]
    for n in range(count):
        rows = pl.ds(n * BLK, BLK)
        scale = KEY_CHANNELS ** (-0.5)
        q = block.rotate(q_ref[rows, :].astype(F32) * scale, block.tables(n))
        k = key_ref[rows, :]
        v = v_ref[rows, :].astype(F32)
        v_bd = jnp.concatenate(
            [jnp.where(wide_low, v, 0.0), jnp.where(wide_low, 0.0, v)], axis=0
        ).astype(BF16)
        scores = jnp.zeros((BLK, 2 * BLK), F32)
        q_ins, carried, reaches = [], [], []
        for d in range(2):
            cumul = cumul_ref[d, rows, :]
            at = BLK // 2 - 1 if d == 0 else BLK // 2
            middle = cumul[at : at + 1, :]
            offset = cumul - middle
            q_scaled = q * jnp.exp(offset)
            k_scaled = k * jnp.exp(-offset)
            both = dot(q_scaled.astype(BF16), spread(k_scaled, low).astype(BF16), NT)
            reach = row2 >= col2 if d == 0 else row2 <= col2
            scores = scores + jnp.where(reach, both, 0.0)
            q_ins.append(q_scaled * jnp.exp(middle))
            carried.append(spread(states_ref[d, n], low))
            passed = range(n) if d == 0 else range(n + 1, count)
            reaches.append(sum((lasts[d][m] for m in passed), zero_row))
        q_in = jnp.concatenate(q_ins, axis=1)
        within = dot(scores.astype(BF16), v_bd)
        across = dot(q_in.astype(BF16), jnp.concatenate(carried, axis=1).astype(BF16), NT)
        part_ref[rows, :] = within + across
        qdev_ref[rows, :] = (q_in * jnp.exp(jnp.concatenate(reaches, axis=1))).astype(BF16)

    expert = iota((EXPERTS, TOK), 0)
    picks = [routes_ref[k : k + 1, :] == expert for k in range(TOPK)]
    chosen = jnp.zeros((EXPERTS, TOK), F32)
    for pick in picks:
        chosen = chosen + pick.astype(F32)
    strict = (row < col).astype(BF16)
    before = dot(chosen.astype(BF16), strict)
    place = before + (CAP * expert).astype(F32)
    for k, pick in enumerate(picks):
        found = jnp.sum(jnp.where(pick, place, 0.0), axis=0, keepdims=True)
        slots_ref[k : k + 1, :] = found.astype(jnp.int32)


def compose_gathered(own, gathered_ref, length, shared_place=False):
    results = []
    for forward in (True, False):
        start, tail_at, first = (0, 2 * DV, 0) if forward else (DV, 2 * DV, 2)
        if shared_place:
            start, tail_at, first = 0, DV, 0
        state, logs = jnp.zeros((DV, LANES), F32), jnp.zeros((1, LANES), F32)
        inner, inner_logs = state, logs
        for step in range(length):
            k = step if forward else length - 1 - step
            here = own == k
            inner = jnp.where(here, state, inner)
            inner_logs = jnp.where(here, logs, inner_logs)
            tail = gathered_ref[k, pl.ds(tail_at, 16), :].astype(F32)
            log = tail[first : first + 1, :] + tail[first + 1 : first + 2, :]
            state = state * jnp.exp(log) + gathered_ref[k, pl.ds(start, DV), :].astype(F32)
            logs = logs + log
        results.append((state, logs, inner, inner_logs))
    return results


def plane_kernel(own_ref, gathered_ref, inner_ref, logs_ref, msg_ref):
    forward, backward = compose_gathered(own_ref[0], gathered_ref, XC)
    inner_ref[0] = forward[2]
    inner_ref[1] = backward[2]
    row_id = iota((8, LANES), 0)
    logs_ref[...] = jnp.where(row_id == 0, forward[3], jnp.where(row_id == 1, backward[3], 0.0))
    for j in range(Z):
        later = own_ref[1] < j
        msg_ref[j, pl.ds(0, DV), :] = jnp.where(later, forward[0], backward[0]).astype(BF16)
        logs = jnp.where(later, forward[1], backward[1])
        msg_ref[j, pl.ds(DV, 16), :] = split_rows([logs]).astype(BF16)


def readout_kernel(
    own_ref, gathered_ref, inner_ref, logs_ref, part_ref, qdev_ref, gate_ref, gain_ref, *out_refs
):
    forward, backward = compose_gathered(own_ref[1], gathered_ref, Z, shared_place=True)
    low = iota((DV, LANES), 1) < KEY_CHANNELS
    carry_f = inner_ref[0] + forward[2] * jnp.exp(logs_ref[0:1, :])
    carry_b = inner_ref[1] + backward[2] * jnp.exp(logs_ref[1:2, :])
    carried = jnp.concatenate([spread(carry_f, low), spread(carry_b, low)], axis=1).astype(BF16)
    for n in range(TP):
        rows = pl.ds(pl.multiple_of((own_ref[2] + n) % TP * TOK, TOK), TOK)
        attended = part_ref[rows, :] + dot(qdev_ref[rows, :], carried, NT)
        heads = []
        for h in range(2):
            head = attended[:, h * DV : (h + 1) * DV]
            heads.append(head * lax.rsqrt(jnp.mean(head * head, axis=-1, keepdims=True) + EPS))
        gate = gate_ref[rows, :].astype(F32)
        mixed = jnp.concatenate(heads, axis=1) * gain_ref[...] * (gate * jax.nn.sigmoid(gate))
        out_refs[n][...] = mixed.astype(BF16)


def normalize(x):
    return x * lax.rsqrt(jnp.mean(x * x, axis=-1, keepdims=True) + EPS)


def project_kernel(
    own_ref, slots_ref, mixed_0, mixed_1, mixed_2, mixed_3, weight_ref, stream_ref, mix_ref,
    ffn_ref, residual_ref, normed_ref, sent_ref, acc_ref, rows_ref,
):
    step = pl.program_id(0)

    @pl.when(step == 0)
    def _():
        acc_ref[...] = dot(mixed_0[...], weight_ref[...])
        sent_ref[...] = jnp.zeros_like(sent_ref)

    for n, mixed_ref in enumerate((mixed_1, mixed_2, mixed_3)):

        @pl.when(step == n + 1)
        def _(mixed_ref=mixed_ref):
            acc_ref[...] += dot(mixed_ref[...], weight_ref[...])

    @pl.when(step == TP - 1)
    def _():
        projected = normalize(acc_ref[...]) * mix_ref[...]
        residual = (stream_ref[...].astype(F32) + projected).astype(BF16)
        residual_ref[...] = residual
        normed = (normalize(residual.astype(F32)) * ffn_ref[...]).astype(BF16)
        normed_ref[...] = normed
        wide = normed.astype(F32)
        for j in range(COLS):
            rows_ref[pl.ds(j, TOK, stride=COLS), :] = wide[:, j * LANES : (j + 1) * LANES]

        def place(t, carry):
            line = rows_ref[pl.ds(pl.multiple_of(t * COLS, COLS), COLS), :].astype(BF16)
            for k in range(TOPK):
                sent_ref[slots_ref[k, t]] = line
            return carry

        lax.fori_loop(0, TOK, place, 0, unroll=8)


def pack_shared_kernel(gate_ref, up_ref, down_ref, after_ref, *out_refs):
    half = CHUNKS // 2
    for i in range(CHUNKS):
        rows = pl.ds(i * CHUNK, CHUNK)
        out_ref, at = out_refs[i // half], i % half
        out_ref[at, pl.ds(0, CHUNK), pl.ds(0, LANES)] = gate_ref[rows, :]
        out_ref[at, pl.ds(0, CHUNK), pl.ds(LANES, LANES)] = up_ref[rows, :]
        out_ref[at, pl.ds(CHUNK, LANES), :] = down_ref[:, rows]


def pack_shared(gate, up, down, after):
    return pl.pallas_call(
        pack_shared_kernel,
        out_shape=(shape((CHUNKS // 2, CHUNK + LANES, CHUNK), BF16),) * 2,
        in_specs=[vmem()] * 3 + [anywhere()],
        out_specs=(vmem(),) * 2,
        compiler_params=params(),
        cost_estimate=cost(1_000_000, 3_200_000),
        name="pack_shared",
    )(gate, up, down, after)


def silu(x):
    return x * jax.nn.sigmoid(x)


def expert_copies(gates, ups, downs, gate_ref, up_ref, down_ref, sems):
    copies = []
    for n in range(len(gates)):
        copies.append([
            pltpu.make_async_copy(gates[n], gate_ref.at[n], sems.at[0, n]),
            pltpu.make_async_copy(ups[n], up_ref.at[n], sems.at[1, n]),
        ])
        if len(downs) == len(gates):
            copies[n].append(pltpu.make_async_copy(downs[n], down_ref.at[n], sems.at[2, n]))
        else:
            half = down_ref.shape[1] // 2
            copies[n] += [
                pltpu.make_async_copy(
                    downs[h], down_ref.at[n, pl.ds(h * half, half)], sems.at[2 + h, n]
                )
                for h in range(2)
            ]
    for group in copies:
        for copy in group:
            copy.start()
    return copies


def expert_near_kernel(*refs):
    sent_ref, gates, ups, downs = refs[0], refs[1:4], refs[4:7], refs[7:10]
    rows_ref, acc_ref, sent, lines_ref, gate_ref, up_ref, down_ref, sent_sems, sems = refs[10:]
    part = SLOTS // PIECES
    arrivals = [
        pltpu.make_async_copy(
            sent_ref.at[pl.ds(p * part * COLS, part * COLS)],
            sent.at[pl.ds(p * part * COLS, part * COLS)],
            sent_sems.at[p],
        )
        for p in range(PIECES)
    ]
    for copy in arrivals:
        copy.start()
    copies = expert_copies(gates, ups, downs, gate_ref, up_ref, down_ref, sems)
    for p, copy in enumerate(arrivals):
        copy.wait()
        span = pl.ds(p * part * COLS, part * COLS)
        lines_ref[span, :] = sent[span, :].astype(F32)
        for j in range(COLS):
            rows_ref[pl.ds(p * part, part), j * LANES : (j + 1) * LANES] = lines_ref[
                pl.ds(p * part * COLS + j, part, stride=COLS), :
            ].astype(BF16)
    for n, group in enumerate(copies):
        group[0].wait()
        group[1].wait()
        rows = rows_ref[...]
        hidden = (silu(dot(rows, gate_ref[n])) * dot(rows, up_ref[n])).astype(BF16)
        group[2].wait()
        for j in range(CHUNKS):
            columns = pl.ds(j * CHUNK, CHUNK)
            product = dot(hidden, down_ref[n, :, columns])
            if n == 0:
                acc_ref[:, columns] = product
            else:
                acc_ref[:, columns] += product


def expert_far_kernel(*refs):
    rows_ref, acc_ref, gates, ups, downs, out_ref = refs[0], refs[1], refs[2:3], refs[3:4], refs[4:6], refs[6]
    sent, lines_ref, gate_ref, up_ref, down_ref, sems, out_sems = refs[7:]
    part = SLOTS // PIECES
    group = expert_copies(gates, ups, downs, gate_ref, up_ref, down_ref, sems)[0]
    for copy in group:
        copy.wait()
    outs = []
    for p in range(PIECES):
        block = pl.ds(p * part, part)
        rows = rows_ref[block, :]
        hidden = (silu(dot(rows, gate_ref[0])) * dot(rows, up_ref[0])).astype(BF16)
        for j in range(CHUNKS):
            columns = pl.ds(j * CHUNK, CHUNK)
            total = acc_ref[block, columns] + dot(hidden, down_ref[0, :, columns])
            for i in range(CHUNK // LANES):
                lines_ref[
                    pl.ds(p * part * COLS + j * (CHUNK // LANES) + i, part, stride=COLS), :
                ] = total[:, i * LANES : (i + 1) * LANES]
        span = pl.ds(p * part * COLS, part * COLS)
        sent[span, :] = lines_ref[span, :].astype(BF16)
        copy = pltpu.make_async_copy(sent.at[span], out_ref.at[span], out_sems.at[p])
        copy.start()
        outs.append(copy)
    for copy in outs:
        copy.wait()


def shared_kernel(*refs):
    rows_ref, shards, out_ref, weight_ref, sems = refs[0], refs[1:9], refs[9], refs[10], refs[11]
    half = CHUNKS // 2
    copies = [
        pltpu.make_async_copy(
            shards[2 * n + h], weight_ref.at[n, pl.ds(h * half, half)], sems.at[n, h]
        )
        for n in range(TP)
        for h in range(2)
    ]
    for copy in copies:
        copy.start()
    for n in range(TP):
        copies[2 * n].wait()
        copies[2 * n + 1].wait()
        joint = jnp.zeros((TOK, 2 * LANES), F32)
        for i in range(CHUNKS):
            columns = pl.ds(i * CHUNK, CHUNK)
            joint = joint + dot(rows_ref[:, columns], weight_ref[n, i, 0:CHUNK, :])
        hidden = (silu(joint[:, :LANES]) * joint[:, LANES:]).astype(BF16)
        for i in range(CHUNKS):
            columns = pl.ds(i * CHUNK, CHUNK)
            product = dot(hidden, weight_ref[n, i, CHUNK:, :])
            if n == 0:
                out_ref[:, columns] = product
            else:
                out_ref[:, columns] += product


def combine_kernel(
    slots_ref, weights_ref, back_ref, shared_ref, residual_ref, gain_ref, out_ref, lines_ref, mix_ref
):
    def gather(t, carry):
        line = jnp.zeros((COLS, LANES), F32)
        for k in range(TOPK):
            line = line + back_ref[slots_ref[k, t]].astype(F32) * weights_ref[k, t]
        lines_ref[pl.ds(pl.multiple_of(t * COLS, COLS), COLS), :] = line
        return carry

    lax.fori_loop(0, TOK, gather, 0, unroll=8)
    for j in range(COLS):
        columns = slice(j * LANES, (j + 1) * LANES)
        mix_ref[:, columns] = shared_ref[:, columns] + lines_ref[pl.ds(j, TOK, stride=COLS), :]
    out_ref[...] = (
        residual_ref[...].astype(F32) + normalize(mix_ref[...]) * gain_ref[...]
    ).astype(BF16)


def vmem():
    return pl.BlockSpec(memory_space=pltpu.VMEM)


def anywhere():
    return pl.BlockSpec(memory_space=pltpu.HBM)


def shift(array, hops):
    return lax.ppermute(array, "tp", [(i, (i + hops) % TP) for i in range(TP)])


def smem():
    return pl.BlockSpec(memory_space=pltpu.SMEM)


def params(mib=60, **extra):
    return pltpu.CompilerParams(vmem_limit_bytes=mib * 1024 * 1024, **extra)


def shape(dims, kind):
    return jax.ShapeDtypeStruct(dims, kind)


def cost(flops, moved):
    return pl.CostEstimate(flops=flops, bytes_accessed=moved, transcendentals=0)


def whole(dims):
    return pl.BlockSpec(dims, lambda i, *_: (0,) * len(dims))


def body(
    stream,
    queries,
    key_rows,
    values,
    out_gate,
    fwd_decay,
    bwd_decay,
    head_gain,
    out_proj,
    mix_gain,
    ffn_gain,
    moe_gain,
    routes,
    route_weight,
    expert_gate,
    expert_up,
    expert_down,
    shared_gate,
    shared_up,
    shared_down,
):
    own = jnp.stack([lax.axis_index(axes) for axes in (PLANE, "sp_0", "tp", "sp_2")])
    own = own.astype(jnp.int32)
    gate, up, down = expert_gate[0], expert_up[0], expert_down[0]
    gate_left = shift(gate, 1)
    gate_right = shift(gate, -1)
    up_left = shift(up, 1)
    up_right = shift(up, -1)

    tables = [jnp.asarray(table) for table in rope_tables()]
    msg, keys, cumuls, states = pl.pallas_call(
        states_kernel,
        out_shape=(
            shape((XC, MSG, LANES), BF16),
            shape((SPAN, LANES), F32),
            shape((2, SPAN, LANES), F32),
            shape((2, SPAN // BLK, DV, LANES), F32),
        ),
        in_specs=[smem()] + [vmem()] * 7,
        out_specs=(vmem(),) * 4,
        compiler_params=params(),
        cost_estimate=cost(200_000_000, 4_000_000),
        name="states",
    )(own, key_rows, values, fwd_decay, bwd_decay, *tables)
    in_plane = lax.all_to_all(msg, PLANE, split_axis=0, concat_axis=0, tiled=True)
    part, qdev, flat_slots = pl.pallas_call(
        attention_kernel,
        out_shape=(
            shape((SPAN, 2 * DV), F32),
            shape((SPAN, 2 * LANES), BF16),
            shape((TOPK, TOK), jnp.int32),
        ),
        in_specs=[smem()] + [vmem()] * 9,
        out_specs=(vmem(),) * 3,
        compiler_params=params(),
        cost_estimate=cost(400_000_000, 4_000_000),
        name="attention",
    )(own, queries, values, keys, cumuls, states, *tables, routes.T)
    inner, logs, msg = pl.pallas_call(
        plane_kernel,
        out_shape=(
            shape((2, DV, LANES), F32),
            shape((8, LANES), F32),
            shape((Z, HALF_MSG, LANES), BF16),
        ),
        in_specs=[smem(), vmem()],
        out_specs=(vmem(),) * 3,
        compiler_params=params(40),
        cost_estimate=cost(10_000_000, 1_000_000),
        name="plane",
    )(own, in_plane)
    planes = lax.all_to_all(msg, "sp_0", split_axis=0, concat_axis=0, tiled=True)
    mixed = pl.pallas_call(
        readout_kernel,
        out_shape=(shape((TOK, 2 * DV), BF16),) * TP,
        in_specs=[smem()] + [vmem()] * 7,
        out_specs=(vmem(),) * TP,
        compiler_params=params(60),
        cost_estimate=cost(100_000_000, 3_000_000),
        name="readout",
    )(
        own, planes, inner, logs, part, qdev, out_gate, head_gain.reshape(1, -1),
    )
    mixed = [shift(piece, n) if n else piece for n, piece in enumerate(mixed)]

    down_left = shift(down, 1)
    down_right = shift(down, -1)
    gate_far = shift(gate_left, 1)
    up_far = shift(up_right, -1)
    down_far_1 = shift(down_left[: down.shape[0] // 2], 1)
    down_far_2 = shift(down_right[down.shape[0] // 2 :], -1)

    residual, normed, sent = pl.pallas_call(
        project_kernel,
        out_shape=(
            shape((TOK, D), BF16),
            shape((TOK, D), BF16),
            shape((SLOTS, COLS, LANES), BF16),
        ),
        grid_spec=pltpu.PrefetchScalarGridSpec(
            num_scalar_prefetch=2,
            grid=(TP,),
            in_specs=[whole((TOK, 2 * DV))] * TP
            + [
                pl.BlockSpec((2 * DV, D), lambda i, own, _: ((own[2] + TP - i) % TP, 0)),
                whole((TOK, D)),
                whole((1, D)),
                whole((1, D)),
            ],
            out_specs=(whole((TOK, D)), whole((TOK, D)), whole((SLOTS, COLS, LANES))),
            scratch_shapes=[pltpu.VMEM((TOK, D), F32), pltpu.VMEM((TOK * COLS, LANES), F32)],
        ),
        compiler_params=params(59, dimension_semantics=("arbitrary",)),
        cost_estimate=cost(600_000_000, 8_000_000),
        name="project",
    )(own, flat_slots, *mixed, out_proj, stream, mix_gain.reshape(1, -1), ffn_gain.reshape(1, -1))

    arrived = lax.all_to_all(
        sent.reshape(EXPERTS, CAP * COLS, LANES), SP, split_axis=0, concat_axis=0, tiled=True
    )
    width = gate.shape[1]
    near = TP - 1
    rows, partial = pl.pallas_call(
        expert_near_kernel,
        out_shape=(shape((SLOTS, D), BF16), shape((SLOTS, D), F32)),
        in_specs=[anywhere()] * (1 + 3 * near),
        out_specs=(vmem(), vmem()),
        scratch_shapes=[
            pltpu.VMEM((SLOTS * COLS, LANES), BF16),
            pltpu.VMEM((SLOTS * COLS, LANES), F32),
            pltpu.VMEM((near, D, width), BF16),
            pltpu.VMEM((near, D, width), BF16),
            pltpu.VMEM((near, width, D), BF16),
            pltpu.SemaphoreType.DMA((PIECES,)),
            pltpu.SemaphoreType.DMA((3, near)),
        ],
        compiler_params=params(26),
        cost_estimate=cost(3_600_000_000, 16_000_000),
        name="experts_near",
    )(
        arrived.reshape(SLOTS * COLS, LANES),
        gate, gate_left, gate_right, up, up_left, up_right, down, down_left, down_right,
    )
    done = pl.pallas_call(
        expert_far_kernel,
        out_shape=shape((SLOTS * COLS, LANES), BF16),
        in_specs=[vmem(), vmem()] + [anywhere()] * 4,
        out_specs=anywhere(),
        scratch_shapes=[
            pltpu.VMEM((SLOTS * COLS, LANES), BF16),
            pltpu.VMEM((SLOTS * COLS, LANES), F32),
            pltpu.VMEM((1, D, width), BF16),
            pltpu.VMEM((1, D, width), BF16),
            pltpu.VMEM((1, width, D), BF16),
            pltpu.SemaphoreType.DMA((4, 1)),
            pltpu.SemaphoreType.DMA((PIECES,)),
        ],
        compiler_params=params(20),
        cost_estimate=cost(1_200_000_000, 8_000_000),
        name="experts_far",
    )(rows, partial, gate_far, up_far, down_far_1, down_far_2)
    back = lax.all_to_all(
        done.reshape(EXPERTS, CAP * COLS, LANES), SP, split_axis=0, concat_axis=0, tiled=True
    )
    packed = pack_shared(shared_gate, shared_up, shared_down, residual)
    shared_left, shared_right = [None, None], [None, None]
    for h in range(2):
        shared_left[h] = shift(packed[h], 1)
        shared_right[h] = shift(packed[h], -1)
    shared_far_0 = shift(shared_left[0], 1)
    shared_far_1 = shift(shared_right[1], -1)
    shared = pl.pallas_call(
        shared_kernel,
        out_shape=shape((TOK, D), F32),
        in_specs=[vmem()] + [anywhere()] * 8,
        out_specs=vmem(),
        scratch_shapes=[
            pltpu.VMEM((TP, CHUNKS, CHUNK + LANES, CHUNK), BF16),
            pltpu.SemaphoreType.DMA((TP, 2)),
        ],
        compiler_params=params(60),
        cost_estimate=cost(800_000_000, 8_000_000),
        name="shared",
    )(normed, *packed, *shared_left, *shared_right, shared_far_0, shared_far_1)
    return pl.pallas_call(
        combine_kernel,
        out_shape=shape((TOK, D), BF16),
        in_specs=[smem(), smem()] + [vmem()] * 4,
        out_specs=vmem(),
        scratch_shapes=[pltpu.VMEM((TOK * COLS, LANES), F32), pltpu.VMEM((TOK, D), F32)],
        compiler_params=params(40),
        cost_estimate=cost(5_000_000, 4_000_000),
        name="combine",
    )(
        flat_slots, route_weight.T, back.reshape(SLOTS, COLS, LANES),
        shared, residual, moe_gain.reshape(1, -1),
    )


def solution(mesh):
    finer = Mesh(mesh.devices.reshape(8, 4, 2, mesh.shape["tp"]), ("sp_0", "sp_1", "sp_2", "tp"))
    placed = (
        P(SP_TP, None),
        P(SP, "tp"),
        P(SP, "tp"),
        P(SP, "tp"),
        P(SP, "tp"),
        P(SP, "tp"),
        P(SP, "tp"),
        P("tp"),
        P(),
        P(),
        P(),
        P(),
        P(SP_TP, None),
        P(SP_TP, None),
        P(SP, None, "tp"),
        P(SP, None, "tp"),
        P(SP, "tp", None),
        P(None, "tp"),
        P(None, "tp"),
        P("tp", None),
    )

    return jax.shard_map(
        body, mesh=finer, in_specs=placed, out_specs=P(SP_TP, None), check_vma=False
    )
```

time: 280 us -> 260 us (0.929)
  blocking collectives: 36.3 us -> 14.9 us
  waiting for transfers between devices: 147 us -> 134 us
  starting transfers between devices: 40.3 us -> 52.2 us
  local copies, waits for them, and re-layouts: 10.9 us -> 14.4 us
    ppermute x17 -> x19, waiting for transfers between devices: 147 us -> 125 us  [shift(): return lax.ppermute(array, 'tp', [(i, (i + hops) % TP) for i in range(TP)])]
    all_gather x1 -> x0, blocking collectives: 14.6 us -> none  [body(): in_plane = lax.all_gather(msg, PLANE, axis=0)]
    all_to_all x0 -> x1, waiting for transfers between devices: none -> 9.7 us  [body(): lax.all_to_all(msg, 'sp_0', split_axis=0, concat_axis=0, tiled=True)]
    all_to_all x0 -> x1, starting transfers between devices: none -> 7.61 us  [body(): lax.all_to_all(msg, 'sp_0', split_axis=0, concat_axis=0, tiled=True)]
    all_to_all x1, blocking collectives: 21.7 us -> 14.9 us  [body(): lax.all_to_all(msg, PLANE, split_axis=0, concat_axis=0, tiled=True)]
    unnamed x36 -> x52, local copies, waits for them, and re-layouts: 8.04 us -> 12.7 us
    ppermute x17 -> x19, starting transfers between devices: 24.8 us -> 28.6 us  [shift(): return lax.ppermute(array, 'tp', [(i, (i + hops) % TP) for i in range(TP)])]
    pallas_call x2 -> x4, Pallas kernels: 15.4 us -> 18.4 us  [the longest x1 7.07 us: body(): pl.pallas_call(expert_near_kernel, out_shape=(shape((SLOTS, D), BF16), sh...]
  transfers between devices with their start and end apart: 19 -> 22, of which waited for: 10 -> 10; matrix products, arithmetic and copies ran while one was open for 1% -> 1% of each run, Pallas kernels for 3% -> 7%
where the time goes in v3:
time: 260 us; the launch traced here: 259 us
  waiting for transfers between devices  134 us (52%)
  starting transfers between devices  52.2 us (20%)
  Pallas kernels  41.9 us (16%)
  blocking collectives  14.9 us (6%)
  local copies, waits for them, and re-layouts  14.4 us (6%)
    ppermute x19, waiting for transfers between devices, shift(): return lax.ppermute(array, 'tp', [(i, (i + hops) % TP) for i in range(TP)])  125 us
    ppermute x19, starting transfers between devices, shift(): return lax.ppermute(array, 'tp', [(i, (i + hops) % TP) for i in range(TP)])  28.6 us
    all_to_all x1, blocking collectives, body(): lax.all_to_all(msg, PLANE, split_axis=0, concat_axis=0, tiled=True)  14.9 us
    unnamed x52, local copies, waits for them, and re-layouts  12.7 us
    all_to_all x1, starting transfers between devices, body(): lax.all_to_all(done.reshape(EXPERTS, CAP * COLS, LANES), SP, split_axis=0...  10.4 us
    all_to_all x1, waiting for transfers between devices, body(): lax.all_to_all(msg, 'sp_0', split_axis=0, concat_axis=0, tiled=True)  9.7 us
    all_to_all x1, starting transfers between devices, body(): lax.all_to_all(msg, 'sp_0', split_axis=0, concat_axis=0, tiled=True)  7.61 us
    pallas_call x1, Pallas kernels, body(): pl.pallas_call(project_kernel, out_shape=(shape((TOK, D), BF16), shape((T...  7.39 us
  transfers between devices with their start and end apart: 22, of which 10 were waited for; matrix products, arithmetic and copies ran while one was open for 1% of the time, Pallas kernels for 7%

profile of v3, /device:TPU:2, one launch (start us, length us, event | category | flops | bytes accessed | tf_op | source)
XLA Modules:
  0.0 258.6 jit_solution(10765756382049946487)
XLA Ops:
  0.6 3.1 %states.1 = (bf16[8,272,128]{2,1,0:T(8,128)(2,1)}, f32[512,128]{1,0:T(8,128)}, f32[2,512,128]{2,1,0:T(8,128)}, f32[2,4,128,128]{3,2,1,0:T(8,128)}) custom-call(s32[4]{0:T(128)} %pad_add_fusion.own_ref, bf16[512,128]{1,0:T(8,128)(2,1)} %k_ref.1, bf16[512,256]{1,0:T(8,128)(2,1)} %v_ref.3, f32[512,128]{1,0:T(8,128)} %fd_ref.1, f32[512,128]{1,0:T(8,128)} %bd_ref.1, ...), custom_call_target="tpu_custom_call" | custom-call | flops 200000000 | bytes 4000000 | tf_op jit(solution)/shard_map/states/pallas_call | solution.py:540
  3.7 14.9 %all_to_all.20.gathered_ref = bf16[8,272,128]{2,1,0:T(8,128)(2,1)S(1)} all-to-all(bf16[8,272,128]{2,1,0:T(8,128)(2,1)} %get-tuple-element.30), channel_id=1, replica_groups=mesh['sp_0'=8,'sp_1'=4,'sp_2'=2,'tp'=4] {'sp_1','sp_2'}, dimensions={0} | all-to-all | bytes 1114112 | tf_op jit(solution)/shard_map/all_to_all | solution.py:554
  21.3 7.6 %all-to-all-start.1 = ((bf16[8,144,128]{2,1,0:T(8,128)(2,1)}), bf16[8,144,128]{2,1,0:T(8,128)(2,1)S(1)}, u32[]{:S(2)}, u32[]{:S(2)}) async-start(bf16[8,144,128]{2,1,0:T(8,128)(2,1)} %get-tuple-element.31), calls=%async_computation.1 | async-start | bytes 589824 | tf_op jit(solution)/shard_map/all_to_all | solution.py:581
  29.0 3.0 %attention.1 = (f32[512,256]{1,0:T(8,128)}, bf16[512,256]{1,0:T(8,128)(2,1)}, s32[2,128]{1,0:T(2,128)}) custom-call(s32[4]{0:T(128)} %pad_add_fusion.own_ref, bf16[512,128]{1,0:T(8,128)(2,1)} %q_ref.1, bf16[512,256]{1,0:T(8,128)(2,1)} %v_ref.3, f32[512,128]{1,0:T(8,128)} %get-tuple-element.26.key_ref, f32[2,512,128]{2,1,0:T(8,128)} %get-tuple-element.27.cumul_ref, ...), custom_call_target="tpu_custom_call" | custom-call | flops 400000000 | bytes 4000000 | tf_op jit(solution)/shard_map/attention/pallas_call | solution.py:555
  31.9 9.7 %all-to-all-done.1.gathered_ref = bf16[8,144,128]{2,1,0:T(8,128)(2,1)S(1)} async-done(((bf16[8,144,128]{2,1,0:T(8,128)(2,1)}), bf16[8,144,128]{2,1,0:T(8,128)(2,1)S(1)}, u32[]{:S(2)}, u32[]{:S(2)}) %all-to-all-start.1) | async-done | bytes 294944 | tf_op jit(solution)/shard_map/all_to_all | solution.py:581
  46.5 2.9 %collective-permute-start.1 = (bf16[128,256]{1,0:T(8,128)(2,1)}, bf16[128,256]{1,0:T(8,128)(2,1)S(1)}, u32[]{:S(2)}, u32[]{:S(2)}) collective-permute-start(bf16[128,256]{1,0:T(8,128)(2,1)} %get-tuple-element.38), channel_id=1, source_target_pairs={{0,2},{1,3},{2,0},{3,1},{4,6},{5,7},{6,4},{7,5},{8,10},{9,11},{10,... | collective-permute-start | bytes 196616 | tf_op jit(solution)/shard_map/ppermute | solution.py:486
  54.5 7.4 %project.1 = (bf16[128,2048]{1,0:T(8,128)(2,1)}, bf16[128,2048]{1,0:T(8,128)(2,1)}, bf16[384,16,128]{2,1,0:T(8,128)(2,1)}) custom-call(s32[4]{0:T(128)} %pad_add_fusion.own_ref, s32[2,128]{1,0:T(2,128)} %get-tuple-element.29.slots_ref, bf16[128,256]{1,0:T(8,128)(2,1)} %get-tuple-element.36.mixed_0, bf16[128,256]{1,0:T(8,128)(2,1)} %copy-done.23, ...), custom_call_target="tpu_custom_call" | custom-call | flops 600000000 | bytes 8000000 | tf_op jit(solution)/shard_map/project/pallas_call | solution.py:602
  61.9 5.6 %all-to-all-start.2 = ((bf16[64,96,128]{2,1,0:T(8,128)(2,1)}), bf16[64,96,128]{2,1,0:T(8,128)(2,1)S(1)}, u32[]{:S(2)}, u32[]{:S(2)}) async-start(bf16[64,96,128]{2,1,0:T(8,128)(2,1)} %bitcast.21), calls=%async_computation.2 | async-start | bytes 3145728 | tf_op jit(solution)/shard_map/all_to_all | solution.py:627
  67.9 2.9 %collective-permute-start.6 = (bf16[2048,256]{1,0:T(8,128)(2,1)}, bf16[2048,256]{1,0:T(8,128)(2,1)}, u32[]{:S(2)}, u32[]{:S(2)}) collective-permute-start(bf16[2048,256]{1,0:T(8,128)(2,1)} %bitcast.12.refs_4_), channel_id=1, source_target_pairs={{0,3},{1,0},{2,1},{3,2},{4,7},{5,4},{6,5},{7,6},{8,11},{9,8},{10,9... | collective-permute-start | bytes 3145736 | tf_op jit(solution)/shard_map/ppermute | solution.py:486
  70.8 3.2 %collective-permute-start.8 = (bf16[256,2048]{1,0:T(8,128)(2,1)}, bf16[256,2048]{1,0:T(8,128)(2,1)S(1)}, u32[]{:S(2)}, u32[]{:S(2)}) collective-permute-start(bf16[256,2048]{1,0:T(8,128)(2,1)} %bitcast.13.refs_7_), channel_id=1, source_target_pairs={{0,3},{1,0},{2,1},{3,2},{4,7},{5,4},{6,5},{7,6},{8,11},{9,8},{10,9... | collective-permute-start | bytes 3145736 | tf_op jit(solution)/shard_map/ppermute | solution.py:486
  74.2 20.9 %collective-permute-done.3.refs_2_ = bf16[2048,256]{1,0:T(8,128)(2,1)} collective-permute-done((bf16[2048,256]{1,0:T(8,128)(2,1)}, bf16[2048,256]{1,0:T(8,128)(2,1)}, u32[]{:S(2)}, u32[]{:S(2)}) %collective-permute-start.3) | collective-permute-done | bytes 1048608 | tf_op jit(solution)/shard_map/ppermute | solution.py:486
  95.8 21.6 %collective-permute-done.7.refs_8_ = bf16[256,2048]{1,0:T(8,128)(2,1)S(1)} collective-permute-done((bf16[256,2048]{1,0:T(8,128)(2,1)}, bf16[256,2048]{1,0:T(8,128)(2,1)S(1)}, u32[]{:S(2)}, u32[]{:S(2)}) %collective-permute-start.7) | collective-permute-done | bytes 1048608 | tf_op jit(solution)/shard_map/ppermute | solution.py:486
  121.2 18.4 %collective-permute-done.4.refs_3_ = bf16[2048,256]{1,0:T(8,128)(2,1)S(1)} collective-permute-done((bf16[2048,256]{1,0:T(8,128)(2,1)}, bf16[2048,256]{1,0:T(8,128)(2,1)S(1)}, u32[]{:S(2)}, u32[]{:S(2)}) %collective-permute-start.4) | collective-permute-done | bytes 1048608 | tf_op jit(solution)/shard_map/ppermute | solution.py:486
  140.6 3.6 %collective-permute-start.12 = (bf16[128,2048]{1,0:T(8,128)(2,1)}, bf16[128,2048]{1,0:T(8,128)(2,1)}, u32[]{:S(2)}, u32[]{:S(2)}) collective-permute-start(bf16[128,2048]{1,0:T(8,128)(2,1)} %slice.9), channel_id=1, source_target_pairs={{0,3},{1,0},{2,1},{3,2},{4,7},{5,4},{6,5},{7,6},{8,11},{9,8},{10,9... | collective-permute-start | bytes 1572872 | tf_op jit(solution)/shard_map/ppermute | solution.py:486
  150.2 7.1 %experts_near.1 = (bf16[384,2048]{1,0:T(8,128)(2,1)S(1)}, f32[384,2048]{1,0:T(8,128)S(1)}) custom-call(bf16[6144,128]{1,0:T(8,128)(2,1)S(1)} %bitcast.18, bf16[2048,256]{1,0:T(8,128)(2,1)} %bitcast.11.refs_1_, bf16[2048,256]{1,0:T(8,128)(2,1)} %collective-permute-done.3.refs_2_, bf16[2048,256]{1,0:T(8,128)(2,1)S(1)} %copy-done.13, ...), custom_call_target="tpu_custom_call" | custom-call | flops 3600000000 | bytes 16000000 | tf_op jit(solution)/shard_map/experts_near/pallas_call | solution.py:632
  157.3 15.5 %collective-permute-done.11.refs_4_ = bf16[128,2048]{1,0:T(8,128)(2,1)S(1)} collective-permute-done((bf16[128,2048]{1,0:T(8,128)(2,1)}, bf16[128,2048]{1,0:T(8,128)(2,1)S(1)}, u32[]{:S(2)}, u32[]{:S(2)}) %collective-permute-start.11) | collective-permute-done | bytes 524320 | tf_op jit(solution)/shard_map/ppermute | solution.py:486
  172.8 5.6 %experts_far.1 = bf16[6144,128]{1,0:T(8,128)(2,1)} custom-call(bf16[384,2048]{1,0:T(8,128)(2,1)S(1)} %get-tuple-element.41.refs_0_, f32[384,2048]{1,0:T(8,128)S(1)} %get-tuple-element.42.refs_1_, bf16[2048,256]{1,0:T(8,128)(2,1)S(1)} %collective-permute-done.9.refs_2_, bf16[2048,256]{1,0:T(8,128)(2,1)} %collective-permute-done.10.refs_3_, ...), custom_call_target="tpu_custom_call" | custom-call | flops 1200000000 | bytes 8000000 | tf_op jit(solution)/shard_map/experts_far/pallas_call | solution.py:653
  178.4 10.4 %all-to-all-start.3 = ((bf16[64,96,128]{2,1,0:T(8,128)(2,1)}), bf16[64,96,128]{2,1,0:T(8,128)(2,1)S(1)}, u32[]{:S(2)}, u32[]{:S(2)}) async-start(bf16[64,96,128]{2,1,0:T(8,128)(2,1)} %bitcast.14), calls=%async_computation.3 | async-start | bytes 3145728 | tf_op jit(solution)/shard_map/all_to_all | solution.py:671
  194.7 3.2 %collective-permute-start.15 = (bf16[4,384,256]{2,1,0:T(8,128)(2,1)}, bf16[4,384,256]{2,1,0:T(8,128)(2,1)S(1)}, u32[]{:S(2)}, u32[]{:S(2)}) collective-permute-start(bf16[4,384,256]{2,1,0:T(8,128)(2,1)} %get-tuple-element.45.refs_1_), channel_id=1, source_target_pairs={{0,3},{1,0},{2,1},{3,2},{4,7},{5,4},{6,5},{7,6},{8,11},{9,8},{10,9... | collective-permute-start | bytes 2359304 | tf_op jit(solution)/shard_map/ppermute | solution.py:486
  197.9 15.4 %collective-permute-done.13.refs_3_ = bf16[4,384,256]{2,1,0:T(8,128)(2,1)S(1)} collective-permute-done((bf16[4,384,256]{2,1,0:T(8,128)(2,1)}, bf16[4,384,256]{2,1,0:T(8,128)(2,1)S(1)}, u32[]{:S(2)}, u32[]{:S(2)}) %collective-permute-start.13) | collective-permute-done | bytes 786464 | tf_op jit(solution)/shard_map/ppermute | solution.py:486
  213.3 3.2 %collective-permute-start.18 = (bf16[4,384,256]{2,1,0:T(8,128)(2,1)S(1)}, bf16[4,384,256]{2,1,0:T(8,128)(2,1)S(1)}, u32[]{:S(2)}, u32[]{:S(2)}) collective-permute-start(bf16[4,384,256]{2,1,0:T(8,128)(2,1)S(1)} %collective-permute-done.16.refs_6_), channel_id=1, source_target_pairs={{0,3},{1,0},{2,1},{3,2},{4,7},{5,4},{6,5},{7,6},{8,11},{9,8},{10,9... | collective-permute-start | bytes 2359304 | tf_op jit(solution)/shard_map/ppermute | solution.py:486
  216.6 13.6 %collective-permute-done.14.refs_4_ = bf16[4,384,256]{2,1,0:T(8,128)(2,1)S(1)} collective-permute-done((bf16[4,384,256]{2,1,0:T(8,128)(2,1)}, bf16[4,384,256]{2,1,0:T(8,128)(2,1)S(1)}, u32[]{:S(2)}, u32[]{:S(2)}) %collective-permute-start.14) | collective-permute-done | bytes 786464 | tf_op jit(solution)/shard_map/ppermute | solution.py:486
  230.2 16.1 %collective-permute-done.17.refs_7_ = bf16[4,384,256]{2,1,0:T(8,128)(2,1)S(1)} collective-permute-done((bf16[4,384,256]{2,1,0:T(8,128)(2,1)S(1)}, bf16[4,384,256]{2,1,0:T(8,128)(2,1)S(1)}, u32[]{:S(2)}, u32[]{:S(2)}) %collective-permute-start.17) | collective-permute-done | bytes 786464 | tf_op jit(solution)/shard_map/ppermute | solution.py:486
  248.2 6.5 %shared.1.shared_ref = f32[128,2048]{1,0:T(8,128)} custom-call(bf16[128,2048]{1,0:T(8,128)(2,1)} %get-tuple-element.43.refs_0_, bf16[4,384,256]{2,1,0:T(8,128)(2,1)} %get-tuple-element.45.refs_1_, bf16[4,384,256]{2,1,0:T(8,128)(2,1)} %get-tuple-element.46.refs_2_, bf16[4,384,256]{2,1,0:T(8,128)(2,1)} %copy-done.17, bf16[4,384,256]{2,1,0:T(8,128)(2,1)} %copy-done.19, ...), custom_call_target="tpu_custom_call" | custom-call | flops 800000000 | bytes 8000000 | tf_op jit(solution)/shard_map/shared/pallas_call | solution.py:681
  (86 shorter events, 36.9 us)
Async XLA Ops:
  21.3 20.3 %all-to-all-start.1 = ((bf16[8,144,128]{2,1,0:T(8,128)(2,1)}), bf16[8,144,128]{2,1,0:T(8,128)(2,1)S(1)}, u32[]{:S(2)}, u32[]{:S(2)}) async-start(bf16[8,144,128]{2,1,0:T(8,128)(2,1)} %get-tuple-element.31), calls=%async_computation.1 | async-start | bytes 589824 | tf_op jit(solution)/shard_map/all_to_all | solution.py:581
  44.9 5.8 %collective-permute-start = (bf16[128,256]{1,0:T(8,128)(2,1)}, bf16[128,256]{1,0:T(8,128)(2,1)S(1)}, u32[]{:S(2)}, u32[]{:S(2)}) collective-permute-start(bf16[128,256]{1,0:T(8,128)(2,1)} %get-tuple-element.37), channel_id=1, source_target_pairs={{0,1},{1,2},{2,3},{3,0},{4,5},{5,6},{6,7},{7,4},{8,9},{9,10},{10,1... | collective-permute-start | bytes 196616 | tf_op jit(solution)/shard_map/ppermute | solution.py:486
  46.5 6.1 %collective-permute-start.1 = (bf16[128,256]{1,0:T(8,128)(2,1)}, bf16[128,256]{1,0:T(8,128)(2,1)S(1)}, u32[]{:S(2)}, u32[]{:S(2)}) collective-permute-start(bf16[128,256]{1,0:T(8,128)(2,1)} %get-tuple-element.38), channel_id=1, source_target_pairs={{0,2},{1,3},{2,0},{3,1},{4,6},{5,7},{6,4},{7,5},{8,10},{9,11},{10,... | collective-permute-start | bytes 196616 | tf_op jit(solution)/shard_map/ppermute | solution.py:486
  49.4 4.5 %collective-permute-start.2 = (bf16[128,256]{1,0:T(8,128)(2,1)}, bf16[128,256]{1,0:T(8,128)(2,1)S(1)}, u32[]{:S(2)}, u32[]{:S(2)}) collective-permute-start(bf16[128,256]{1,0:T(8,128)(2,1)} %get-tuple-element.39), channel_id=1, source_target_pairs={{0,3},{1,0},{2,1},{3,2},{4,7},{5,4},{6,5},{7,6},{8,11},{9,8},{10,9... | collective-permute-start | bytes 196616 | tf_op jit(solution)/shard_map/ppermute | solution.py:486
  61.9 83.4 %all-to-all-start.2 = ((bf16[64,96,128]{2,1,0:T(8,128)(2,1)}), bf16[64,96,128]{2,1,0:T(8,128)(2,1)S(1)}, u32[]{:S(2)}, u32[]{:S(2)}) async-start(bf16[64,96,128]{2,1,0:T(8,128)(2,1)} %bitcast.21), calls=%async_computation.2 | async-start | bytes 3145728 | tf_op jit(solution)/shard_map/all_to_all | solution.py:627
  67.5 27.6 %collective-permute-start.3 = (bf16[2048,256]{1,0:T(8,128)(2,1)}, bf16[2048,256]{1,0:T(8,128)(2,1)}, u32[]{:S(2)}, u32[]{:S(2)}) collective-permute-start(bf16[2048,256]{1,0:T(8,128)(2,1)} %bitcast.11.refs_1_), channel_id=1, source_target_pairs={{0,1},{1,2},{2,3},{3,0},{4,5},{5,6},{6,7},{7,4},{8,9},{9,10},{10,1... | collective-permute-start | bytes 3145736 | tf_op jit(solution)/shard_map/ppermute | solution.py:486
  67.9 27.2 %collective-permute-start.6 = (bf16[2048,256]{1,0:T(8,128)(2,1)}, bf16[2048,256]{1,0:T(8,128)(2,1)}, u32[]{:S(2)}, u32[]{:S(2)}) collective-permute-start(bf16[2048,256]{1,0:T(8,128)(2,1)} %bitcast.12.refs_4_), channel_id=1, source_target_pairs={{0,3},{1,0},{2,1},{3,2},{4,7},{5,4},{6,5},{7,6},{8,11},{9,8},{10,9... | collective-permute-start | bytes 3145736 | tf_op jit(solution)/shard_map/ppermute | solution.py:486
  70.8 46.7 %collective-permute-start.7 = (bf16[256,2048]{1,0:T(8,128)(2,1)}, bf16[256,2048]{1,0:T(8,128)(2,1)S(1)}, u32[]{:S(2)}, u32[]{:S(2)}) collective-permute-start(bf16[256,2048]{1,0:T(8,128)(2,1)} %bitcast.13.refs_7_), channel_id=1, source_target_pairs={{0,1},{1,2},{2,3},{3,0},{4,5},{5,6},{6,7},{7,4},{8,9},{9,10},{10,1... | collective-permute-start | bytes 3145736 | tf_op jit(solution)/shard_map/ppermute | solution.py:486
  70.8 48.9 %collective-permute-start.8 = (bf16[256,2048]{1,0:T(8,128)(2,1)}, bf16[256,2048]{1,0:T(8,128)(2,1)S(1)}, u32[]{:S(2)}, u32[]{:S(2)}) collective-permute-start(bf16[256,2048]{1,0:T(8,128)(2,1)} %bitcast.13.refs_7_), channel_id=1, source_target_pairs={{0,3},{1,0},{2,1},{3,2},{4,7},{5,4},{6,5},{7,6},{8,11},{9,8},{10,9... | collective-permute-start | bytes 3145736 | tf_op jit(solution)/shard_map/ppermute | solution.py:486
  74.0 65.6 %collective-permute-start.4 = (bf16[2048,256]{1,0:T(8,128)(2,1)}, bf16[2048,256]{1,0:T(8,128)(2,1)S(1)}, u32[]{:S(2)}, u32[]{:S(2)}) collective-permute-start(bf16[2048,256]{1,0:T(8,128)(2,1)} %bitcast.11.refs_1_), channel_id=1, source_target_pairs={{0,3},{1,0},{2,1},{3,2},{4,7},{5,4},{6,5},{7,6},{8,11},{9,8},{10,9... | collective-permute-start | bytes 3145736 | tf_op jit(solution)/shard_map/ppermute | solution.py:486
  95.1 49.1 %collective-permute-start.5 = (bf16[2048,256]{1,0:T(8,128)(2,1)}, bf16[2048,256]{1,0:T(8,128)(2,1)S(1)}, u32[]{:S(2)}, u32[]{:S(2)}) collective-permute-start(bf16[2048,256]{1,0:T(8,128)(2,1)} %bitcast.12.refs_4_), channel_id=1, source_target_pairs={{0,1},{1,2},{2,3},{3,0},{4,5},{5,6},{6,7},{7,4},{8,9},{9,10},{10,1... | collective-permute-start | bytes 3145736 | tf_op jit(solution)/shard_map/ppermute | solution.py:486
  95.1 77.7 %collective-permute-start.9 = (bf16[2048,256]{1,0:T(8,128)(2,1)}, bf16[2048,256]{1,0:T(8,128)(2,1)S(1)}, u32[]{:S(2)}, u32[]{:S(2)}) collective-permute-start(bf16[2048,256]{1,0:T(8,128)(2,1)} %collective-permute-done.3.refs_2_), channel_id=1, source_target_pairs={{0,1},{1,2},{2,3},{3,0},{4,5},{5,6},{6,7},{7,4},{8,9},{9,10},{10,1... | collective-permute-start | bytes 3145736 | tf_op jit(solution)/shard_map/ppermute | solution.py:486
  117.5 55.3 %collective-permute-start.10 = (bf16[2048,256]{1,0:T(8,128)(2,1)}, bf16[2048,256]{1,0:T(8,128)(2,1)}, u32[]{:S(2)}, u32[]{:S(2)}) collective-permute-start(bf16[2048,256]{1,0:T(8,128)(2,1)} %collective-permute-done.6.refs_6_), channel_id=1, source_target_pairs={{0,3},{1,0},{2,1},{3,2},{4,7},{5,4},{6,5},{7,6},{8,11},{9,8},{10,9... | collective-permute-start | bytes 3145736 | tf_op jit(solution)/shard_map/ppermute | solution.py:486
  119.7 53.1 %collective-permute-start.11 = (bf16[128,2048]{1,0:T(8,128)(2,1)}, bf16[128,2048]{1,0:T(8,128)(2,1)S(1)}, u32[]{:S(2)}, u32[]{:S(2)}) collective-permute-start(bf16[128,2048]{1,0:T(8,128)(2,1)} %slice.8), channel_id=1, source_target_pairs={{0,1},{1,2},{2,3},{3,0},{4,5},{5,6},{6,7},{7,4},{8,9},{9,10},{10,1... | collective-permute-start | bytes 1572872 | tf_op jit(solution)/shard_map/ppermute | solution.py:486
  140.6 32.1 %collective-permute-start.12 = (bf16[128,2048]{1,0:T(8,128)(2,1)}, bf16[128,2048]{1,0:T(8,128)(2,1)}, u32[]{:S(2)}, u32[]{:S(2)}) collective-permute-start(bf16[128,2048]{1,0:T(8,128)(2,1)} %slice.9), channel_id=1, source_target_pairs={{0,3},{1,0},{2,1},{3,2},{4,7},{5,4},{6,5},{7,6},{8,11},{9,8},{10,9... | collective-permute-start | bytes 1572872 | tf_op jit(solution)/shard_map/ppermute | solution.py:486
  178.4 76.3 %all-to-all-start.3 = ((bf16[64,96,128]{2,1,0:T(8,128)(2,1)}), bf16[64,96,128]{2,1,0:T(8,128)(2,1)S(1)}, u32[]{:S(2)}, u32[]{:S(2)}) async-start(bf16[64,96,128]{2,1,0:T(8,128)(2,1)} %bitcast.14), calls=%async_computation.3 | async-start | bytes 3145728 | tf_op jit(solution)/shard_map/all_to_all | solution.py:671
  191.5 21.8 %collective-permute-start.13 = (bf16[4,384,256]{2,1,0:T(8,128)(2,1)}, bf16[4,384,256]{2,1,0:T(8,128)(2,1)S(1)}, u32[]{:S(2)}, u32[]{:S(2)}) collective-permute-start(bf16[4,384,256]{2,1,0:T(8,128)(2,1)} %get-tuple-element.45.refs_1_), channel_id=1, source_target_pairs={{0,1},{1,2},{2,3},{3,0},{4,5},{5,6},{6,7},{7,4},{8,9},{9,10},{10,1... | collective-permute-start | bytes 2359304 | tf_op jit(solution)/shard_map/ppermute | solution.py:486
  192.3 21.0 %collective-permute-start.16 = (bf16[4,384,256]{2,1,0:T(8,128)(2,1)}, bf16[4,384,256]{2,1,0:T(8,128)(2,1)S(1)}, u32[]{:S(2)}, u32[]{:S(2)}) collective-permute-start(bf16[4,384,256]{2,1,0:T(8,128)(2,1)} %get-tuple-element.46.refs_2_), channel_id=1, source_target_pairs={{0,3},{1,0},{2,1},{3,2},{4,7},{5,4},{6,5},{7,6},{8,11},{9,8},{10,9... | collective-permute-start | bytes 2359304 | tf_op jit(solution)/shard_map/ppermute | solution.py:486
  194.7 35.5 %collective-permute-start.14 = (bf16[4,384,256]{2,1,0:T(8,128)(2,1)}, bf16[4,384,256]{2,1,0:T(8,128)(2,1)S(1)}, u32[]{:S(2)}, u32[]{:S(2)}) collective-permute-start(bf16[4,384,256]{2,1,0:T(8,128)(2,1)} %get-tuple-element.46.refs_2_), channel_id=1, source_target_pairs={{0,1},{1,2},{2,3},{3,0},{4,5},{5,6},{6,7},{7,4},{8,9},{9,10},{10,1... | collective-permute-start | bytes 2359304 | tf_op jit(solution)/shard_map/ppermute | solution.py:486
  194.7 35.5 %collective-permute-start.15 = (bf16[4,384,256]{2,1,0:T(8,128)(2,1)}, bf16[4,384,256]{2,1,0:T(8,128)(2,1)S(1)}, u32[]{:S(2)}, u32[]{:S(2)}) collective-permute-start(bf16[4,384,256]{2,1,0:T(8,128)(2,1)} %get-tuple-element.45.refs_1_), channel_id=1, source_target_pairs={{0,3},{1,0},{2,1},{3,2},{4,7},{5,4},{6,5},{7,6},{8,11},{9,8},{10,9... | collective-permute-start | bytes 2359304 | tf_op jit(solution)/shard_map/ppermute | solution.py:486
  213.3 34.9 %copy-start.17 = (bf16[4,384,256]{2,1,0:T(8,128)(2,1)}, bf16[4,384,256]{2,1,0:T(8,128)(2,1)S(1)}, u32[]{:S(2)}) copy-start(bf16[4,384,256]{2,1,0:T(8,128)(2,1)S(1)} %collective-permute-done.13.refs_3_) | copy-start | bytes 2359300
  213.3 33.0 %collective-permute-start.17 = (bf16[4,384,256]{2,1,0:T(8,128)(2,1)S(1)}, bf16[4,384,256]{2,1,0:T(8,128)(2,1)S(1)}, u32[]{:S(2)}, u32[]{:S(2)}) collective-permute-start(bf16[4,384,256]{2,1,0:T(8,128)(2,1)S(1)} %collective-permute-done.13.refs_3_), channel_id=1, source_target_pairs={{0,1},{1,2},{2,3},{3,0},{4,5},{5,6},{6,7},{7,4},{8,9},{9,10},{10,1... | collective-permute-start | bytes 2359304 | tf_op jit(solution)/shard_map/ppermute | solution.py:486
  213.3 33.0 %copy-start.18 = (bf16[4,384,256]{2,1,0:T(8,128)(2,1)}, bf16[4,384,256]{2,1,0:T(8,128)(2,1)S(1)}, u32[]{:S(2)}) copy-start(bf16[4,384,256]{2,1,0:T(8,128)(2,1)S(1)} %collective-permute-done.16.refs_6_) | copy-start | bytes 2359300
  213.3 32.9 %collective-permute-start.18 = (bf16[4,384,256]{2,1,0:T(8,128)(2,1)S(1)}, bf16[4,384,256]{2,1,0:T(8,128)(2,1)S(1)}, u32[]{:S(2)}, u32[]{:S(2)}) collective-permute-start(bf16[4,384,256]{2,1,0:T(8,128)(2,1)S(1)} %collective-permute-done.16.refs_6_), channel_id=1, source_target_pairs={{0,3},{1,0},{2,1},{3,2},{4,7},{5,4},{6,5},{7,6},{8,11},{9,8},{10,9... | collective-permute-start | bytes 2359304 | tf_op jit(solution)/shard_map/ppermute | solution.py:486
  (24 other events, 145.1 us)

commit v4 on v3

--- a/solution.py
+++ b/solution.py
@@ -26,6 +26,7 @@
 COLS = D // LANES
 CHUNK = 256
 PIECES = 4
+FAR_PIECES = 2
 CHUNKS = D // CHUNK
 MSG = 272
 HALF_MSG = 144
@@ -401,12 +402,12 @@
 def expert_far_kernel(*refs):
     rows_ref, acc_ref, gates, ups, downs, out_ref = refs[0], refs[1], refs[2:3], refs[3:4], refs[4:6], refs[6]
     sent, lines_ref, gate_ref, up_ref, down_ref, sems, out_sems = refs[7:]
-    part = SLOTS // PIECES
+    part = SLOTS // FAR_PIECES
     group = expert_copies(gates, ups, downs, gate_ref, up_ref, down_ref, sems)[0]
     for copy in group:
         copy.wait()
     outs = []
-    for p in range(PIECES):
+    for p in range(FAR_PIECES):
         block = pl.ds(p * part, part)
         rows = rows_ref[block, :]
         hidden = (silu(dot(rows, gate_ref[0])) * dot(rows, up_ref[0])).astype(BF16)
@@ -662,7 +663,7 @@
             pltpu.VMEM((1, D, width), BF16),
             pltpu.VMEM((1, width, D), BF16),
             pltpu.SemaphoreType.DMA((4, 1)),
-            pltpu.SemaphoreType.DMA((PIECES,)),
+            pltpu.SemaphoreType.DMA((FAR_PIECES,)),
         ],
         compiler_params=params(20),
         cost_estimate=cost(1_200_000_000, 8_000_000),
@@ -687,7 +688,7 @@
             pltpu.VMEM((TP, CHUNKS, CHUNK + LANES, CHUNK), BF16),
             pltpu.SemaphoreType.DMA((TP, 2)),
         ],
-        compiler_params=params(60),
+        compiler_params=params(40),
         cost_estimate=cost(800_000_000, 8_000_000),
         name="shared",
     )(normed, *packed, *shared_left, *shared_right, shared_far_0, shared_far_1)

time: 260 us -> 255 us (0.981)
  Pallas kernels: 41.9 us -> 38 us
    pallas_call x1, Pallas kernels: 6.51 us -> 3.49 us  [body(): pl.pallas_call(shared_kernel, out_shape=shape((TOK, D), F32), in_specs=[v...]
    unnamed x52 -> x44, local copies, waits for them, and re-layouts: 12.7 us -> 11.9 us
  transfers between devices with their start and end apart: 22 -> 22, of which waited for: 10 -> 10; matrix products, arithmetic and copies ran while one was open for 1% -> 1% of each run, Pallas kernels for 7% -> 6%
where the time goes in v4:
time: 255 us; the launch traced here: 254 us
  waiting for transfers between devices  134 us (53%)
  starting transfers between devices  52.2 us (20%)
  Pallas kernels  38 us (15%)
  blocking collectives  14.9 us (6%)
  local copies, waits for them, and re-layouts  13.6 us (5%)
    ppermute x19, waiting for transfers between devices, shift(): return lax.ppermute(array, 'tp', [(i, (i + hops) % TP) for i in range(TP)])  125 us
    ppermute x19, starting transfers between devices, shift(): return lax.ppermute(array, 'tp', [(i, (i + hops) % TP) for i in range(TP)])  28.6 us
    all_to_all x1, blocking collectives, body(): lax.all_to_all(msg, PLANE, split_axis=0, concat_axis=0, tiled=True)  14.9 us
    unnamed x44, local copies, waits for them, and re-layouts  11.9 us
    all_to_all x1, starting transfers between devices, body(): lax.all_to_all(done.reshape(EXPERTS, CAP * COLS, LANES), SP, split_axis=0...  10.4 us
    all_to_all x1, waiting for transfers between devices, body(): lax.all_to_all(msg, 'sp_0', split_axis=0, concat_axis=0, tiled=True)  9.72 us
    all_to_all x1, starting transfers between devices, body(): lax.all_to_all(msg, 'sp_0', split_axis=0, concat_axis=0, tiled=True)  7.61 us
    pallas_call x1, Pallas kernels, body(): pl.pallas_call(project_kernel, out_shape=(shape((TOK, D), BF16), shape((T...  7.38 us
  transfers between devices with their start and end apart: 22, of which 10 were waited for; matrix products, arithmetic and copies ran while one was open for 1% of the time, Pallas kernels for 6%

profile of v4, /device:TPU:2, one launch (start us, length us, event | category | flops | bytes accessed | tf_op | source)
XLA Modules:
  0.0 253.8 jit_solution(15612991379854955104)
XLA Ops:
  0.6 3.1 %states.1 = (bf16[8,272,128]{2,1,0:T(8,128)(2,1)}, f32[512,128]{1,0:T(8,128)}, f32[2,512,128]{2,1,0:T(8,128)}, f32[2,4,128,128]{3,2,1,0:T(8,128)}) custom-call(s32[4]{0:T(128)} %pad_add_fusion.own_ref, bf16[512,128]{1,0:T(8,128)(2,1)} %k_ref.1, bf16[512,256]{1,0:T(8,128)(2,1)} %v_ref.3, f32[512,128]{1,0:T(8,128)} %fd_ref.1, f32[512,128]{1,0:T(8,128)} %bd_ref.1, ...), custom_call_target="tpu_custom_call" | custom-call | flops 200000000 | bytes 4000000 | tf_op jit(solution)/shard_map/states/pallas_call | solution.py:541
  3.7 14.9 %all_to_all.20.gathered_ref = bf16[8,272,128]{2,1,0:T(8,128)(2,1)S(1)} all-to-all(bf16[8,272,128]{2,1,0:T(8,128)(2,1)} %get-tuple-element.30), channel_id=1, replica_groups=mesh['sp_0'=8,'sp_1'=4,'sp_2'=2,'tp'=4] {'sp_1','sp_2'}, dimensions={0} | all-to-all | bytes 1114112 | tf_op jit(solution)/shard_map/all_to_all | solution.py:555
  21.3 7.6 %all-to-all-start.1 = ((bf16[8,144,128]{2,1,0:T(8,128)(2,1)}), bf16[8,144,128]{2,1,0:T(8,128)(2,1)S(1)}, u32[]{:S(2)}, u32[]{:S(2)}) async-start(bf16[8,144,128]{2,1,0:T(8,128)(2,1)} %get-tuple-element.31), calls=%async_computation.1 | async-start | bytes 589824 | tf_op jit(solution)/shard_map/all_to_all | solution.py:582
  28.9 3.0 %attention.1 = (f32[512,256]{1,0:T(8,128)}, bf16[512,256]{1,0:T(8,128)(2,1)}, s32[2,128]{1,0:T(2,128)}) custom-call(s32[4]{0:T(128)} %pad_add_fusion.own_ref, bf16[512,128]{1,0:T(8,128)(2,1)} %q_ref.1, bf16[512,256]{1,0:T(8,128)(2,1)} %v_ref.3, f32[512,128]{1,0:T(8,128)} %get-tuple-element.26.key_ref, f32[2,512,128]{2,1,0:T(8,128)} %get-tuple-element.27.cumul_ref, ...), custom_call_target="tpu_custom_call" | custom-call | flops 400000000 | bytes 4000000 | tf_op jit(solution)/shard_map/attention/pallas_call | solution.py:556
  31.9 9.7 %all-to-all-done.1.gathered_ref = bf16[8,144,128]{2,1,0:T(8,128)(2,1)S(1)} async-done(((bf16[8,144,128]{2,1,0:T(8,128)(2,1)}), bf16[8,144,128]{2,1,0:T(8,128)(2,1)S(1)}, u32[]{:S(2)}, u32[]{:S(2)}) %all-to-all-start.1) | async-done | bytes 294944 | tf_op jit(solution)/shard_map/all_to_all | solution.py:582
  46.4 2.9 %collective-permute-start.1 = (bf16[128,256]{1,0:T(8,128)(2,1)}, bf16[128,256]{1,0:T(8,128)(2,1)S(1)}, u32[]{:S(2)}, u32[]{:S(2)}) collective-permute-start(bf16[128,256]{1,0:T(8,128)(2,1)} %get-tuple-element.38), channel_id=1, source_target_pairs={{0,2},{1,3},{2,0},{3,1},{4,6},{5,7},{6,4},{7,5},{8,10},{9,11},{10,... | collective-permute-start | bytes 196616 | tf_op jit(solution)/shard_map/ppermute | solution.py:487
  54.4 7.4 %project.1 = (bf16[128,2048]{1,0:T(8,128)(2,1)}, bf16[128,2048]{1,0:T(8,128)(2,1)}, bf16[384,16,128]{2,1,0:T(8,128)(2,1)}) custom-call(s32[4]{0:T(128)} %pad_add_fusion.own_ref, s32[2,128]{1,0:T(2,128)} %get-tuple-element.29.slots_ref, bf16[128,256]{1,0:T(8,128)(2,1)} %get-tuple-element.36.mixed_0, bf16[128,256]{1,0:T(8,128)(2,1)} %copy-done.19, ...), custom_call_target="tpu_custom_call" | custom-call | flops 600000000 | bytes 8000000 | tf_op jit(solution)/shard_map/project/pallas_call | solution.py:603
  61.8 5.6 %all-to-all-start.2 = ((bf16[64,96,128]{2,1,0:T(8,128)(2,1)}), bf16[64,96,128]{2,1,0:T(8,128)(2,1)S(1)}, u32[]{:S(2)}, u32[]{:S(2)}) async-start(bf16[64,96,128]{2,1,0:T(8,128)(2,1)} %bitcast.21), calls=%async_computation.2 | async-start | bytes 3145728 | tf_op jit(solution)/shard_map/all_to_all | solution.py:628
  67.8 2.9 %collective-permute-start.6 = (bf16[2048,256]{1,0:T(8,128)(2,1)}, bf16[2048,256]{1,0:T(8,128)(2,1)}, u32[]{:S(2)}, u32[]{:S(2)}) collective-permute-start(bf16[2048,256]{1,0:T(8,128)(2,1)} %bitcast.12.refs_4_), channel_id=1, source_target_pairs={{0,3},{1,0},{2,1},{3,2},{4,7},{5,4},{6,5},{7,6},{8,11},{9,8},{10,9... | collective-permute-start | bytes 3145736 | tf_op jit(solution)/shard_map/ppermute | solution.py:487
  70.7 3.2 %collective-permute-start.8 = (bf16[256,2048]{1,0:T(8,128)(2,1)}, bf16[256,2048]{1,0:T(8,128)(2,1)S(1)}, u32[]{:S(2)}, u32[]{:S(2)}) collective-permute-start(bf16[256,2048]{1,0:T(8,128)(2,1)} %bitcast.13.refs_7_), channel_id=1, source_target_pairs={{0,3},{1,0},{2,1},{3,2},{4,7},{5,4},{6,5},{7,6},{8,11},{9,8},{10,9... | collective-permute-start | bytes 3145736 | tf_op jit(solution)/shard_map/ppermute | solution.py:487
  74.1 20.9 %collective-permute-done.3.refs_2_ = bf16[2048,256]{1,0:T(8,128)(2,1)} collective-permute-done((bf16[2048,256]{1,0:T(8,128)(2,1)}, bf16[2048,256]{1,0:T(8,128)(2,1)}, u32[]{:S(2)}, u32[]{:S(2)}) %collective-permute-start.3) | collective-permute-done | bytes 1048608 | tf_op jit(solution)/shard_map/ppermute | solution.py:487
  95.8 21.6 %collective-permute-done.7.refs_8_ = bf16[256,2048]{1,0:T(8,128)(2,1)S(1)} collective-permute-done((bf16[256,2048]{1,0:T(8,128)(2,1)}, bf16[256,2048]{1,0:T(8,128)(2,1)S(1)}, u32[]{:S(2)}, u32[]{:S(2)}) %collective-permute-start.7) | collective-permute-done | bytes 1048608 | tf_op jit(solution)/shard_map/ppermute | solution.py:487
  121.1 18.4 %collective-permute-done.4.refs_3_ = bf16[2048,256]{1,0:T(8,128)(2,1)S(1)} collective-permute-done((bf16[2048,256]{1,0:T(8,128)(2,1)}, bf16[2048,256]{1,0:T(8,128)(2,1)S(1)}, u32[]{:S(2)}, u32[]{:S(2)}) %collective-permute-start.4) | collective-permute-done | bytes 1048608 | tf_op jit(solution)/shard_map/ppermute | solution.py:487
  140.6 3.6 %collective-permute-start.12 = (bf16[128,2048]{1,0:T(8,128)(2,1)}, bf16[128,2048]{1,0:T(8,128)(2,1)}, u32[]{:S(2)}, u32[]{:S(2)}) collective-permute-start(bf16[128,2048]{1,0:T(8,128)(2,1)} %slice.9), channel_id=1, source_target_pairs={{0,3},{1,0},{2,1},{3,2},{4,7},{5,4},{6,5},{7,6},{8,11},{9,8},{10,9... | collective-permute-start | bytes 1572872 | tf_op jit(solution)/shard_map/ppermute | solution.py:487
  150.2 7.1 %experts_near.1 = (bf16[384,2048]{1,0:T(8,128)(2,1)S(1)}, f32[384,2048]{1,0:T(8,128)S(1)}) custom-call(bf16[6144,128]{1,0:T(8,128)(2,1)S(1)} %bitcast.18, bf16[2048,256]{1,0:T(8,128)(2,1)} %bitcast.11.refs_1_, bf16[2048,256]{1,0:T(8,128)(2,1)} %collective-permute-done.3.refs_2_, bf16[2048,256]{1,0:T(8,128)(2,1)S(1)} %copy-done.15, ...), custom_call_target="tpu_custom_call" | custom-call | flops 3600000000 | bytes 16000000 | tf_op jit(solution)/shard_map/experts_near/pallas_call | solution.py:633
  157.2 15.5 %collective-permute-done.11.refs_4_ = bf16[128,2048]{1,0:T(8,128)(2,1)S(1)} collective-permute-done((bf16[128,2048]{1,0:T(8,128)(2,1)}, bf16[128,2048]{1,0:T(8,128)(2,1)S(1)}, u32[]{:S(2)}, u32[]{:S(2)}) %collective-permute-start.11) | collective-permute-done | bytes 524320 | tf_op jit(solution)/shard_map/ppermute | solution.py:487
  172.7 4.7 %experts_far.1 = bf16[6144,128]{1,0:T(8,128)(2,1)} custom-call(bf16[384,2048]{1,0:T(8,128)(2,1)S(1)} %get-tuple-element.41.refs_0_, f32[384,2048]{1,0:T(8,128)S(1)} %get-tuple-element.42.refs_1_, bf16[2048,256]{1,0:T(8,128)(2,1)S(1)} %collective-permute-done.9.refs_2_, bf16[2048,256]{1,0:T(8,128)(2,1)} %collective-permute-done.10.refs_3_, ...), custom_call_target="tpu_custom_call" | custom-call | flops 1200000000 | bytes 8000000 | tf_op jit(solution)/shard_map/experts_far/pallas_call | solution.py:654
  177.5 10.4 %all-to-all-start.3 = ((bf16[64,96,128]{2,1,0:T(8,128)(2,1)}), bf16[64,96,128]{2,1,0:T(8,128)(2,1)S(1)}, u32[]{:S(2)}, u32[]{:S(2)}) async-start(bf16[64,96,128]{2,1,0:T(8,128)(2,1)} %bitcast.14), calls=%async_computation.3 | async-start | bytes 3145728 | tf_op jit(solution)/shard_map/all_to_all | solution.py:672
  193.8 3.2 %collective-permute-start.15 = (bf16[4,384,256]{2,1,0:T(8,128)(2,1)}, bf16[4,384,256]{2,1,0:T(8,128)(2,1)S(1)}, u32[]{:S(2)}, u32[]{:S(2)}) collective-permute-start(bf16[4,384,256]{2,1,0:T(8,128)(2,1)} %get-tuple-element.45.refs_1_), channel_id=1, source_target_pairs={{0,3},{1,0},{2,1},{3,2},{4,7},{5,4},{6,5},{7,6},{8,11},{9,8},{10,9... | collective-permute-start | bytes 2359304 | tf_op jit(solution)/shard_map/ppermute | solution.py:487
  197.1 15.4 %collective-permute-done.13.refs_3_ = bf16[4,384,256]{2,1,0:T(8,128)(2,1)S(1)} collective-permute-done((bf16[4,384,256]{2,1,0:T(8,128)(2,1)}, bf16[4,384,256]{2,1,0:T(8,128)(2,1)S(1)}, u32[]{:S(2)}, u32[]{:S(2)}) %collective-permute-start.13) | collective-permute-done | bytes 786464 | tf_op jit(solution)/shard_map/ppermute | solution.py:487
  212.4 3.2 %collective-permute-start.18 = (bf16[4,384,256]{2,1,0:T(8,128)(2,1)S(1)}, bf16[4,384,256]{2,1,0:T(8,128)(2,1)S(1)}, u32[]{:S(2)}, u32[]{:S(2)}) collective-permute-start(bf16[4,384,256]{2,1,0:T(8,128)(2,1)S(1)} %collective-permute-done.16.refs_6_), channel_id=1, source_target_pairs={{0,3},{1,0},{2,1},{3,2},{4,7},{5,4},{6,5},{7,6},{8,11},{9,8},{10,9... | collective-permute-start | bytes 2359304 | tf_op jit(solution)/shard_map/ppermute | solution.py:487
  215.7 13.6 %collective-permute-done.14.refs_4_ = bf16[4,384,256]{2,1,0:T(8,128)(2,1)S(1)} collective-permute-done((bf16[4,384,256]{2,1,0:T(8,128)(2,1)}, bf16[4,384,256]{2,1,0:T(8,128)(2,1)S(1)}, u32[]{:S(2)}, u32[]{:S(2)}) %collective-permute-start.14) | collective-permute-done | bytes 786464 | tf_op jit(solution)/shard_map/ppermute | solution.py:487
  229.3 16.1 %collective-permute-done.17.refs_7_ = bf16[4,384,256]{2,1,0:T(8,128)(2,1)S(1)} collective-permute-done((bf16[4,384,256]{2,1,0:T(8,128)(2,1)S(1)}, bf16[4,384,256]{2,1,0:T(8,128)(2,1)S(1)}, u32[]{:S(2)}, u32[]{:S(2)}) %collective-permute-start.17) | collective-permute-done | bytes 786464 | tf_op jit(solution)/shard_map/ppermute | solution.py:487
  247.7 3.5 %shared.1.shared_ref = f32[128,2048]{1,0:T(8,128)S(1)} custom-call(bf16[128,2048]{1,0:T(8,128)(2,1)S(1)} %copy-done.3, bf16[4,384,256]{2,1,0:T(8,128)(2,1)S(1)} %copy-done.1, bf16[4,384,256]{2,1,0:T(8,128)(2,1)S(1)} %copy-done.2, bf16[4,384,256]{2,1,0:T(8,128)(2,1)S(1)} %collective-permute-done.13.refs_3_, ...), custom_call_target="tpu_custom_call" | custom-call | flops 800000000 | bytes 8000000 | tf_op jit(solution)/shard_map/shared/pallas_call | solution.py:682
  (78 shorter events, 36.0 us)
Async XLA Ops:
  21.3 20.3 %all-to-all-start.1 = ((bf16[8,144,128]{2,1,0:T(8,128)(2,1)}), bf16[8,144,128]{2,1,0:T(8,128)(2,1)S(1)}, u32[]{:S(2)}, u32[]{:S(2)}) async-start(bf16[8,144,128]{2,1,0:T(8,128)(2,1)} %get-tuple-element.31), calls=%async_computation.1 | async-start | bytes 589824 | tf_op jit(solution)/shard_map/all_to_all | solution.py:582
  44.9 5.8 %collective-permute-start = (bf16[128,256]{1,0:T(8,128)(2,1)}, bf16[128,256]{1,0:T(8,128)(2,1)S(1)}, u32[]{:S(2)}, u32[]{:S(2)}) collective-permute-start(bf16[128,256]{1,0:T(8,128)(2,1)} %get-tuple-element.37), channel_id=1, source_target_pairs={{0,1},{1,2},{2,3},{3,0},{4,5},{5,6},{6,7},{7,4},{8,9},{9,10},{10,1... | collective-permute-start | bytes 196616 | tf_op jit(solution)/shard_map/ppermute | solution.py:487
  46.4 6.1 %collective-permute-start.1 = (bf16[128,256]{1,0:T(8,128)(2,1)}, bf16[128,256]{1,0:T(8,128)(2,1)S(1)}, u32[]{:S(2)}, u32[]{:S(2)}) collective-permute-start(bf16[128,256]{1,0:T(8,128)(2,1)} %get-tuple-element.38), channel_id=1, source_target_pairs={{0,2},{1,3},{2,0},{3,1},{4,6},{5,7},{6,4},{7,5},{8,10},{9,11},{10,... | collective-permute-start | bytes 196616 | tf_op jit(solution)/shard_map/ppermute | solution.py:487
  49.3 4.5 %collective-permute-start.2 = (bf16[128,256]{1,0:T(8,128)(2,1)}, bf16[128,256]{1,0:T(8,128)(2,1)S(1)}, u32[]{:S(2)}, u32[]{:S(2)}) collective-permute-start(bf16[128,256]{1,0:T(8,128)(2,1)} %get-tuple-element.39), channel_id=1, source_target_pairs={{0,3},{1,0},{2,1},{3,2},{4,7},{5,4},{6,5},{7,6},{8,11},{9,8},{10,9... | collective-permute-start | bytes 196616 | tf_op jit(solution)/shard_map/ppermute | solution.py:487
  61.8 83.4 %all-to-all-start.2 = ((bf16[64,96,128]{2,1,0:T(8,128)(2,1)}), bf16[64,96,128]{2,1,0:T(8,128)(2,1)S(1)}, u32[]{:S(2)}, u32[]{:S(2)}) async-start(bf16[64,96,128]{2,1,0:T(8,128)(2,1)} %bitcast.21), calls=%async_computation.2 | async-start | bytes 3145728 | tf_op jit(solution)/shard_map/all_to_all | solution.py:628
  67.4 27.6 %collective-permute-start.3 = (bf16[2048,256]{1,0:T(8,128)(2,1)}, bf16[2048,256]{1,0:T(8,128)(2,1)}, u32[]{:S(2)}, u32[]{:S(2)}) collective-permute-start(bf16[2048,256]{1,0:T(8,128)(2,1)} %bitcast.11.refs_1_), channel_id=1, source_target_pairs={{0,1},{1,2},{2,3},{3,0},{4,5},{5,6},{6,7},{7,4},{8,9},{9,10},{10,1... | collective-permute-start | bytes 3145736 | tf_op jit(solution)/shard_map/ppermute | solution.py:487
  67.8 27.2 %collective-permute-start.6 = (bf16[2048,256]{1,0:T(8,128)(2,1)}, bf16[2048,256]{1,0:T(8,128)(2,1)}, u32[]{:S(2)}, u32[]{:S(2)}) collective-permute-start(bf16[2048,256]{1,0:T(8,128)(2,1)} %bitcast.12.refs_4_), channel_id=1, source_target_pairs={{0,3},{1,0},{2,1},{3,2},{4,7},{5,4},{6,5},{7,6},{8,11},{9,8},{10,9... | collective-permute-start | bytes 3145736 | tf_op jit(solution)/shard_map/ppermute | solution.py:487
  70.7 46.7 %collective-permute-start.7 = (bf16[256,2048]{1,0:T(8,128)(2,1)}, bf16[256,2048]{1,0:T(8,128)(2,1)S(1)}, u32[]{:S(2)}, u32[]{:S(2)}) collective-permute-start(bf16[256,2048]{1,0:T(8,128)(2,1)} %bitcast.13.refs_7_), channel_id=1, source_target_pairs={{0,1},{1,2},{2,3},{3,0},{4,5},{5,6},{6,7},{7,4},{8,9},{9,10},{10,1... | collective-permute-start | bytes 3145736 | tf_op jit(solution)/shard_map/ppermute | solution.py:487
  70.7 48.9 %collective-permute-start.8 = (bf16[256,2048]{1,0:T(8,128)(2,1)}, bf16[256,2048]{1,0:T(8,128)(2,1)S(1)}, u32[]{:S(2)}, u32[]{:S(2)}) collective-permute-start(bf16[256,2048]{1,0:T(8,128)(2,1)} %bitcast.13.refs_7_), channel_id=1, source_target_pairs={{0,3},{1,0},{2,1},{3,2},{4,7},{5,4},{6,5},{7,6},{8,11},{9,8},{10,9... | collective-permute-start | bytes 3145736 | tf_op jit(solution)/shard_map/ppermute | solution.py:487
  74.0 65.6 %collective-permute-start.4 = (bf16[2048,256]{1,0:T(8,128)(2,1)}, bf16[2048,256]{1,0:T(8,128)(2,1)S(1)}, u32[]{:S(2)}, u32[]{:S(2)}) collective-permute-start(bf16[2048,256]{1,0:T(8,128)(2,1)} %bitcast.11.refs_1_), channel_id=1, source_target_pairs={{0,3},{1,0},{2,1},{3,2},{4,7},{5,4},{6,5},{7,6},{8,11},{9,8},{10,9... | collective-permute-start | bytes 3145736 | tf_op jit(solution)/shard_map/ppermute | solution.py:487
  95.0 49.1 %collective-permute-start.5 = (bf16[2048,256]{1,0:T(8,128)(2,1)}, bf16[2048,256]{1,0:T(8,128)(2,1)S(1)}, u32[]{:S(2)}, u32[]{:S(2)}) collective-permute-start(bf16[2048,256]{1,0:T(8,128)(2,1)} %bitcast.12.refs_4_), channel_id=1, source_target_pairs={{0,1},{1,2},{2,3},{3,0},{4,5},{5,6},{6,7},{7,4},{8,9},{9,10},{10,1... | collective-permute-start | bytes 3145736 | tf_op jit(solution)/shard_map/ppermute | solution.py:487
  95.0 77.7 %collective-permute-start.9 = (bf16[2048,256]{1,0:T(8,128)(2,1)}, bf16[2048,256]{1,0:T(8,128)(2,1)S(1)}, u32[]{:S(2)}, u32[]{:S(2)}) collective-permute-start(bf16[2048,256]{1,0:T(8,128)(2,1)} %collective-permute-done.3.refs_2_), channel_id=1, source_target_pairs={{0,1},{1,2},{2,3},{3,0},{4,5},{5,6},{6,7},{7,4},{8,9},{9,10},{10,1... | collective-permute-start | bytes 3145736 | tf_op jit(solution)/shard_map/ppermute | solution.py:487
  117.4 26.8 %copy-start.4 = (bf16[256,2048]{1,0:T(8,128)(2,1)}, bf16[256,2048]{1,0:T(8,128)(2,1)S(1)}, u32[]{:S(2)}) copy-start(bf16[256,2048]{1,0:T(8,128)(2,1)S(1)} %collective-permute-done.7.refs_8_) | copy-start | bytes 3145732
  117.4 55.3 %collective-permute-start.10 = (bf16[2048,256]{1,0:T(8,128)(2,1)}, bf16[2048,256]{1,0:T(8,128)(2,1)}, u32[]{:S(2)}, u32[]{:S(2)}) collective-permute-start(bf16[2048,256]{1,0:T(8,128)(2,1)} %collective-permute-done.6.refs_6_), channel_id=1, source_target_pairs={{0,3},{1,0},{2,1},{3,2},{4,7},{5,4},{6,5},{7,6},{8,11},{9,8},{10,9... | collective-permute-start | bytes 3145736 | tf_op jit(solution)/shard_map/ppermute | solution.py:487
  119.6 53.1 %collective-permute-start.11 = (bf16[128,2048]{1,0:T(8,128)(2,1)}, bf16[128,2048]{1,0:T(8,128)(2,1)S(1)}, u32[]{:S(2)}, u32[]{:S(2)}) collective-permute-start(bf16[128,2048]{1,0:T(8,128)(2,1)} %slice.8), channel_id=1, source_target_pairs={{0,1},{1,2},{2,3},{3,0},{4,5},{5,6},{6,7},{7,4},{8,9},{9,10},{10,1... | collective-permute-start | bytes 1572872 | tf_op jit(solution)/shard_map/ppermute | solution.py:487
  140.6 32.2 %collective-permute-start.12 = (bf16[128,2048]{1,0:T(8,128)(2,1)}, bf16[128,2048]{1,0:T(8,128)(2,1)}, u32[]{:S(2)}, u32[]{:S(2)}) collective-permute-start(bf16[128,2048]{1,0:T(8,128)(2,1)} %slice.9), channel_id=1, source_target_pairs={{0,3},{1,0},{2,1},{3,2},{4,7},{5,4},{6,5},{7,6},{8,11},{9,8},{10,9... | collective-permute-start | bytes 1572872 | tf_op jit(solution)/shard_map/ppermute | solution.py:487
  177.5 73.7 %all-to-all-start.3 = ((bf16[64,96,128]{2,1,0:T(8,128)(2,1)}), bf16[64,96,128]{2,1,0:T(8,128)(2,1)S(1)}, u32[]{:S(2)}, u32[]{:S(2)}) async-start(bf16[64,96,128]{2,1,0:T(8,128)(2,1)} %bitcast.14), calls=%async_computation.3 | async-start | bytes 3145728 | tf_op jit(solution)/shard_map/all_to_all | solution.py:672
  187.9 57.5 %copy-start.3 = (bf16[128,2048]{1,0:T(8,128)(2,1)S(1)}, bf16[128,2048]{1,0:T(8,128)(2,1)}, u32[]{:S(2)}) copy-start(bf16[128,2048]{1,0:T(8,128)(2,1)} %get-tuple-element.43.refs_0_) | copy-start | bytes 1572868
  190.6 21.8 %collective-permute-start.13 = (bf16[4,384,256]{2,1,0:T(8,128)(2,1)}, bf16[4,384,256]{2,1,0:T(8,128)(2,1)S(1)}, u32[]{:S(2)}, u32[]{:S(2)}) collective-permute-start(bf16[4,384,256]{2,1,0:T(8,128)(2,1)} %get-tuple-element.45.refs_1_), channel_id=1, source_target_pairs={{0,1},{1,2},{2,3},{3,0},{4,5},{5,6},{6,7},{7,4},{8,9},{9,10},{10,1... | collective-permute-start | bytes 2359304 | tf_op jit(solution)/shard_map/ppermute | solution.py:487
  191.4 21.0 %collective-permute-start.16 = (bf16[4,384,256]{2,1,0:T(8,128)(2,1)}, bf16[4,384,256]{2,1,0:T(8,128)(2,1)S(1)}, u32[]{:S(2)}, u32[]{:S(2)}) collective-permute-start(bf16[4,384,256]{2,1,0:T(8,128)(2,1)} %get-tuple-element.46.refs_2_), channel_id=1, source_target_pairs={{0,3},{1,0},{2,1},{3,2},{4,7},{5,4},{6,5},{7,6},{8,11},{9,8},{10,9... | collective-permute-start | bytes 2359304 | tf_op jit(solution)/shard_map/ppermute | solution.py:487
  193.8 35.5 %collective-permute-start.14 = (bf16[4,384,256]{2,1,0:T(8,128)(2,1)}, bf16[4,384,256]{2,1,0:T(8,128)(2,1)S(1)}, u32[]{:S(2)}, u32[]{:S(2)}) collective-permute-start(bf16[4,384,256]{2,1,0:T(8,128)(2,1)} %get-tuple-element.46.refs_2_), channel_id=1, source_target_pairs={{0,1},{1,2},{2,3},{3,0},{4,5},{5,6},{6,7},{7,4},{8,9},{9,10},{10,1... | collective-permute-start | bytes 2359304 | tf_op jit(solution)/shard_map/ppermute | solution.py:487
  193.8 35.5 %collective-permute-start.15 = (bf16[4,384,256]{2,1,0:T(8,128)(2,1)}, bf16[4,384,256]{2,1,0:T(8,128)(2,1)S(1)}, u32[]{:S(2)}, u32[]{:S(2)}) collective-permute-start(bf16[4,384,256]{2,1,0:T(8,128)(2,1)} %get-tuple-element.45.refs_1_), channel_id=1, source_target_pairs={{0,3},{1,0},{2,1},{3,2},{4,7},{5,4},{6,5},{7,6},{8,11},{9,8},{10,9... | collective-permute-start | bytes 2359304 | tf_op jit(solution)/shard_map/ppermute | solution.py:487
  212.4 32.9 %collective-permute-start.17 = (bf16[4,384,256]{2,1,0:T(8,128)(2,1)S(1)}, bf16[4,384,256]{2,1,0:T(8,128)(2,1)S(1)}, u32[]{:S(2)}, u32[]{:S(2)}) collective-permute-start(bf16[4,384,256]{2,1,0:T(8,128)(2,1)S(1)} %collective-permute-done.13.refs_3_), channel_id=1, source_target_pairs={{0,1},{1,2},{2,3},{3,0},{4,5},{5,6},{6,7},{7,4},{8,9},{9,10},{10,1... | collective-permute-start | bytes 2359304 | tf_op jit(solution)/shard_map/ppermute | solution.py:487
  212.4 32.9 %collective-permute-start.18 = (bf16[4,384,256]{2,1,0:T(8,128)(2,1)S(1)}, bf16[4,384,256]{2,1,0:T(8,128)(2,1)S(1)}, u32[]{:S(2)}, u32[]{:S(2)}) collective-permute-start(bf16[4,384,256]{2,1,0:T(8,128)(2,1)S(1)} %collective-permute-done.16.refs_6_), channel_id=1, source_target_pairs={{0,3},{1,0},{2,1},{3,2},{4,7},{5,4},{6,5},{7,6},{8,11},{9,8},{10,9... | collective-permute-start | bytes 2359304 | tf_op jit(solution)/shard_map/ppermute | solution.py:487
  (20 other events, 73.1 us)

commit v5 on v4

--- a/solution.py
+++ b/solution.py
@@ -26,7 +26,7 @@
 COLS = D // LANES
 CHUNK = 256
 PIECES = 4
-FAR_PIECES = 2
+FAR_PIECES = 4
 CHUNKS = D // CHUNK
 MSG = 272
 HALF_MSG = 144
@@ -406,18 +406,17 @@
     group = expert_copies(gates, ups, downs, gate_ref, up_ref, down_ref, sems)[0]
     for copy in group:
         copy.wait()
+    rows = rows_ref[...]
+    hidden = (silu(dot(rows, gate_ref[0])) * dot(rows, up_ref[0])).astype(BF16)
+    for j in range(CHUNKS):
+        columns = pl.ds(j * CHUNK, CHUNK)
+        total = acc_ref[:, columns] + dot(hidden, down_ref[0, :, columns])
+        for i in range(CHUNK // LANES):
+            lines_ref[pl.ds(j * (CHUNK // LANES) + i, SLOTS, stride=COLS), :] = total[
+                :, i * LANES : (i + 1) * LANES
+            ]
     outs = []
     for p in range(FAR_PIECES):
-        block = pl.ds(p * part, part)
-        rows = rows_ref[block, :]
-        hidden = (silu(dot(rows, gate_ref[0])) * dot(rows, up_ref[0])).astype(BF16)
-        for j in range(CHUNKS):
-            columns = pl.ds(j * CHUNK, CHUNK)
-            total = acc_ref[block, columns] + dot(hidden, down_ref[0, :, columns])
-            for i in range(CHUNK // LANES):
-                lines_ref[
-                    pl.ds(p * part * COLS + j * (CHUNK // LANES) + i, part, stride=COLS), :
-                ] = total[:, i * LANES : (i + 1) * LANES]
         span = pl.ds(p * part * COLS, part * COLS)
         sent[span, :] = lines_ref[span, :].astype(BF16)
         copy = pltpu.make_async_copy(sent.at[span], out_ref.at[span], out_sems.at[p])

time: 255 us -> 255 us (level)
  no operation moved by 1% of the time
where the time goes in v5:
time: 255 us; the launch traced here: 254 us
  waiting for transfers between devices  134 us (53%)
  starting transfers between devices  52.2 us (20%)
  Pallas kernels  37.9 us (15%)
  blocking collectives  14.9 us (6%)
  local copies, waits for them, and re-layouts  13.6 us (5%)
    ppermute x19, waiting for transfers between devices, shift(): return lax.ppermute(array, 'tp', [(i, (i + hops) % TP) for i in range(TP)])  125 us
    ppermute x19, starting transfers between devices, shift(): return lax.ppermute(array, 'tp', [(i, (i + hops) % TP) for i in range(TP)])  28.6 us
    all_to_all x1, blocking collectives, body(): lax.all_to_all(msg, PLANE, split_axis=0, concat_axis=0, tiled=True)  14.9 us
    unnamed x44, local copies, waits for them, and re-layouts  11.9 us
    all_to_all x1, starting transfers between devices, body(): lax.all_to_all(done.reshape(EXPERTS, CAP * COLS, LANES), SP, split_axis=0...  10.4 us
    all_to_all x1, waiting for transfers between devices, body(): lax.all_to_all(msg, 'sp_0', split_axis=0, concat_axis=0, tiled=True)  9.72 us
    all_to_all x1, starting transfers between devices, body(): lax.all_to_all(msg, 'sp_0', split_axis=0, concat_axis=0, tiled=True)  7.61 us
    pallas_call x1, Pallas kernels, body(): pl.pallas_call(project_kernel, out_shape=(shape((TOK, D), BF16), shape((T...  7.38 us
  transfers between devices with their start and end apart: 22, of which 10 were waited for; matrix products, arithmetic and copies ran while one was open for 1% of the time, Pallas kernels for 6%

profile of v5, /device:TPU:2, one launch (start us, length us, event | category | flops | bytes accessed | tf_op | source)
XLA Modules:
  0.0 253.7 jit_solution(17517242333923220312)
XLA Ops:
  0.6 3.1 %states.1 = (bf16[8,272,128]{2,1,0:T(8,128)(2,1)}, f32[512,128]{1,0:T(8,128)}, f32[2,512,128]{2,1,0:T(8,128)}, f32[2,4,128,128]{3,2,1,0:T(8,128)}) custom-call(s32[4]{0:T(128)} %pad_add_fusion.own_ref, bf16[512,128]{1,0:T(8,128)(2,1)} %k_ref.1, bf16[512,256]{1,0:T(8,128)(2,1)} %v_ref.3, f32[512,128]{1,0:T(8,128)} %fd_ref.1, f32[512,128]{1,0:T(8,128)} %bd_ref.1, ...), custom_call_target="tpu_custom_call" | custom-call | flops 200000000 | bytes 4000000 | tf_op jit(solution)/shard_map/states/pallas_call | solution.py:540
  3.7 14.9 %all_to_all.20.gathered_ref = bf16[8,272,128]{2,1,0:T(8,128)(2,1)S(1)} all-to-all(bf16[8,272,128]{2,1,0:T(8,128)(2,1)} %get-tuple-element.30), channel_id=1, replica_groups=mesh['sp_0'=8,'sp_1'=4,'sp_2'=2,'tp'=4] {'sp_1','sp_2'}, dimensions={0} | all-to-all | bytes 1114112 | tf_op jit(solution)/shard_map/all_to_all | solution.py:554
  21.3 7.6 %all-to-all-start.1 = ((bf16[8,144,128]{2,1,0:T(8,128)(2,1)}), bf16[8,144,128]{2,1,0:T(8,128)(2,1)S(1)}, u32[]{:S(2)}, u32[]{:S(2)}) async-start(bf16[8,144,128]{2,1,0:T(8,128)(2,1)} %get-tuple-element.31), calls=%async_computation.1 | async-start | bytes 589824 | tf_op jit(solution)/shard_map/all_to_all | solution.py:581
  28.9 3.0 %attention.1 = (f32[512,256]{1,0:T(8,128)}, bf16[512,256]{1,0:T(8,128)(2,1)}, s32[2,128]{1,0:T(2,128)}) custom-call(s32[4]{0:T(128)} %pad_add_fusion.own_ref, bf16[512,128]{1,0:T(8,128)(2,1)} %q_ref.1, bf16[512,256]{1,0:T(8,128)(2,1)} %v_ref.3, f32[512,128]{1,0:T(8,128)} %get-tuple-element.26.key_ref, f32[2,512,128]{2,1,0:T(8,128)} %get-tuple-element.27.cumul_ref, ...), custom_call_target="tpu_custom_call" | custom-call | flops 400000000 | bytes 4000000 | tf_op jit(solution)/shard_map/attention/pallas_call | solution.py:555
  31.9 9.7 %all-to-all-done.1.gathered_ref = bf16[8,144,128]{2,1,0:T(8,128)(2,1)S(1)} async-done(((bf16[8,144,128]{2,1,0:T(8,128)(2,1)}), bf16[8,144,128]{2,1,0:T(8,128)(2,1)S(1)}, u32[]{:S(2)}, u32[]{:S(2)}) %all-to-all-start.1) | async-done | bytes 294944 | tf_op jit(solution)/shard_map/all_to_all | solution.py:581
  46.4 2.9 %collective-permute-start.1 = (bf16[128,256]{1,0:T(8,128)(2,1)}, bf16[128,256]{1,0:T(8,128)(2,1)S(1)}, u32[]{:S(2)}, u32[]{:S(2)}) collective-permute-start(bf16[128,256]{1,0:T(8,128)(2,1)} %get-tuple-element.38), channel_id=1, source_target_pairs={{0,2},{1,3},{2,0},{3,1},{4,6},{5,7},{6,4},{7,5},{8,10},{9,11},{10,... | collective-permute-start | bytes 196616 | tf_op jit(solution)/shard_map/ppermute | solution.py:486
  54.4 7.4 %project.1 = (bf16[128,2048]{1,0:T(8,128)(2,1)}, bf16[128,2048]{1,0:T(8,128)(2,1)}, bf16[384,16,128]{2,1,0:T(8,128)(2,1)}) custom-call(s32[4]{0:T(128)} %pad_add_fusion.own_ref, s32[2,128]{1,0:T(2,128)} %get-tuple-element.29.slots_ref, bf16[128,256]{1,0:T(8,128)(2,1)} %get-tuple-element.36.mixed_0, bf16[128,256]{1,0:T(8,128)(2,1)} %copy-done.19, ...), custom_call_target="tpu_custom_call" | custom-call | flops 600000000 | bytes 8000000 | tf_op jit(solution)/shard_map/project/pallas_call | solution.py:602
  61.8 5.6 %all-to-all-start.2 = ((bf16[64,96,128]{2,1,0:T(8,128)(2,1)}), bf16[64,96,128]{2,1,0:T(8,128)(2,1)S(1)}, u32[]{:S(2)}, u32[]{:S(2)}) async-start(bf16[64,96,128]{2,1,0:T(8,128)(2,1)} %bitcast.21), calls=%async_computation.2 | async-start | bytes 3145728 | tf_op jit(solution)/shard_map/all_to_all | solution.py:627
  67.8 2.9 %collective-permute-start.6 = (bf16[2048,256]{1,0:T(8,128)(2,1)}, bf16[2048,256]{1,0:T(8,128)(2,1)}, u32[]{:S(2)}, u32[]{:S(2)}) collective-permute-start(bf16[2048,256]{1,0:T(8,128)(2,1)} %bitcast.12.refs_4_), channel_id=1, source_target_pairs={{0,3},{1,0},{2,1},{3,2},{4,7},{5,4},{6,5},{7,6},{8,11},{9,8},{10,9... | collective-permute-start | bytes 3145736 | tf_op jit(solution)/shard_map/ppermute | solution.py:486
  70.7 3.2 %collective-permute-start.8 = (bf16[256,2048]{1,0:T(8,128)(2,1)}, bf16[256,2048]{1,0:T(8,128)(2,1)S(1)}, u32[]{:S(2)}, u32[]{:S(2)}) collective-permute-start(bf16[256,2048]{1,0:T(8,128)(2,1)} %bitcast.13.refs_7_), channel_id=1, source_target_pairs={{0,3},{1,0},{2,1},{3,2},{4,7},{5,4},{6,5},{7,6},{8,11},{9,8},{10,9... | collective-permute-start | bytes 3145736 | tf_op jit(solution)/shard_map/ppermute | solution.py:486
  74.1 20.9 %collective-permute-done.3.refs_2_ = bf16[2048,256]{1,0:T(8,128)(2,1)} collective-permute-done((bf16[2048,256]{1,0:T(8,128)(2,1)}, bf16[2048,256]{1,0:T(8,128)(2,1)}, u32[]{:S(2)}, u32[]{:S(2)}) %collective-permute-start.3) | collective-permute-done | bytes 1048608 | tf_op jit(solution)/shard_map/ppermute | solution.py:486
  95.8 21.6 %collective-permute-done.7.refs_8_ = bf16[256,2048]{1,0:T(8,128)(2,1)S(1)} collective-permute-done((bf16[256,2048]{1,0:T(8,128)(2,1)}, bf16[256,2048]{1,0:T(8,128)(2,1)S(1)}, u32[]{:S(2)}, u32[]{:S(2)}) %collective-permute-start.7) | collective-permute-done | bytes 1048608 | tf_op jit(solution)/shard_map/ppermute | solution.py:486
  121.1 18.4 %collective-permute-done.4.refs_3_ = bf16[2048,256]{1,0:T(8,128)(2,1)S(1)} collective-permute-done((bf16[2048,256]{1,0:T(8,128)(2,1)}, bf16[2048,256]{1,0:T(8,128)(2,1)S(1)}, u32[]{:S(2)}, u32[]{:S(2)}) %collective-permute-start.4) | collective-permute-done | bytes 1048608 | tf_op jit(solution)/shard_map/ppermute | solution.py:486
  140.6 3.6 %collective-permute-start.12 = (bf16[128,2048]{1,0:T(8,128)(2,1)}, bf16[128,2048]{1,0:T(8,128)(2,1)}, u32[]{:S(2)}, u32[]{:S(2)}) collective-permute-start(bf16[128,2048]{1,0:T(8,128)(2,1)} %slice.9), channel_id=1, source_target_pairs={{0,3},{1,0},{2,1},{3,2},{4,7},{5,4},{6,5},{7,6},{8,11},{9,8},{10,9... | collective-permute-start | bytes 1572872 | tf_op jit(solution)/shard_map/ppermute | solution.py:486
  150.2 7.1 %experts_near.1 = (bf16[384,2048]{1,0:T(8,128)(2,1)S(1)}, f32[384,2048]{1,0:T(8,128)S(1)}) custom-call(bf16[6144,128]{1,0:T(8,128)(2,1)S(1)} %bitcast.18, bf16[2048,256]{1,0:T(8,128)(2,1)} %bitcast.11.refs_1_, bf16[2048,256]{1,0:T(8,128)(2,1)} %collective-permute-done.3.refs_2_, bf16[2048,256]{1,0:T(8,128)(2,1)S(1)} %copy-done.15, ...), custom_call_target="tpu_custom_call" | custom-call | flops 3600000000 | bytes 16000000 | tf_op jit(solution)/shard_map/experts_near/pallas_call | solution.py:632
  157.2 15.5 %collective-permute-done.11.refs_4_ = bf16[128,2048]{1,0:T(8,128)(2,1)S(1)} collective-permute-done((bf16[128,2048]{1,0:T(8,128)(2,1)}, bf16[128,2048]{1,0:T(8,128)(2,1)S(1)}, u32[]{:S(2)}, u32[]{:S(2)}) %collective-permute-start.11) | collective-permute-done | bytes 524320 | tf_op jit(solution)/shard_map/ppermute | solution.py:486
  172.7 4.6 %experts_far.1 = bf16[6144,128]{1,0:T(8,128)(2,1)} custom-call(bf16[384,2048]{1,0:T(8,128)(2,1)S(1)} %get-tuple-element.41.refs_0_, f32[384,2048]{1,0:T(8,128)S(1)} %get-tuple-element.42.refs_1_, bf16[2048,256]{1,0:T(8,128)(2,1)S(1)} %collective-permute-done.9.refs_2_, bf16[2048,256]{1,0:T(8,128)(2,1)} %collective-permute-done.10.refs_3_, ...), custom_call_target="tpu_custom_call" | custom-call | flops 1200000000 | bytes 8000000 | tf_op jit(solution)/shard_map/experts_far/pallas_call | solution.py:653
  177.4 10.4 %all-to-all-start.3 = ((bf16[64,96,128]{2,1,0:T(8,128)(2,1)}), bf16[64,96,128]{2,1,0:T(8,128)(2,1)S(1)}, u32[]{:S(2)}, u32[]{:S(2)}) async-start(bf16[64,96,128]{2,1,0:T(8,128)(2,1)} %bitcast.14), calls=%async_computation.3 | async-start | bytes 3145728 | tf_op jit(solution)/shard_map/all_to_all | solution.py:671
  193.7 3.2 %collective-permute-start.15 = (bf16[4,384,256]{2,1,0:T(8,128)(2,1)}, bf16[4,384,256]{2,1,0:T(8,128)(2,1)S(1)}, u32[]{:S(2)}, u32[]{:S(2)}) collective-permute-start(bf16[4,384,256]{2,1,0:T(8,128)(2,1)} %get-tuple-element.45.refs_1_), channel_id=1, source_target_pairs={{0,3},{1,0},{2,1},{3,2},{4,7},{5,4},{6,5},{7,6},{8,11},{9,8},{10,9... | collective-permute-start | bytes 2359304 | tf_op jit(solution)/shard_map/ppermute | solution.py:486
  197.0 15.4 %collective-permute-done.13.refs_3_ = bf16[4,384,256]{2,1,0:T(8,128)(2,1)S(1)} collective-permute-done((bf16[4,384,256]{2,1,0:T(8,128)(2,1)}, bf16[4,384,256]{2,1,0:T(8,128)(2,1)S(1)}, u32[]{:S(2)}, u32[]{:S(2)}) %collective-permute-start.13) | collective-permute-done | bytes 786464 | tf_op jit(solution)/shard_map/ppermute | solution.py:486
  212.3 3.2 %collective-permute-start.18 = (bf16[4,384,256]{2,1,0:T(8,128)(2,1)S(1)}, bf16[4,384,256]{2,1,0:T(8,128)(2,1)S(1)}, u32[]{:S(2)}, u32[]{:S(2)}) collective-permute-start(bf16[4,384,256]{2,1,0:T(8,128)(2,1)S(1)} %collective-permute-done.16.refs_6_), channel_id=1, source_target_pairs={{0,3},{1,0},{2,1},{3,2},{4,7},{5,4},{6,5},{7,6},{8,11},{9,8},{10,9... | collective-permute-start | bytes 2359304 | tf_op jit(solution)/shard_map/ppermute | solution.py:486
  215.6 13.6 %collective-permute-done.14.refs_4_ = bf16[4,384,256]{2,1,0:T(8,128)(2,1)S(1)} collective-permute-done((bf16[4,384,256]{2,1,0:T(8,128)(2,1)}, bf16[4,384,256]{2,1,0:T(8,128)(2,1)S(1)}, u32[]{:S(2)}, u32[]{:S(2)}) %collective-permute-start.14) | collective-permute-done | bytes 786464 | tf_op jit(solution)/shard_map/ppermute | solution.py:486
  229.2 16.1 %collective-permute-done.17.refs_7_ = bf16[4,384,256]{2,1,0:T(8,128)(2,1)S(1)} collective-permute-done((bf16[4,384,256]{2,1,0:T(8,128)(2,1)S(1)}, bf16[4,384,256]{2,1,0:T(8,128)(2,1)S(1)}, u32[]{:S(2)}, u32[]{:S(2)}) %collective-permute-start.17) | collective-permute-done | bytes 786464 | tf_op jit(solution)/shard_map/ppermute | solution.py:486
  247.6 3.5 %shared.1.shared_ref = f32[128,2048]{1,0:T(8,128)S(1)} custom-call(bf16[128,2048]{1,0:T(8,128)(2,1)S(1)} %copy-done.3, bf16[4,384,256]{2,1,0:T(8,128)(2,1)S(1)} %copy-done.1, bf16[4,384,256]{2,1,0:T(8,128)(2,1)S(1)} %copy-done.2, bf16[4,384,256]{2,1,0:T(8,128)(2,1)S(1)} %collective-permute-done.13.refs_3_, ...), custom_call_target="tpu_custom_call" | custom-call | flops 800000000 | bytes 8000000 | tf_op jit(solution)/shard_map/shared/pallas_call | solution.py:681
  (78 shorter events, 36.0 us)
Async XLA Ops:
  21.3 20.3 %all-to-all-start.1 = ((bf16[8,144,128]{2,1,0:T(8,128)(2,1)}), bf16[8,144,128]{2,1,0:T(8,128)(2,1)S(1)}, u32[]{:S(2)}, u32[]{:S(2)}) async-start(bf16[8,144,128]{2,1,0:T(8,128)(2,1)} %get-tuple-element.31), calls=%async_computation.1 | async-start | bytes 589824 | tf_op jit(solution)/shard_map/all_to_all | solution.py:581
  44.9 5.8 %collective-permute-start = (bf16[128,256]{1,0:T(8,128)(2,1)}, bf16[128,256]{1,0:T(8,128)(2,1)S(1)}, u32[]{:S(2)}, u32[]{:S(2)}) collective-permute-start(bf16[128,256]{1,0:T(8,128)(2,1)} %get-tuple-element.37), channel_id=1, source_target_pairs={{0,1},{1,2},{2,3},{3,0},{4,5},{5,6},{6,7},{7,4},{8,9},{9,10},{10,1... | collective-permute-start | bytes 196616 | tf_op jit(solution)/shard_map/ppermute | solution.py:486
  46.4 6.1 %collective-permute-start.1 = (bf16[128,256]{1,0:T(8,128)(2,1)}, bf16[128,256]{1,0:T(8,128)(2,1)S(1)}, u32[]{:S(2)}, u32[]{:S(2)}) collective-permute-start(bf16[128,256]{1,0:T(8,128)(2,1)} %get-tuple-element.38), channel_id=1, source_target_pairs={{0,2},{1,3},{2,0},{3,1},{4,6},{5,7},{6,4},{7,5},{8,10},{9,11},{10,... | collective-permute-start | bytes 196616 | tf_op jit(solution)/shard_map/ppermute | solution.py:486
  49.3 4.5 %collective-permute-start.2 = (bf16[128,256]{1,0:T(8,128)(2,1)}, bf16[128,256]{1,0:T(8,128)(2,1)S(1)}, u32[]{:S(2)}, u32[]{:S(2)}) collective-permute-start(bf16[128,256]{1,0:T(8,128)(2,1)} %get-tuple-element.39), channel_id=1, source_target_pairs={{0,3},{1,0},{2,1},{3,2},{4,7},{5,4},{6,5},{7,6},{8,11},{9,8},{10,9... | collective-permute-start | bytes 196616 | tf_op jit(solution)/shard_map/ppermute | solution.py:486
  61.8 83.4 %all-to-all-start.2 = ((bf16[64,96,128]{2,1,0:T(8,128)(2,1)}), bf16[64,96,128]{2,1,0:T(8,128)(2,1)S(1)}, u32[]{:S(2)}, u32[]{:S(2)}) async-start(bf16[64,96,128]{2,1,0:T(8,128)(2,1)} %bitcast.21), calls=%async_computation.2 | async-start | bytes 3145728 | tf_op jit(solution)/shard_map/all_to_all | solution.py:627
  67.4 27.6 %collective-permute-start.3 = (bf16[2048,256]{1,0:T(8,128)(2,1)}, bf16[2048,256]{1,0:T(8,128)(2,1)}, u32[]{:S(2)}, u32[]{:S(2)}) collective-permute-start(bf16[2048,256]{1,0:T(8,128)(2,1)} %bitcast.11.refs_1_), channel_id=1, source_target_pairs={{0,1},{1,2},{2,3},{3,0},{4,5},{5,6},{6,7},{7,4},{8,9},{9,10},{10,1... | collective-permute-start | bytes 3145736 | tf_op jit(solution)/shard_map/ppermute | solution.py:486
  67.8 27.2 %collective-permute-start.6 = (bf16[2048,256]{1,0:T(8,128)(2,1)}, bf16[2048,256]{1,0:T(8,128)(2,1)}, u32[]{:S(2)}, u32[]{:S(2)}) collective-permute-start(bf16[2048,256]{1,0:T(8,128)(2,1)} %bitcast.12.refs_4_), channel_id=1, source_target_pairs={{0,3},{1,0},{2,1},{3,2},{4,7},{5,4},{6,5},{7,6},{8,11},{9,8},{10,9... | collective-permute-start | bytes 3145736 | tf_op jit(solution)/shard_map/ppermute | solution.py:486
  70.7 46.7 %collective-permute-start.7 = (bf16[256,2048]{1,0:T(8,128)(2,1)}, bf16[256,2048]{1,0:T(8,128)(2,1)S(1)}, u32[]{:S(2)}, u32[]{:S(2)}) collective-permute-start(bf16[256,2048]{1,0:T(8,128)(2,1)} %bitcast.13.refs_7_), channel_id=1, source_target_pairs={{0,1},{1,2},{2,3},{3,0},{4,5},{5,6},{6,7},{7,4},{8,9},{9,10},{10,1... | collective-permute-start | bytes 3145736 | tf_op jit(solution)/shard_map/ppermute | solution.py:486
  70.7 48.9 %collective-permute-start.8 = (bf16[256,2048]{1,0:T(8,128)(2,1)}, bf16[256,2048]{1,0:T(8,128)(2,1)S(1)}, u32[]{:S(2)}, u32[]{:S(2)}) collective-permute-start(bf16[256,2048]{1,0:T(8,128)(2,1)} %bitcast.13.refs_7_), channel_id=1, source_target_pairs={{0,3},{1,0},{2,1},{3,2},{4,7},{5,4},{6,5},{7,6},{8,11},{9,8},{10,9... | collective-permute-start | bytes 3145736 | tf_op jit(solution)/shard_map/ppermute | solution.py:486
  74.0 65.6 %collective-permute-start.4 = (bf16[2048,256]{1,0:T(8,128)(2,1)}, bf16[2048,256]{1,0:T(8,128)(2,1)S(1)}, u32[]{:S(2)}, u32[]{:S(2)}) collective-permute-start(bf16[2048,256]{1,0:T(8,128)(2,1)} %bitcast.11.refs_1_), channel_id=1, source_target_pairs={{0,3},{1,0},{2,1},{3,2},{4,7},{5,4},{6,5},{7,6},{8,11},{9,8},{10,9... | collective-permute-start | bytes 3145736 | tf_op jit(solution)/shard_map/ppermute | solution.py:486
  95.0 49.1 %collective-permute-start.5 = (bf16[2048,256]{1,0:T(8,128)(2,1)}, bf16[2048,256]{1,0:T(8,128)(2,1)S(1)}, u32[]{:S(2)}, u32[]{:S(2)}) collective-permute-start(bf16[2048,256]{1,0:T(8,128)(2,1)} %bitcast.12.refs_4_), channel_id=1, source_target_pairs={{0,1},{1,2},{2,3},{3,0},{4,5},{5,6},{6,7},{7,4},{8,9},{9,10},{10,1... | collective-permute-start | bytes 3145736 | tf_op jit(solution)/shard_map/ppermute | solution.py:486
  95.0 77.7 %collective-permute-start.9 = (bf16[2048,256]{1,0:T(8,128)(2,1)}, bf16[2048,256]{1,0:T(8,128)(2,1)S(1)}, u32[]{:S(2)}, u32[]{:S(2)}) collective-permute-start(bf16[2048,256]{1,0:T(8,128)(2,1)} %collective-permute-done.3.refs_2_), channel_id=1, source_target_pairs={{0,1},{1,2},{2,3},{3,0},{4,5},{5,6},{6,7},{7,4},{8,9},{9,10},{10,1... | collective-permute-start | bytes 3145736 | tf_op jit(solution)/shard_map/ppermute | solution.py:486
  117.4 26.8 %copy-start.4 = (bf16[256,2048]{1,0:T(8,128)(2,1)}, bf16[256,2048]{1,0:T(8,128)(2,1)S(1)}, u32[]{:S(2)}) copy-start(bf16[256,2048]{1,0:T(8,128)(2,1)S(1)} %collective-permute-done.7.refs_8_) | copy-start | bytes 3145732
  117.4 55.3 %collective-permute-start.10 = (bf16[2048,256]{1,0:T(8,128)(2,1)}, bf16[2048,256]{1,0:T(8,128)(2,1)}, u32[]{:S(2)}, u32[]{:S(2)}) collective-permute-start(bf16[2048,256]{1,0:T(8,128)(2,1)} %collective-permute-done.6.refs_6_), channel_id=1, source_target_pairs={{0,3},{1,0},{2,1},{3,2},{4,7},{5,4},{6,5},{7,6},{8,11},{9,8},{10,9... | collective-permute-start | bytes 3145736 | tf_op jit(solution)/shard_map/ppermute | solution.py:486
  119.6 53.1 %collective-permute-start.11 = (bf16[128,2048]{1,0:T(8,128)(2,1)}, bf16[128,2048]{1,0:T(8,128)(2,1)S(1)}, u32[]{:S(2)}, u32[]{:S(2)}) collective-permute-start(bf16[128,2048]{1,0:T(8,128)(2,1)} %slice.8), channel_id=1, source_target_pairs={{0,1},{1,2},{2,3},{3,0},{4,5},{5,6},{6,7},{7,4},{8,9},{9,10},{10,1... | collective-permute-start | bytes 1572872 | tf_op jit(solution)/shard_map/ppermute | solution.py:486
  140.6 32.2 %collective-permute-start.12 = (bf16[128,2048]{1,0:T(8,128)(2,1)}, bf16[128,2048]{1,0:T(8,128)(2,1)}, u32[]{:S(2)}, u32[]{:S(2)}) collective-permute-start(bf16[128,2048]{1,0:T(8,128)(2,1)} %slice.9), channel_id=1, source_target_pairs={{0,3},{1,0},{2,1},{3,2},{4,7},{5,4},{6,5},{7,6},{8,11},{9,8},{10,9... | collective-permute-start | bytes 1572872 | tf_op jit(solution)/shard_map/ppermute | solution.py:486
  177.4 73.7 %all-to-all-start.3 = ((bf16[64,96,128]{2,1,0:T(8,128)(2,1)}), bf16[64,96,128]{2,1,0:T(8,128)(2,1)S(1)}, u32[]{:S(2)}, u32[]{:S(2)}) async-start(bf16[64,96,128]{2,1,0:T(8,128)(2,1)} %bitcast.14), calls=%async_computation.3 | async-start | bytes 3145728 | tf_op jit(solution)/shard_map/all_to_all | solution.py:671
  187.8 57.5 %copy-start.3 = (bf16[128,2048]{1,0:T(8,128)(2,1)S(1)}, bf16[128,2048]{1,0:T(8,128)(2,1)}, u32[]{:S(2)}) copy-start(bf16[128,2048]{1,0:T(8,128)(2,1)} %get-tuple-element.43.refs_0_) | copy-start | bytes 1572868
  190.5 21.8 %collective-permute-start.13 = (bf16[4,384,256]{2,1,0:T(8,128)(2,1)}, bf16[4,384,256]{2,1,0:T(8,128)(2,1)S(1)}, u32[]{:S(2)}, u32[]{:S(2)}) collective-permute-start(bf16[4,384,256]{2,1,0:T(8,128)(2,1)} %get-tuple-element.45.refs_1_), channel_id=1, source_target_pairs={{0,1},{1,2},{2,3},{3,0},{4,5},{5,6},{6,7},{7,4},{8,9},{9,10},{10,1... | collective-permute-start | bytes 2359304 | tf_op jit(solution)/shard_map/ppermute | solution.py:486
  191.3 21.0 %collective-permute-start.16 = (bf16[4,384,256]{2,1,0:T(8,128)(2,1)}, bf16[4,384,256]{2,1,0:T(8,128)(2,1)S(1)}, u32[]{:S(2)}, u32[]{:S(2)}) collective-permute-start(bf16[4,384,256]{2,1,0:T(8,128)(2,1)} %get-tuple-element.46.refs_2_), channel_id=1, source_target_pairs={{0,3},{1,0},{2,1},{3,2},{4,7},{5,4},{6,5},{7,6},{8,11},{9,8},{10,9... | collective-permute-start | bytes 2359304 | tf_op jit(solution)/shard_map/ppermute | solution.py:486
  193.7 35.5 %collective-permute-start.14 = (bf16[4,384,256]{2,1,0:T(8,128)(2,1)}, bf16[4,384,256]{2,1,0:T(8,128)(2,1)S(1)}, u32[]{:S(2)}, u32[]{:S(2)}) collective-permute-start(bf16[4,384,256]{2,1,0:T(8,128)(2,1)} %get-tuple-element.46.refs_2_), channel_id=1, source_target_pairs={{0,1},{1,2},{2,3},{3,0},{4,5},{5,6},{6,7},{7,4},{8,9},{9,10},{10,1... | collective-permute-start | bytes 2359304 | tf_op jit(solution)/shard_map/ppermute | solution.py:486
  193.7 35.5 %collective-permute-start.15 = (bf16[4,384,256]{2,1,0:T(8,128)(2,1)}, bf16[4,384,256]{2,1,0:T(8,128)(2,1)S(1)}, u32[]{:S(2)}, u32[]{:S(2)}) collective-permute-start(bf16[4,384,256]{2,1,0:T(8,128)(2,1)} %get-tuple-element.45.refs_1_), channel_id=1, source_target_pairs={{0,3},{1,0},{2,1},{3,2},{4,7},{5,4},{6,5},{7,6},{8,11},{9,8},{10,9... | collective-permute-start | bytes 2359304 | tf_op jit(solution)/shard_map/ppermute | solution.py:486
  212.3 33.0 %collective-permute-start.17 = (bf16[4,384,256]{2,1,0:T(8,128)(2,1)S(1)}, bf16[4,384,256]{2,1,0:T(8,128)(2,1)S(1)}, u32[]{:S(2)}, u32[]{:S(2)}) collective-permute-start(bf16[4,384,256]{2,1,0:T(8,128)(2,1)S(1)} %collective-permute-done.13.refs_3_), channel_id=1, source_target_pairs={{0,1},{1,2},{2,3},{3,0},{4,5},{5,6},{6,7},{7,4},{8,9},{9,10},{10,1... | collective-permute-start | bytes 2359304 | tf_op jit(solution)/shard_map/ppermute | solution.py:486
  212.3 33.0 %collective-permute-start.18 = (bf16[4,384,256]{2,1,0:T(8,128)(2,1)S(1)}, bf16[4,384,256]{2,1,0:T(8,128)(2,1)S(1)}, u32[]{:S(2)}, u32[]{:S(2)}) collective-permute-start(bf16[4,384,256]{2,1,0:T(8,128)(2,1)S(1)} %collective-permute-done.16.refs_6_), channel_id=1, source_target_pairs={{0,3},{1,0},{2,1},{3,2},{4,7},{5,4},{6,5},{7,6},{8,11},{9,8},{10,9... | collective-permute-start | bytes 2359304 | tf_op jit(solution)/shard_map/ppermute | solution.py:486
  (20 other events, 73.1 us)
